TPU v7x, 512 devices: a whole 4x4x16 slice. The times are simulated.
512 devices in a mesh: ep: 32 (over z, core), tp: 16 (over y, x).
Axes of the slice: x: 4, y: 4, z: 16, core: 2. Of those that a mesh axis runs over, the one named last changes fastest.
Arguments:
- gate_out: bfloat16 [8192, 1024], P('ep', 'tp'), may hold values from -6 to 6
- gate_in: bfloat16 [8192, 1024], P('ep', 'tp'), may hold values from -6 to 6
- conv_values: bfloat16 [8192, 1024], P('ep', 'tp'), may hold values from -6 to 6
- conv_taps: float32 [3, 1024], P(None, 'tp'), may hold values from -3 to 3
- mixer_proj: bfloat16 [1024, 2048], P('tp'), may hold values from -0.25 to 0.25
- expert_in: bfloat16 [8192, 2048], P('ep'), may hold values from -6 to 6
- norm_gain: float32 [2048], replicated, may hold values from 0.1 to 1.9
- route_ids: int32 [8192, 2], P('ep'), may hold values from 0 to 31, all different within a row; in each aligned block of 256 rows (0 to 255, 256 to 511, ...) at most 22 rows name the same one
- route_scores: float32 [8192, 2], P('ep'), may hold values from 0.1 to 1
- gate_proj: bfloat16 [32, 2048, 4096], P('ep', None, 'tp'), may hold values from -0.125 to 0.125
- up_proj: bfloat16 [32, 2048, 4096], P('ep', None, 'tp'), may hold values from -0.125 to 0.125
- down_proj: bfloat16 [32, 4096, 2048], P('ep', 'tp'), may hold values from -0.125 to 0.125
Outputs:
- mixed: bfloat16 [8192, 2048], P('ep', 'tp')
- expert_mix: bfloat16 [8192, 2048], P('ep', 'tp')
Inputs may be any that keep to these rules, and one draw needn't show every extreme that they name: `route_ids`: each row names 2 different experts. Within each aligned block of 256 rows (the rows of one device of ep) no expert is named by more than 22 rows, and in some block an expert is named by exactly 22 rows.
All inputs are finite; a program needn't handle non-finite values.
Results may differ from a plain program's by a relative error of at most 0.015.
Values may be sent and summed in bfloat16 or wider, within the bound.
No kernel may reach another device: no remote copies, remote signals or barrier semaphores. Data moves between devices by JAX's collectives and lax.ppermute only.
A program may use at most 64 MiB of HBM per device.

v0:
```python
import jax
import jax.numpy as jnp
from jax import lax
from jax.sharding import Mesh
from jax.sharding import PartitionSpec as P

TP = ("tp_0", "tp_1")


def shifted(block, axis, distance):
    devices = range(lax.axis_size(axis))
    route = [(i - distance, i) for i in devices if i - distance in devices]
    return lax.ppermute(block, axis, route)


def split_up(array, dim, peers):
    shape = array.shape
    parts = array.reshape(*shape[:dim], peers, shape[dim] // peers, *shape[dim + 1 :])
    return jnp.moveaxis(parts, dim, 0)


def sum_at_owner(array, axis, dim):
    peers = lax.axis_size(axis)
    parts = lax.all_to_all(split_up(array, dim, peers), axis, 0, 0, tiled=True)
    return jnp.sum(parts.astype(jnp.float32), axis=0)


def gathered_by_axis(array, axes, dim):
    result = array
    for number in range(len(axes) - 1, -1, -1):
        result = lax.all_gather(result, axes[number], axis=dim, tiled=True)
    return result


def slot_table(route_ids, experts_total, capacity):
    pairs = route_ids.reshape(-1)
    onehot = (pairs[:, None] == jnp.arange(experts_total, dtype=jnp.int32)[None, :]).astype(
        jnp.int32
    )
    before = jnp.cumsum(onehot, axis=0) - onehot
    ranking = jnp.sum(before * onehot, axis=1)
    return (pairs * capacity + ranking).reshape(route_ids.shape)


def shards(
    gate_out,
    gate_in,
    conv_values,
    conv_taps,
    mixer_proj,
    expert_in,
    norm_gain,
    route_ids,
    route_scores,
    gate_proj,
    up_proj,
    down_proj,
):
    product = gate_in.astype(jnp.float32) * conv_values.astype(jnp.float32)
    seq_len = product.shape[0]
    tap_count = conv_taps.shape[0]
    earlier = shifted(product[seq_len - (tap_count - 1) :], "ep", 1)
    padded = jnp.concatenate([earlier, product], axis=0)
    convolved = conv_taps[0] * padded[0:seq_len]
    for offset in range(1, tap_count):
        convolved = convolved + conv_taps[offset] * padded[offset : offset + seq_len]
    branch = (gate_out.astype(jnp.float32) * convolved).astype(jnp.bfloat16)
    partial_mix = jnp.dot(branch, mixer_proj, preferred_element_type=jnp.float32)
    mixed = sum_at_owner(partial_mix.astype(jnp.bfloat16), TP, 1).astype(jnp.bfloat16)
    rows_wide = expert_in.astype(jnp.float32)
    scaling = lax.rsqrt(jnp.mean(rows_wide * rows_wide, axis=1, keepdims=True) + 1e-06)
    normed = (rows_wide * scaling * norm_gain).astype(jnp.bfloat16)
    token_count = expert_in.shape[0]
    choose_count = route_ids.shape[1]
    model_width = expert_in.shape[1]
    ep_count = lax.axis_size("ep")
    local_experts = gate_proj.shape[0]
    experts_total = ep_count * local_experts
    capacity = max(
        2, (4 * token_count * choose_count + 3 * experts_total - 1) // (3 * experts_total)
    )
    slot_count = experts_total * capacity
    slots = slot_table(route_ids, experts_total, capacity)
    hits = slots[None, :, :] == jnp.arange(slot_count, dtype=jnp.int32)[:, None, None]
    dispatch = jnp.sum(hits.astype(jnp.int32), axis=2).astype(jnp.bfloat16)
    column_count = model_width // lax.axis_size(TP)
    own_columns = lax.dynamic_slice_in_dim(
        normed, lax.axis_index(TP) * column_count, column_count, 1
    )
    sent = jnp.dot(dispatch, own_columns, preferred_element_type=jnp.float32).astype(jnp.bfloat16)
    arrived = lax.all_to_all(sent, "ep", split_axis=0, concat_axis=0, tiled=True)
    piece = gathered_by_axis(arrived, TP, 1)
    grouped_piece = piece.reshape(ep_count, local_experts, capacity, piece.shape[1])
    gate_part = jnp.einsum(
        "secd,edf->secf", grouped_piece, gate_proj, preferred_element_type=jnp.float32
    )
    up_part = jnp.einsum(
        "secd,edf->secf", grouped_piece, up_proj, preferred_element_type=jnp.float32
    )
    hidden = (jax.nn.silu(gate_part) * up_part).astype(jnp.bfloat16)
    partial_out = jnp.einsum(
        "secf,efd->secd", hidden, down_proj, preferred_element_type=jnp.float32
    )
    summed = sum_at_owner(partial_out.astype(jnp.bfloat16), TP, 3).astype(jnp.bfloat16)
    returned = lax.all_to_all(summed, "ep", split_axis=0, concat_axis=0, tiled=True)
    slot_rows = returned.reshape(slot_count, returned.shape[3])
    picked = jnp.take(slot_rows, slots.reshape(-1), axis=0).reshape(
        token_count, choose_count, slot_rows.shape[1]
    )
    weights = route_scores / jnp.sum(route_scores, axis=1, keepdims=True)
    expert_mix = jnp.sum(weights[:, :, None] * picked.astype(jnp.float32), axis=1).astype(
        jnp.bfloat16
    )
    return (mixed, expert_mix)


def solution(mesh):
    torus = Mesh(mesh.devices.reshape(mesh.shape["ep"], 4, 4), ("ep", "tp_0", "tp_1"))
    in_specs = (
        P("ep", TP),
        P("ep", TP),
        P("ep", TP),
        P(None, TP),
        P(TP, None),
        P("ep", None),
        P(),
        P("ep", None),
        P("ep", None),
        P("ep", None, TP),
        P("ep", None, TP),
        P("ep", TP, None),
    )
    out_specs = (P("ep", TP), P("ep", TP))
    return jax.shard_map(
        shards, mesh=torus, in_specs=in_specs, out_specs=out_specs, check_vma=False
    )
```

profile of v0, /device:TPU:1, one launch (start us, length us, event | category | flops | bytes accessed | tf_op | source)
XLA Modules:
  0.0 228.1 jit_solution(6024917854152906022)
XLA Ops:
  7.2 0.0 copy-start
  7.2 0.0 all-gather.2.cloned.1.call-start
  7.3 0.9 copy.47
  8.2 0.1 eq.39
  8.3 0.1 reshape.119
  8.5 2.8 %convert_element_type.71 = f32[256,2048]{1,0:T(8,128)} convert(bf16[256,2048]{1,0:T(8,128)(2,1)} %param.17) | non-fusion elementwise | flops 524288 | bytes 3145728 | tf_op jit(solution)/shard_map/convert_element_type | solution.py:70
  11.3 0.3 multiply_reduce_fusion
  11.6 1.2 reduce-window.6
  12.8 0.2 slice_reduce_fusion
  13.1 0.1 fusion.21
  13.2 0.1 reduce_sum.78
  13.3 0.1 copy.50
  13.4 0.3 convert_reduce_fusion
  13.7 0.8 dynamic-slice
  14.5 1.2 convolution_convert_fusion.2
  15.7 0.1 all_to_all.18
  15.8 35.3 %all_to_all.27 = bf16[32,22,128]{2,1,0:T(8,128)(2,1)S(1)} all-to-all(bf16[32,22,128]{2,1,0:T(8,128)(2,1)S(1)} %all_to_all.18), channel_id=1, replica_groups=mesh['ep'=32,'tp_0'=4,'tp_1'=4] {'ep'}, dimensions={0} | all-to-all | bytes 360448 | tf_op jit(solution)/shard_map/all_to_all | solution.py:91
  51.1 0.1 all_to_all.20
  51.2 14.9 %all_gather.6 = bf16[704,512]{1,0:T(8,128)(2,1)} all-gather(bf16[704,128]{1,0:T(8,128)(2,1)S(1)} %all_to_all.20), channel_id=1, replica_groups=mesh['ep'=32,'tp_0'=4,'tp_1'=4] {'tp_1'}, dimensions={1}, use_global_device_ids=true | all-gather | bytes 901120 | tf_op jit(solution)/shard_map/all_gather | solution.py:31
  66.1 0.0 all-gather.2.cloned.1.call-update
  66.1 38.2 %all-gather.2.cloned.1.call-done = bf16[704,2048]{1,0:T(8,128)(2,1)} async-done(((bf16[704,512]{1,0:T(8,128)(2,1)}), bf16[704,2048]{1,0:T(8,128)(2,1)}) %all-gather.2.cloned.1.call-update) | async-done | bytes 2883600 | tf_op jit(solution)/shard_map/all_gather | solution.py:31
  104.4 4.4 %reshape.121 = bf16[32,22,2048]{2,1,0:T(8,128)(2,1)} reshape(bf16[704,2048]{1,0:T(8,128)(2,1)} %all-gather.2.cloned.1.call-done) | data formatting | bytes 5767168 | tf_op jit(solution)/shard_map/reshape.5
  108.8 3.0 %convolution_bitcast_fusion.1 = f32[32,1,22,256]{3,2,0,1:T(8,128)S(1)} fusion(bf16[32,22,2048]{2,1,0:T(8,128)(2,1)} %reshape.121, bf16[1,2048,256]{2,1,0:T(8,128)(2,1)S(1)} %copy-done.10), kind=kOutput, calls=%fused_computation.10 | convolution fusion | flops 738197504 | bytes 4653056 | tf_op jit(solution)/shard_map/secd,edf->secf/dot_general | solution.py:94
  111.8 0.1 copy-done.11
  111.9 1.1 fusion.4
  113.0 0.9 fusion
  113.9 2.4 %copy.66 = bf16[1,22,4,16,8,128]{5,4,2,1,0,3:T(8,128)(2,1)} copy(bf16[1,22,4,16,8,128]{5,4,3,2,1,0:T(8,128)(2,1)S(1)} %fusion) | data formatting | bytes 5767168 | tf_op jit(solution)/shard_map/reshape | solution.py:18
  116.3 5.6 %all-to-all-start.2 = ((bf16[16,32,1,22,128]{4,1,3,2,0:T(8,128)(2,1)}), bf16[16,32,1,22,128]{4,1,3,2,0:T(8,128)(2,1)}, u32[]{:S(2)}, u32[]{:S(2)}) async-start(bf16[16,32,1,22,128]{4,1,3,2,0:T(8,128)(2,1)} %bitcast.85), calls=%async_computation.2 | async-start | bytes 5767168 | tf_op jit(solution)/shard_map/all_to_all | solution.py:24
  121.9 0.1 slice.34
  122.0 4.2 %collective-permute-start = (f32[2,64]{0,1:T(8,128)S(1)}, f32[2,64]{0,1:T(8,128)S(1)}, u32[]{:S(2)}, u32[]{:S(2)}) collective-permute-start(f32[2,64]{0,1:T(8,128)S(1)} %slice.34), channel_id=1, source_target_pairs={{0,16},{16,32},{32,48},{48,64},{64,80},{80,96},{96,112},{112,128},... | collective-permute-start | bytes 1544 | tf_op jit(solution)/shard_map/ppermute | solution.py:13
  126.2 1.0 collective-permute-done
  127.2 0.6 fusion.1
  127.8 1.3 copy.67
  129.0 35.4 %all-to-all-done.2 = bf16[16,32,1,22,128]{4,1,3,2,0:T(8,128)(2,1)} async-done(((bf16[16,32,1,22,128]{4,1,3,2,0:T(8,128)(2,1)}), bf16[16,32,1,22,128]{4,1,3,2,0:T(8,128)(2,1)}, u32[]{:S(2)}, u32[]{:S(2)}) %all-to-all-start.2) | async-done | bytes 2883616 | tf_op jit(solution)/shard_map/all_to_all | solution.py:24
  164.4 3.8 %all-to-all-start = ((bf16[16,256,128]{2,1,0:T(8,128)(2,1)}), bf16[16,256,128]{2,1,0:T(8,128)(2,1)S(1)}, u32[]{:S(2)}, u32[]{:S(2)}) async-start(bf16[16,256,128]{2,1,0:T(8,128)(2,1)} %bitcast.84), calls=%async_computation | async-start | bytes 2097152 | tf_op jit(solution)/shard_map/all_to_all | solution.py:24
  168.2 2.2 reduce_sum.81
  170.4 0.7 copy.55
  171.2 12.0 %all-to-all-done = bf16[16,256,128]{2,1,0:T(8,128)(2,1)S(1)} async-done(((bf16[16,256,128]{2,1,0:T(8,128)(2,1)}), bf16[16,256,128]{2,1,0:T(8,128)(2,1)S(1)}, u32[]{:S(2)}, u32[]{:S(2)}) %all-to-all-start) | async-done | bytes 1048608 | tf_op jit(solution)/shard_map/all_to_all | solution.py:24
  183.2 15.8 %all-to-all-start.3 = ((bf16[32,1,22,128]{3,2,1,0:T(8,128)(2,1)}), bf16[32,1,22,128]{3,2,1,0:T(8,128)(2,1)S(1)}, u32[]{:S(2)}, u32[]{:S(2)}) async-start(bf16[32,1,22,128]{3,2,1,0:T(8,128)(2,1)} %copy.55), calls=%async_computation.3 | async-start | bytes 393216 | tf_op jit(solution)/shard_map/all_to_all | solution.py:105
  199.0 0.1 copy.56
  199.1 0.1 mul.124
  199.3 0.2 copy.51
  199.5 0.1 copy.46
  199.7 0.8 reduce_sum.75
  200.4 17.3 %all-to-all-done.3 = bf16[32,1,22,128]{3,2,1,0:T(8,128)(2,1)S(1)} async-done(((bf16[32,1,22,128]{3,2,1,0:T(8,128)(2,1)}), bf16[32,1,22,128]{3,2,1,0:T(8,128)(2,1)S(1)}, u32[]{:S(2)}, u32[]{:S(2)}) %all-to-all-start.3) | async-done | bytes 180256 | tf_op jit(solution)/shard_map/all_to_all | solution.py:105
  217.7 0.1 reshape.127
  217.8 1.3 gather_fusion
  219.1 2.1 multiply_reduce_fusion.1
  (34 shorter events, 0.2 us)
Async XLA Ops:
  7.2 105.8 %copy-start = (bf16[1,256,2048]{2,1,0:T(8,128)(2,1)S(1)}, bf16[1,256,2048]{2,1,0:T(8,128)(2,1)}, u32[]{:S(2)}) copy-start(bf16[1,256,2048]{2,1,0:T(8,128)(2,1)} %param.23) | copy-start | bytes 3145732
  7.2 6.2 %copy-start.7 = (s32[256,2]{0,1:T(2,128)S(1)}, s32[256,2]{0,1:T(2,128)}, u32[]{:S(2)}) copy-start(s32[256,2]{0,1:T(2,128)} %param.19) | copy-start | bytes 6148
  7.2 4.1 %copy-start.1 = (bf16[256,2048]{1,0:T(8,128)(2,1)S(1)}, bf16[256,2048]{1,0:T(8,128)(2,1)}, u32[]{:S(2)}) copy-start(bf16[256,2048]{1,0:T(8,128)(2,1)} %param.17) | copy-start | bytes 3145732
  7.2 97.2 %all-gather.2.cloned.1.call-start = ((), (), s32[]{:S(2)}) async-start(), calls=%async_computation.4 | async-start | bytes 3604480 | tf_op jit(solution)/shard_map/all_gather | solution.py:31
  66.1 42.7 %copy-start.10 = (bf16[1,2048,256]{2,1,0:T(8,128)(2,1)S(1)}, bf16[1,2048,256]{2,1,0:T(8,128)(2,1)}, u32[]{:S(2)}) copy-start(bf16[1,2048,256]{2,1,0:T(8,128)(2,1)} %param.21) | copy-start | bytes 3145732
  108.8 3.0 %copy-start.2 = (bf16[32,22,2048]{2,1,0:T(8,128)(2,1)S(1)}, bf16[32,22,2048]{2,1,0:T(8,128)(2,1)}, u32[]{:S(2)}) copy-start(bf16[32,22,2048]{2,1,0:T(8,128)(2,1)} %reshape.121) | copy-start | bytes 8650756
  108.8 3.1 %copy-start.11 = (bf16[1,2048,256]{2,1,0:T(8,128)(2,1)S(1)}, bf16[1,2048,256]{2,1,0:T(8,128)(2,1)}, u32[]{:S(2)}) copy-start(bf16[1,2048,256]{2,1,0:T(8,128)(2,1)} %param.22) | copy-start | bytes 3145732
  116.3 5.6 %copy-start.5 = (bf16[256,64]{0,1:T(8,128)(2,1)S(1)}, bf16[256,64]{0,1:T(8,128)(2,1)}, u32[]{:S(2)}) copy-start(bf16[256,64]{0,1:T(8,128)(2,1)} %param.14) | copy-start | bytes 98308
  116.3 5.6 %copy-start.6 = (bf16[256,64]{0,1:T(8,128)(2,1)S(1)}, bf16[256,64]{0,1:T(8,128)(2,1)}, u32[]{:S(2)}) copy-start(bf16[256,64]{0,1:T(8,128)(2,1)} %param.13) | copy-start | bytes 98308
  116.3 9.9 %copy-start.9 = (f32[3,64]{1,0:T(4,128)S(1)}, f32[3,64]{1,0:T(4,128)}, u32[]{:S(2)}) copy-start(f32[3,64]{1,0:T(4,128)} %param.15) | copy-start | bytes 2308
  116.3 10.9 %copy-start.3 = (bf16[64,2048]{1,0:T(8,128)(2,1)S(1)}, bf16[64,2048]{1,0:T(8,128)(2,1)}, u32[]{:S(2)}) copy-start(bf16[64,2048]{1,0:T(8,128)(2,1)} %param.16) | copy-start | bytes 786436
  116.3 10.9 %copy-start.4 = (bf16[256,64]{0,1:T(8,128)(2,1)S(1)}, bf16[256,64]{0,1:T(8,128)(2,1)}, u32[]{:S(2)}) copy-start(bf16[256,64]{0,1:T(8,128)(2,1)} %param.12) | copy-start | bytes 98308
  116.3 48.1 %all-to-all-start.2 = ((bf16[16,32,1,22,128]{4,1,3,2,0:T(8,128)(2,1)}), bf16[16,32,1,22,128]{4,1,3,2,0:T(8,128)(2,1)}, u32[]{:S(2)}, u32[]{:S(2)}) async-start(bf16[16,32,1,22,128]{4,1,3,2,0:T(8,128)(2,1)} %bitcast.85), calls=%async_computation.2 | async-start | bytes 5767168 | tf_op jit(solution)/shard_map/all_to_all | solution.py:24
  122.0 5.2 %collective-permute-start = (f32[2,64]{0,1:T(8,128)S(1)}, f32[2,64]{0,1:T(8,128)S(1)}, u32[]{:S(2)}, u32[]{:S(2)}) collective-permute-start(f32[2,64]{0,1:T(8,128)S(1)} %slice.34), channel_id=1, source_target_pairs={{0,16},{16,32},{32,48},{48,64},{64,80},{80,96},{96,112},{112,128},... | collective-permute-start | bytes 1544 | tf_op jit(solution)/shard_map/ppermute | solution.py:13
  164.4 35.0 %copy-start.8 = (f32[256,2]{0,1:T(2,128)S(1)}, f32[256,2]{0,1:T(2,128)}, u32[]{:S(2)}) copy-start(f32[256,2]{0,1:T(2,128)} %param.20) | copy-start | bytes 6148
  164.4 18.7 %all-to-all-start = ((bf16[16,256,128]{2,1,0:T(8,128)(2,1)}), bf16[16,256,128]{2,1,0:T(8,128)(2,1)S(1)}, u32[]{:S(2)}, u32[]{:S(2)}) async-start(bf16[16,256,128]{2,1,0:T(8,128)(2,1)} %bitcast.84), calls=%async_computation | async-start | bytes 2097152 | tf_op jit(solution)/shard_map/all_to_all | solution.py:24
  183.2 34.6 %all-to-all-start.3 = ((bf16[32,1,22,128]{3,2,1,0:T(8,128)(2,1)}), bf16[32,1,22,128]{3,2,1,0:T(8,128)(2,1)S(1)}, u32[]{:S(2)}, u32[]{:S(2)}) async-start(bf16[32,1,22,128]{3,2,1,0:T(8,128)(2,1)} %copy.55), calls=%async_computation.3 | async-start | bytes 393216 | tf_op jit(solution)/shard_map/all_to_all | solution.py:105
Sparse Core Ops, SparseCore 0:
  66.2 38.0 all-gather.1
where the time goes:
time: 229 us; the launch traced here: 228 us
  waiting for transfers between devices  104 us (45%)
  blocking collectives  50.2 us (22%)
  starting transfers between devices  29.4 us (13%)
  between operations  14.3 us (6%)
  local copies, waits for them, and re-layouts  13.6 us (6%)
  other arithmetic  9.89 us (4%)
  matrix products  6.79 us (3%)
    all_to_all x2, waiting for transfers between devices, sum_at_owner(): parts = lax.all_to_all(split_up(array, dim, peers), axis, 0, 0, tiled=True)  47.3 us
    all_gather x1, waiting for transfers between devices, gathered_by_axis(): result = lax.all_gather(result, axes[number], axis=dim, tiled=True)  38.2 us
    all_to_all x1, blocking collectives, shards(): lax.all_to_all(sent, 'ep', split_axis=0, concat_axis=0, tiled=True)  35.3 us
    all_to_all x1, waiting for transfers between devices, shards(): lax.all_to_all(summed, 'ep', split_axis=0, concat_axis=0, tiled=True)  17.3 us
    all_to_all x1, starting transfers between devices, shards(): lax.all_to_all(summed, 'ep', split_axis=0, concat_axis=0, tiled=True)  15.8 us
    all_gather x1, blocking collectives, gathered_by_axis(): result = lax.all_gather(result, axes[number], axis=dim, tiled=True)  14.9 us
    all_to_all x2, starting transfers between devices, sum_at_owner(): parts = lax.all_to_all(split_up(array, dim, peers), axis, 0, 0, tiled=True)  9.36 us
  transfers between devices with their start and end apart: 5, of which 5 were waited for; matrix products, arithmetic and copies ran while one was open for 3% of the time, Pallas kernels for 0%

commit v1 on v0

v1 whole, which is shorter than its diff:
```python
import jax
import jax.numpy as jnp
from jax import lax
from jax.experimental import pallas as pl
from jax.experimental.pallas import tpu as pltpu
from jax.sharding import Mesh
from jax.sharding import PartitionSpec as P

TP = ("tp_0", "tp_1")
F32 = jnp.float32
BF16 = jnp.bfloat16
VMEM = pl.BlockSpec(memory_space=pltpu.VMEM)
SMEM = pl.BlockSpec(memory_space=pltpu.SMEM)


def shifted(block, axis, distance):
    devices = range(lax.axis_size(axis))
    route = [(i - distance, i) for i in devices if i - distance in devices]
    return lax.ppermute(block, axis, route)


def call(body, out, limit, flops, *operands, specs=None):
    return pl.pallas_call(
        body,
        out_shape=out,
        in_specs=specs or [VMEM] * len(operands),
        out_specs=jax.tree.map(lambda _: VMEM, out),
        compiler_params=pltpu.CompilerParams(vmem_limit_bytes=limit),
        cost_estimate=pl.CostEstimate(
            flops=flops, bytes_accessed=1 << 20, transcendentals=0
        ),
    )(*operands)


def dispatch_body(capacity, experts, place, rows, gain, ids, sent, slots):
    tokens, width = rows.shape
    columns = sent.shape[1]
    wide = rows[...].astype(F32)
    scaling = lax.rsqrt(jnp.sum(wide * wide, axis=1, keepdims=True) / width + 1e-06)
    start = pl.multiple_of(place[0] * columns, columns)
    own = rows[:, pl.ds(start, columns)].astype(F32)
    normed = (own * scaling * gain[:, pl.ds(start, columns)]).astype(BF16)
    chosen = ids[...]
    expert = lax.broadcasted_iota(jnp.int32, (experts, tokens), 0)
    hits = [expert == chosen[k : k + 1, :] for k in range(chosen.shape[0])]
    marks = [jnp.where(h, 1.0, 0.0).astype(F32) for h in hits]
    total = marks[0]
    for m in marks[1:]:
        total = total + m
    earlier = lax.broadcasted_iota(jnp.int32, (tokens, tokens), 0)
    later = lax.broadcasted_iota(jnp.int32, (tokens, tokens), 1)
    before = jnp.dot(
        total.astype(BF16),
        jnp.where(earlier < later, 1.0, 0.0).astype(BF16),
        preferred_element_type=F32,
    )
    base = (expert * capacity).astype(F32)
    where = [
        jnp.sum(m * (before + base), axis=0, keepdims=True).astype(jnp.int32) for m in marks
    ]
    slots[...] = jnp.concatenate(where, axis=0)
    slot = lax.broadcasted_iota(jnp.int32, (sent.shape[0], tokens), 0)
    table = slot == where[0]
    for w in where[1:]:
        table = table | (slot == w)
    sent[...] = jnp.dot(
        jnp.where(table, 1.0, 0.0).astype(BF16), normed, preferred_element_type=F32
    ).astype(BF16)


def expert_body(step, tokens, gate_w, up_w, down_w, branch, mixer_w, out):
    blocks, rows, columns = tokens.shape

    def tile(number, carry):
        at = pl.ds(pl.multiple_of(number * step, step), step)
        left = jnp.concatenate([tokens[b, at, :] for b in range(blocks)], axis=1)
        gate = jnp.dot(left, gate_w[...], preferred_element_type=F32)
        up = jnp.dot(left, up_w[...], preferred_element_type=F32)
        hidden = (gate / (1.0 + jnp.exp(-gate)) * up).astype(BF16)
        part = jnp.dot(hidden, down_w[...], preferred_element_type=F32).astype(BF16)
        for b in range(blocks):
            out[b, at, :] = part[:, b * columns : (b + 1) * columns]
        return carry

    lax.fori_loop(0, rows // step, tile, 0)
    part = jnp.dot(branch[...], mixer_w[...], preferred_element_type=F32).astype(BF16)
    for b in range(blocks):
        out[b, rows:, :] = part[:, b * columns : (b + 1) * columns]


def total_body(parts, outputs, mixed):
    rows = outputs.shape[0]
    total = parts[0].astype(F32)
    for b in range(1, parts.shape[0]):
        total = total + parts[b].astype(F32)
    total = total.astype(BF16)
    outputs[...] = total[:rows]
    mixed[...] = total[rows:]


def combine_body(rows, slots, scores, out):
    tokens = out.shape[0]
    slot = lax.broadcasted_iota(jnp.int32, (tokens, rows.shape[0]), 1)
    held = rows[...]
    score = scores[...]
    whole = jnp.sum(score, axis=1, keepdims=True)
    total = None
    for k in range(score.shape[1]):
        pick = jnp.where(slot == slots[:, k : k + 1], 1.0, 0.0).astype(BF16)
        term = jnp.dot(pick, held, preferred_element_type=F32)
        term = term * (score[:, k : k + 1] / whole)
        total = term if total is None else total + term
    out[...] = total.astype(BF16)


def shards(
    gate_out,
    gate_in,
    conv_values,
    conv_taps,
    mixer_proj,
    expert_in,
    norm_gain,
    route_ids,
    route_scores,
    gate_proj,
    up_proj,
    down_proj,
):
    tokens, choices = route_ids.shape
    width = expert_in.shape[1]
    ep_count = lax.axis_size("ep")
    tp_count = lax.axis_size(TP)
    local_experts = gate_proj.shape[0]
    experts = ep_count * local_experts
    capacity = max(2, (4 * tokens * choices + 3 * experts - 1) // (3 * experts))
    slot_count = experts * capacity
    columns = width // tp_count
    place = lax.axis_index(TP).astype(jnp.int32).reshape(1)

    sent, slots = call(
        lambda *refs: dispatch_body(capacity, experts, *refs),
        (
            jax.ShapeDtypeStruct((slot_count, columns), BF16),
            jax.ShapeDtypeStruct((choices, tokens), jnp.int32),
        ),
        16 << 20,
        1 << 28,
        place,
        expert_in,
        norm_gain.reshape(1, width),
        route_ids.T,
        specs=[SMEM, VMEM, VMEM, VMEM],
    )
    arrived = lax.all_to_all(
        sent.reshape(experts, capacity, columns), "ep", split_axis=0, concat_axis=0, tiled=True
    )
    own_block = arrived.reshape(1, slot_count, columns)
    copies = jnp.broadcast_to(own_block, (tp_count, slot_count, columns))
    gathered = lax.all_to_all(copies, TP, 0, 0, tiled=True)

    product = gate_in.astype(F32) * conv_values.astype(F32)
    seq_len = product.shape[0]
    tap_count = conv_taps.shape[0]
    earlier = shifted(product[seq_len - (tap_count - 1) :], "ep", 1)
    padded = jnp.concatenate([earlier, product], axis=0)
    convolved = conv_taps[0] * padded[0:seq_len]
    for offset in range(1, tap_count):
        convolved = convolved + conv_taps[offset] * padded[offset : offset + seq_len]
    branch = (gate_out.astype(F32) * convolved).astype(BF16)

    step = slot_count // 4
    parts = call(
        lambda *refs: expert_body(step, *refs),
        jax.ShapeDtypeStruct((tp_count, slot_count + seq_len, columns), BF16),
        24 << 20,
        1 << 32,
        gathered,
        gate_proj[0],
        up_proj[0],
        down_proj[0],
        branch,
        mixer_proj,
    )
    shared = lax.all_to_all(parts, TP, 0, 0, tiled=True)
    outputs, mixed = call(
        total_body,
        (
            jax.ShapeDtypeStruct((slot_count, columns), BF16),
            jax.ShapeDtypeStruct((seq_len, columns), BF16),
        ),
        16 << 20,
        1 << 24,
        shared,
    )
    returned = lax.all_to_all(
        outputs.reshape(experts, capacity, columns), "ep", split_axis=0, concat_axis=0, tiled=True
    )
    expert_mix = call(
        combine_body,
        jax.ShapeDtypeStruct((tokens, columns), BF16),
        16 << 20,
        1 << 27,
        returned.reshape(slot_count, columns),
        slots.T,
        route_scores,
    )
    return (mixed, expert_mix)


def solution(mesh):
    torus = Mesh(mesh.devices.reshape(mesh.shape["ep"], 4, 4), ("ep", "tp_0", "tp_1"))
    in_specs = (
        P("ep", TP),
        P("ep", TP),
        P("ep", TP),
        P(None, TP),
        P(TP, None),
        P("ep", None),
        P(),
        P("ep", None),
        P("ep", None),
        P("ep", None, TP),
        P("ep", None, TP),
        P("ep", TP, None),
    )
    out_specs = (P("ep", TP), P("ep", TP))
    return jax.shard_map(
        shards, mesh=torus, in_specs=in_specs, out_specs=out_specs, check_vma=False
    )
```

time: 229 us -> 179 us (0.78)
  waiting for transfers between devices: 104 us -> 54.9 us
  blocking collectives: 50.2 us -> 85.9 us
  between operations: 14.3 us -> 0.84 us
  other arithmetic: 9.89 us -> 0.08 us
  starting transfers between devices: 29.4 us -> 20.4 us
  matrix products: 6.79 us -> 0 us
  Pallas kernels: 0 us -> 6.31 us
  local copies, waits for them, and re-layouts: 13.6 us -> 9.92 us
    all_to_all x1 -> x2, blocking collectives: 35.3 us -> 85.9 us  [the longest x1 50.6 us: shards(): shared = lax.all_to_all(parts, TP, 0, 0, tiled=True)]
    all_gather x1 -> x0, waiting for transfers between devices: 38.2 us -> none  [gathered_by_axis(): result = lax.all_gather(result, axes[number], axis=dim, tiled=True)]
    all_gather x1 -> x0, blocking collectives: 14.9 us -> none  [gathered_by_axis(): result = lax.all_gather(result, axes[number], axis=dim, tiled=True)]
    all_to_all x3 -> x2, waiting for transfers between devices: 64.6 us -> 54.4 us  [the longest x1 35.9 us: shards(): gathered = lax.all_to_all(copies, TP, 0, 0, tiled=True)]
    all_to_all x3 -> x2, starting transfers between devices: 25.2 us -> 17.1 us  [the longest x1 10.2 us: shards(): lax.all_to_all(outputs.reshape(experts, capacity, columns), 'ep', split_a...]
    dot_general x5 -> x0, matrix products: 6.79 us -> none  [the longest x1 3.02 us: shards(): jnp.einsum('secd,edf->secf', grouped_piece, gate_proj, preferred_element_...]
    pallas_call x0 -> x4, Pallas kernels: none -> 6.31 us  [call(): pl.pallas_call(body, out_shape=out, in_specs=specs or [VMEM] * len(operan...]
    reduce_sum x7 -> x0, other arithmetic: 5.79 us -> none  [the longest x2 3.01 us: sum_at_owner(): return jnp.sum(parts.astype(jnp.float32), axis=0)]
  transfers between devices with their start and end apart: 5 -> 3, of which waited for: 5 -> 3; matrix products, arithmetic and copies ran while one was open for 3% -> 0% of each run, Pallas kernels for 0% -> 0%
where the time goes in v1:
time: 179 us; the launch traced here: 178 us
  blocking collectives  85.9 us (48%)
  waiting for transfers between devices  54.9 us (31%)
  starting transfers between devices  20.4 us (11%)
  local copies, waits for them, and re-layouts  9.92 us (6%)
  Pallas kernels  6.31 us (4%)
    all_to_all x1, blocking collectives, shards(): shared = lax.all_to_all(parts, TP, 0, 0, tiled=True)  50.6 us
    all_to_all x1, waiting for transfers between devices, shards(): gathered = lax.all_to_all(copies, TP, 0, 0, tiled=True)  35.9 us
    all_to_all x1, blocking collectives, shards(): lax.all_to_all(sent.reshape(experts, capacity, columns), 'ep', split_axis...  35.3 us
    all_to_all x1, waiting for transfers between devices, shards(): lax.all_to_all(outputs.reshape(experts, capacity, columns), 'ep', split_a...  18.5 us
    all_to_all x1, starting transfers between devices, shards(): lax.all_to_all(outputs.reshape(experts, capacity, columns), 'ep', split_a...  10.2 us
    all_to_all x1, starting transfers between devices, shards(): gathered = lax.all_to_all(copies, TP, 0, 0, tiled=True)  6.89 us
    unnamed x27, local copies, waits for them, and re-layouts  6.66 us
    pallas_call x4, Pallas kernels, call(): pl.pallas_call(body, out_shape=out, in_specs=specs or [VMEM] * len(operan...  6.31 us
  transfers between devices with their start and end apart: 3, of which 3 were waited for; matrix products, arithmetic and copies ran while one was open for 0% of the time, Pallas kernels for 0%

profile of v1, /device:TPU:1, one launch (start us, length us, event | category | flops | bytes accessed | tf_op | source)
XLA Modules:
  0.0 178.4 jit_solution(9589190263414208371)
XLA Ops:
  0.6 0.0 copy-start
  0.6 1.2 copy-done
  1.9 0.0 copy-start.1
  1.9 0.7 copy-done.1
  2.6 0.0 copy-start.2
  2.6 0.7 copy-done.2
  3.2 0.6 shard_map.131
  3.9 0.1 reshape.23
  3.9 35.3 %all_to_all.20 = bf16[32,22,128]{2,1,0:T(8,128)(2,1)S(1)} all-to-all(bf16[32,22,128]{2,1,0:T(8,128)(2,1)S(1)} %reshape.23), channel_id=1, replica_groups=mesh['ep'=32,'tp_0'=4,'tp_1'=4] {'ep'}, dimensions={0} | all-to-all | bytes 360448 | tf_op jit(solution)/shard_map/all_to_all | solution.py:155
  39.3 0.1 broadcast_in_dim.7
  39.3 0.0 copy-start.7
  39.3 0.0 copy-start.8
  39.3 0.0 copy-start.11
  39.3 0.0 copy-start.9
  39.4 2.1 %broadcast_in_dim.8 = bf16[16,704,128]{2,1,0:T(8,128)(2,1)} broadcast(bf16[704,128]{1,0:T(8,128)(2,1)S(1)} %broadcast_in_dim.7), dimensions={1,2} | broadcast | bytes 3063808 | tf_op jit(solution)/shard_map/broadcast_in_dim | solution.py:159
  41.5 0.0 copy-start.6
  41.5 6.9 %all-to-all-start.1 = ((bf16[16,704,128]{2,1,0:T(8,128)(2,1)}), bf16[16,704,128]{2,1,0:T(8,128)(2,1)S(1)}, u32[]{:S(2)}, u32[]{:S(2)}) async-start(bf16[16,704,128]{2,1,0:T(8,128)(2,1)} %broadcast_in_dim.8), calls=%async_computation.1 | async-start | bytes 5767168 | tf_op jit(solution)/shard_map/all_to_all | solution.py:160
  48.4 0.0 copy-done.7
  48.4 0.1 copy.24
  48.5 0.0 copy-done.8
  48.5 0.1 copy.25
  48.7 3.3 %collective-permute-start = (f32[2,64]{1,0:T(2,128)S(1)}, f32[2,64]{1,0:T(2,128)S(1)}, u32[]{:S(2)}, u32[]{:S(2)}) collective-permute-start(f32[2,64]{1,0:T(2,128)S(1)} %slice.24), channel_id=1, source_target_pairs={{0,16},{16,32},{32,48},{48,64},{64,80},{80,96},{96,112},{112,128},... | collective-permute-start | bytes 1544 | tf_op jit(solution)/shard_map/ppermute | solution.py:19
  52.0 0.0 copy-done.11
  52.1 0.0 copy-done.9
  52.1 0.1 copy.26
  52.2 0.6 collective-permute-done
  52.7 0.1 fusion.5.refs_4_
  52.8 35.9 %all-to-all-done.1.refs_0_ = bf16[16,704,128]{2,1,0:T(8,128)(2,1)S(1)} async-done(((bf16[16,704,128]{2,1,0:T(8,128)(2,1)}), bf16[16,704,128]{2,1,0:T(8,128)(2,1)S(1)}, u32[]{:S(2)}, u32[]{:S(2)}) %all-to-all-start.1) | async-done | bytes 2883616 | tf_op jit(solution)/shard_map/all_to_all | solution.py:160
  88.7 0.0 copy-done.6
  88.7 0.0 copy-start.3
  88.7 1.2 copy-done.3
  89.9 0.0 copy-start.4
  89.9 1.2 copy-done.4
  91.1 0.0 copy-start.5
  91.1 1.2 copy-done.5
  92.3 3.9 %shard_map.132 = bf16[16,960,128]{2,1,0:T(8,128)(2,1)S(1)} custom-call(bf16[16,704,128]{2,1,0:T(8,128)(2,1)S(1)} %all-to-all-done.1.refs_0_, bf16[2048,256]{1,0:T(8,128)(2,1)S(1)} %bitcast.16, bf16[2048,256]{1,0:T(8,128)(2,1)S(1)} %bitcast.17, bf16[256,2048]{1,0:T(8,128)(2,1)S(1)} %bitcast.18, bf16[256,64]{1,0:T(8,128)(2,1)S(1)} %fusion.5.refs_4_, ...), custom_call_target="tpu_custom_call" | custom-call | flops 4294967296 | bytes 1048576 | tf_op jit(solution)/shard_map/pallas_call | solution.py:23
  96.2 50.6 %all_to_all.21.parts = bf16[16,960,128]{2,1,0:T(8,128)(2,1)S(1)} all-to-all(bf16[16,960,128]{2,1,0:T(8,128)(2,1)S(1)} %shard_map.132), channel_id=1, replica_groups=mesh['ep'=32,'tp_0'=4,'tp_1'=4] {'tp_0','tp_1'}, dimensions={0} | all-to-all | bytes 7864320 | tf_op jit(solution)/shard_map/all_to_all | solution.py:185
  146.8 0.0 copy-start.10
  146.8 0.8 shard_map.133
  147.6 0.7 reshape.24
  148.3 10.2 %all-to-all-start.3 = ((bf16[32,22,128]{2,1,0:T(8,128)(2,1)}), bf16[32,22,128]{2,1,0:T(8,128)(2,1)S(1)}, u32[]{:S(2)}, u32[]{:S(2)}) async-start(bf16[32,22,128]{2,1,0:T(8,128)(2,1)} %reshape.24), calls=%async_computation.3 | async-start | bytes 393216 | tf_op jit(solution)/shard_map/all_to_all | solution.py:196
  158.5 0.1 copy.27
  158.6 0.0 copy-done.10
  158.6 0.1 copy.28.scores
  158.8 18.5 %all-to-all-done.3 = bf16[32,22,128]{2,1,0:T(8,128)(2,1)S(1)} async-done(((bf16[32,22,128]{2,1,0:T(8,128)(2,1)}), bf16[32,22,128]{2,1,0:T(8,128)(2,1)S(1)}, u32[]{:S(2)}, u32[]{:S(2)}) %all-to-all-start.3) | async-done | bytes 180256 | tf_op jit(solution)/shard_map/all_to_all | solution.py:196
  177.2 0.1 reshape.25.rows
  177.3 1.1 shard_map.134
  (3 shorter events, 0.0 us)
Async XLA Ops:
  0.6 1.2 copy-start
  1.9 0.7 copy-start.1
  2.6 0.7 copy-start.2
  39.3 9.1 %copy-start.7 = (bf16[256,64]{0,1:T(8,128)(2,1)S(1)}, bf16[256,64]{0,1:T(8,128)(2,1)}, u32[]{:S(2)}) copy-start(bf16[256,64]{0,1:T(8,128)(2,1)} %param.13) | copy-start | bytes 98308
  39.3 9.2 %copy-start.8 = (bf16[256,64]{0,1:T(8,128)(2,1)S(1)}, bf16[256,64]{0,1:T(8,128)(2,1)}, u32[]{:S(2)}) copy-start(bf16[256,64]{0,1:T(8,128)(2,1)} %param.14) | copy-start | bytes 98308
  39.3 12.7 %copy-start.11 = (f32[3,64]{1,0:T(4,128)S(1)}, f32[3,64]{1,0:T(4,128)}, u32[]{:S(2)}) copy-start(f32[3,64]{1,0:T(4,128)} %param.15) | copy-start | bytes 2308
  39.3 12.7 %copy-start.9 = (bf16[256,64]{0,1:T(8,128)(2,1)S(1)}, bf16[256,64]{0,1:T(8,128)(2,1)}, u32[]{:S(2)}) copy-start(bf16[256,64]{0,1:T(8,128)(2,1)} %param.12) | copy-start | bytes 98308
  41.5 47.2 %copy-start.6 = (bf16[64,2048]{1,0:T(8,128)(2,1)S(1)}, bf16[64,2048]{1,0:T(8,128)(2,1)}, u32[]{:S(2)}) copy-start(bf16[64,2048]{1,0:T(8,128)(2,1)} %refs_5_.1) | copy-start | bytes 786436
  41.5 47.2 %all-to-all-start.1 = ((bf16[16,704,128]{2,1,0:T(8,128)(2,1)}), bf16[16,704,128]{2,1,0:T(8,128)(2,1)S(1)}, u32[]{:S(2)}, u32[]{:S(2)}) async-start(bf16[16,704,128]{2,1,0:T(8,128)(2,1)} %broadcast_in_dim.8), calls=%async_computation.1 | async-start | bytes 5767168 | tf_op jit(solution)/shard_map/all_to_all | solution.py:160
  48.7 4.1 %collective-permute-start = (f32[2,64]{1,0:T(2,128)S(1)}, f32[2,64]{1,0:T(2,128)S(1)}, u32[]{:S(2)}, u32[]{:S(2)}) collective-permute-start(f32[2,64]{1,0:T(2,128)S(1)} %slice.24), channel_id=1, source_target_pairs={{0,16},{16,32},{32,48},{48,64},{64,80},{80,96},{96,112},{112,128},... | collective-permute-start | bytes 1544 | tf_op jit(solution)/shard_map/ppermute | solution.py:19
  88.7 1.2 copy-start.3
  89.9 1.2 copy-start.4
  91.1 1.2 copy-start.5
  146.8 11.8 %copy-start.10 = (f32[256,2]{0,1:T(2,128)S(1)}, f32[256,2]{0,1:T(2,128)}, u32[]{:S(2)}) copy-start(f32[256,2]{0,1:T(2,128)} %param.20) | copy-start | bytes 6148
  148.3 29.0 %all-to-all-start.3 = ((bf16[32,22,128]{2,1,0:T(8,128)(2,1)}), bf16[32,22,128]{2,1,0:T(8,128)(2,1)S(1)}, u32[]{:S(2)}, u32[]{:S(2)}) async-start(bf16[32,22,128]{2,1,0:T(8,128)(2,1)} %reshape.24), calls=%async_computation.3 | async-start | bytes 393216 | tf_op jit(solution)/shard_map/all_to_all | solution.py:196

commit v2 on v1

v2 whole, which is shorter than its diff:
```python
import jax
import jax.numpy as jnp
from jax import lax
from jax.experimental import pallas as pl
from jax.experimental.pallas import tpu as pltpu
from jax.sharding import Mesh
from jax.sharding import PartitionSpec as P


TP = ("tp_0", "tp_1")
F32 = jnp.float32
BF16 = jnp.bfloat16
VMEM = pl.BlockSpec(memory_space=pltpu.VMEM)
SMEM = pl.BlockSpec(memory_space=pltpu.SMEM)
HBM = pl.BlockSpec(memory_space=pltpu.HBM)


def shifted(block, axis, distance):
    devices = range(lax.axis_size(axis))
    route = [(i - distance, i) for i in devices if i - distance in devices]
    return lax.ppermute(block, axis, route)


def call(body, out, limit, flops, *operands, specs=None, scratch=()):
    return pl.pallas_call(
        body,
        out_shape=out,
        in_specs=specs or [VMEM] * len(operands),
        out_specs=jax.tree.map(lambda _: VMEM, out),
        scratch_shapes=scratch,
        compiler_params=pltpu.CompilerParams(vmem_limit_bytes=limit),
        cost_estimate=pl.CostEstimate(
            flops=flops, bytes_accessed=1 << 20, transcendentals=0
        ),
    )(*operands)


def dispatch_body(
    stride, experts, place, rows_far, gain_far, ids_far, sent, slots, rows, gain, ids, done
):
    copies = [
        pltpu.make_async_copy(far, near, done.at[n])
        for n, (far, near) in enumerate(((ids_far, ids), (gain_far, gain), (rows_far, rows)))
    ]
    for copy in copies:
        copy.start()
    for copy in copies:
        copy.wait()
    tokens, width = rows.shape
    capacity, columns = sent.shape[1:]
    wide = rows[...].astype(F32)
    scaling = lax.rsqrt(jnp.sum(wide * wide, axis=1, keepdims=True) / width + 1e-06)
    start = pl.multiple_of(place[0] * columns, columns)
    own = rows[:, pl.ds(start, columns)].astype(F32)
    normed = (own * scaling * gain[:, pl.ds(start, columns)]).astype(BF16)
    chosen = ids[...]
    expert = lax.broadcasted_iota(jnp.int32, (experts, tokens), 0)
    hits = [expert == chosen[k : k + 1, :] for k in range(chosen.shape[0])]
    marks = [jnp.where(h, 1.0, 0.0).astype(F32) for h in hits]
    total = marks[0]
    for m in marks[1:]:
        total = total + m
    earlier = lax.broadcasted_iota(jnp.int32, (tokens, tokens), 0)
    later = lax.broadcasted_iota(jnp.int32, (tokens, tokens), 1)
    before = jnp.dot(
        total.astype(BF16),
        jnp.where(earlier < later, 1.0, 0.0).astype(BF16),
        preferred_element_type=F32,
    )
    base = (expert * stride).astype(F32)
    where = [
        jnp.sum(m * (before + base), axis=0, keepdims=True).astype(jnp.int32) for m in marks
    ]
    slots[...] = jnp.concatenate(where, axis=0)
    slot = lax.broadcasted_iota(jnp.int32, (experts * stride, tokens), 0)
    table = slot == where[0]
    for w in where[1:]:
        table = table | (slot == w)
    placed = jnp.dot(
        jnp.where(table, 1.0, 0.0).astype(BF16), normed, preferred_element_type=F32
    ).reshape(experts, stride, columns)
    sent[...] = placed[:, :capacity, :].astype(BF16)


def expert_body(step, tokens, gate_w, up_w, down_w, out):
    blocks, rows, columns = tokens.shape

    def tile(number, carry):
        at = pl.ds(pl.multiple_of(number * step, step), step)
        left = jnp.concatenate([tokens[b, at, :] for b in range(blocks)], axis=1)
        gate = jnp.dot(left, gate_w[0], preferred_element_type=F32)
        up = jnp.dot(left, up_w[0], preferred_element_type=F32)
        hidden = (gate / (1.0 + jnp.exp(-gate)) * up).astype(BF16)
        part = jnp.dot(hidden, down_w[0], preferred_element_type=F32).astype(BF16)
        for b in range(blocks):
            out[b, at, :] = part[:, b * columns : (b + 1) * columns]
        return carry

    lax.fori_loop(0, rows // step, tile, 0)


def sum_body(parts, out, total):
    experts, capacity, _ = out.shape
    value = parts[0].astype(F32)
    for b in range(1, parts.shape[0]):
        value = value + parts[b].astype(F32)
    total[...] = value
    for e in range(experts):
        out[e] = total[e * capacity : (e + 1) * capacity, :].astype(BF16)


def mixer_body(place, gate_out, gate_in, values, taps, halo, proj, *outs):
    count = len(outs)
    groups, _, columns = outs[0].shape
    product = gate_in[...].astype(F32).T * values[...].astype(F32).T
    row = lax.broadcasted_iota(jnp.int32, product.shape, 0)
    last = halo[1:2, :]
    back_one = jnp.where(row == 0, last, pltpu.roll(product, 1, 0))
    back_two = jnp.where(
        row == 0, halo[0:1, :], jnp.where(row == 1, last, pltpu.roll(product, 2, 0))
    )
    convolved = taps[0:1, :] * back_two + taps[1:2, :] * back_one + taps[2:3, :] * product
    branch = (gate_out[...].astype(F32).T * convolved).astype(BF16)
    for away, out in enumerate(outs):
        target = lax.rem(place[0] + away, count)
        for g in range(groups):
            start = pl.multiple_of((g * count + target) * columns, columns)
            out[g] = jnp.dot(
                branch, proj[:, pl.ds(start, columns)], preferred_element_type=F32
            ).astype(BF16)


def regroup_body(place, *refs):
    half = len(refs) // 2
    parts, outs = refs[:half], refs[half:]
    for away, out in enumerate(outs):
        target = lax.rem(place[0] + away, half)
        total = parts[0][target].astype(F32)
        for part in parts[1:]:
            total = total + part[target].astype(F32)
        out[...] = total.astype(BF16)


def final_body(*refs):
    total = refs[0][...].astype(F32)
    for part in refs[1:-1]:
        total = total + part[...].astype(F32)
    refs[-1][...] = total.astype(BF16)


def turned(block, axis, distance):
    count = lax.axis_size(axis)
    return lax.ppermute(block, axis, [(i, (i + distance) % count) for i in range(count)])


def combine_body(rows, slots, scores, out, padded):
    tokens = out.shape[0]
    experts, capacity, columns = rows.shape
    stride = padded.shape[1]
    slot = lax.broadcasted_iota(jnp.int32, (tokens, experts * stride), 1)
    padded[...] = jnp.zeros_like(padded)
    padded[:, :capacity, :] = rows[...].astype(F32)
    held = padded[...].reshape(experts * stride, columns).astype(BF16)
    score = scores[...]
    whole = jnp.sum(score, axis=1, keepdims=True)
    total = None
    for k in range(score.shape[1]):
        pick = jnp.where(slot == slots[:, k : k + 1], 1.0, 0.0).astype(BF16)
        term = jnp.dot(pick, held, preferred_element_type=F32)
        term = term * (score[:, k : k + 1] / whole)
        total = term if total is None else total + term
    out[...] = total.astype(BF16)


def shards(
    gate_out,
    gate_in,
    conv_values,
    conv_taps,
    mixer_proj,
    expert_in,
    norm_gain,
    route_ids,
    route_scores,
    gate_proj,
    up_proj,
    down_proj,
):
    tokens, choices = route_ids.shape
    width = expert_in.shape[1]
    ep_count = lax.axis_size("ep")
    tp_count = lax.axis_size(TP)
    local_experts = gate_proj.shape[0]
    experts = ep_count * local_experts
    capacity = max(2, (4 * tokens * choices + 3 * experts - 1) // (3 * experts))
    slot_count = experts * capacity
    stride = (capacity + 7) // 8 * 8
    columns = width // tp_count
    place = lax.axis_index(TP).astype(jnp.int32).reshape(1)
    place_0 = lax.axis_index(TP[0]).astype(jnp.int32).reshape(1)
    place_1 = lax.axis_index(TP[1]).astype(jnp.int32).reshape(1)
    groups = lax.axis_size(TP[0])
    turns = lax.axis_size(TP[1])
    seq_len = gate_in.shape[0]
    tail = seq_len - (conv_taps.shape[0] - 1)

    halo = shifted(gate_in[tail:].astype(F32) * conv_values[tail:].astype(F32), "ep", 1)

    sent, slots = call(
        lambda *refs: dispatch_body(stride, experts, *refs),
        (
            jax.ShapeDtypeStruct((experts, capacity, columns), BF16),
            jax.ShapeDtypeStruct((choices, tokens), jnp.int32),
        ),
        56 << 20,
        1 << 28,
        place,
        expert_in,
        norm_gain.reshape(1, width),
        route_ids.T,
        specs=[SMEM, HBM, HBM, HBM],
        scratch=[
            pltpu.VMEM((tokens, width), BF16),
            pltpu.VMEM((1, width), F32),
            pltpu.VMEM((choices, tokens), jnp.int32),
            pltpu.SemaphoreType.DMA((3,)),
        ],
    )
    arrived = lax.all_to_all(sent, "ep", 0, 0, tiled=True)

    first = call(
        mixer_body,
        (jax.ShapeDtypeStruct((groups, seq_len, columns), BF16),) * turns,
        56 << 20,
        1 << 26,
        place_1,
        gate_out.T,
        gate_in.T,
        conv_values.T,
        conv_taps,
        halo,
        mixer_proj,
        specs=[SMEM] + [VMEM] * 6,
    )
    first = [first[0]] + [turned(first[d], TP[1], d) for d in range(1, turns)]

    own_block = arrived.reshape(1, slot_count, columns)
    copies = jnp.broadcast_to(own_block, (tp_count, slot_count, columns))
    gathered = lax.all_to_all(copies, TP, 0, 0, tiled=True)
    parts = call(
        lambda *refs: expert_body(slot_count // 4, *refs),
        jax.ShapeDtypeStruct((tp_count, slot_count, columns), BF16),
        24 << 20,
        1 << 32,
        gathered,
        gate_proj,
        up_proj,
        down_proj,
    )
    shared = lax.all_to_all(parts, TP, 0, 0, tiled=True)
    outputs = call(
        sum_body,
        jax.ShapeDtypeStruct((experts, capacity, columns), BF16),
        16 << 20,
        1 << 24,
        shared,
        scratch=[pltpu.VMEM((slot_count, columns), F32)],
    )
    returned = lax.all_to_all(outputs, "ep", 0, 0, tiled=True)

    second = call(
        regroup_body,
        (jax.ShapeDtypeStruct((seq_len, columns), BF16),) * groups,
        12 << 20,
        1 << 22,
        place_0,
        *first,
        specs=[SMEM] + [VMEM] * turns,
    )
    second = [second[0]] + [turned(second[d], TP[0], d) for d in range(1, groups)]
    mixed = call(
        final_body, jax.ShapeDtypeStruct((seq_len, columns), BF16), 8 << 20, 1 << 20, *second
    )
    expert_mix = call(
        combine_body,
        jax.ShapeDtypeStruct((tokens, columns), BF16),
        16 << 20,
        1 << 27,
        returned,
        slots.T,
        route_scores,
        scratch=[pltpu.VMEM((experts, stride, columns), F32)],
    )
    return (mixed, expert_mix)


def solution(mesh):
    torus = Mesh(mesh.devices.reshape(mesh.shape["ep"], 4, 4), ("ep", "tp_0", "tp_1"))
    in_specs = (
        P("ep", TP),
        P("ep", TP),
        P("ep", TP),
        P(None, TP),
        P(TP, None),
        P("ep", None),
        P(),
        P("ep", None),
        P("ep", None),
        P("ep", None, TP),
        P("ep", None, TP),
        P("ep", TP, None),
    )
    out_specs = (P("ep", TP), P("ep", TP))

    return jax.shard_map(
        shards, mesh=torus, in_specs=in_specs, out_specs=out_specs, check_vma=False
    )
```

time: 179 us -> 176 us (0.983)
  the two profiles are of different devices: /device:TPU:1 before, /device:TPU:72 now
where the time goes in v2:
time: 176 us; the launch traced here: 175 us
  blocking collectives  114 us (65%)
  starting transfers between devices  27.2 us (15%)
  waiting for transfers between devices  19 us (11%)
  Pallas kernels  11.6 us (7%)
  local copies, waits for them, and re-layouts  2.75 us (2%)
    all_to_all x1, blocking collectives, shards(): gathered = lax.all_to_all(copies, TP, 0, 0, tiled=True)  42.6 us
    all_to_all x1, blocking collectives, shards(): shared = lax.all_to_all(parts, TP, 0, 0, tiled=True)  39.5 us
    all_to_all x1, blocking collectives, shards(): arrived = lax.all_to_all(sent, 'ep', 0, 0, tiled=True)  31.8 us
    ppermute x6, starting transfers between devices, turned(): lax.ppermute(block, axis, [(i, (i + distance) % count) for i in range(cou...  19.9 us
    ppermute x6, waiting for transfers between devices, turned(): lax.ppermute(block, axis, [(i, (i + distance) % count) for i in range(cou...  13.8 us
    pallas_call x7, Pallas kernels, call(): pl.pallas_call(body, out_shape=out, in_specs=specs or [VMEM] * len(operan...  11.6 us
    all_to_all x1, starting transfers between devices, shards(): returned = lax.all_to_all(outputs, 'ep', 0, 0, tiled=True)  5.31 us
    ppermute x1, waiting for transfers between devices, shifted(): return lax.ppermute(block, axis, route)  5.26 us
  transfers between devices with their start and end apart: 8, of which 5 were waited for; matrix products, arithmetic and copies ran while one was open for 0% of the time, Pallas kernels for 2%

profile of v2, /device:TPU:72, one launch (start us, length us, event | category | flops | bytes accessed | tf_op | source)
XLA Modules:
  0.0 175.4 jit_solution(11231396991838038918)
XLA Ops:
  0.6 2.6 %shard_map.134 = (bf16[32,22,128]{2,1,0:T(8,128)(2,1)}, s32[2,256]{1,0:T(2,128)}) custom-call(s32[1]{0:T(128)} %bitcast.5.refs_0_, bf16[256,2048]{1,0:T(8,128)(2,1)} %refs_1_.2, f32[1,2048]{1,0:T(1,128)} %bitcast.13, s32[2,256]{1,0:T(2,128)} %bitcast.14), custom_call_target="tpu_custom_call" | custom-call | flops 268435456 | bytes 1048576 | tf_op jit(solution)/shard_map/pallas_call | solution.py:25
  3.2 31.8 %all_to_all.20 = bf16[32,22,128]{2,1,0:T(8,128)(2,1)S(1)} all-to-all(bf16[32,22,128]{2,1,0:T(8,128)(2,1)} %get-tuple-element.20), channel_id=1, replica_groups=mesh['ep'=32,'tp_0'=4,'tp_1'=4] {'ep'}, dimensions={0} | all-to-all | bytes 360448 | tf_op jit(solution)/shard_map/all_to_all | solution.py:229
  35.1 0.1 broadcast_in_dim.7
  35.1 0.5 broadcast_in_dim.8
  35.7 0.0 copy-start.1
  35.7 0.0 copy-start.2
  35.7 0.0 copy-start.3
  35.7 42.6 %all_to_all.21.refs_0_ = bf16[16,704,128]{2,1,0:T(8,128)(2,1)S(1)} all-to-all(bf16[16,704,128]{2,1,0:T(8,128)(2,1)S(1)} %broadcast_in_dim.8), channel_id=1, replica_groups=mesh['ep'=32,'tp_0'=4,'tp_1'=4] {'tp_0','tp_1'}, dimensions={0} | all-to-all | bytes 5767168 | tf_op jit(solution)/shard_map/all_to_all | solution.py:249
  78.3 0.0 copy-done.1
  78.3 0.0 copy-done.2
  78.3 0.0 copy-done.3
  78.4 3.5 %shard_map.135 = bf16[16,704,128]{2,1,0:T(8,128)(2,1)S(1)} custom-call(bf16[16,704,128]{2,1,0:T(8,128)(2,1)S(1)} %all_to_all.21.refs_0_, bf16[1,2048,256]{2,1,0:T(8,128)(2,1)S(1)} %copy-done.1, bf16[1,2048,256]{2,1,0:T(8,128)(2,1)S(1)} %copy-done.2, bf16[1,256,2048]{2,1,0:T(8,128)(2,1)S(1)} %copy-done.3), custom_call_target="tpu_custom_call" | custom-call | flops 4294967296 | bytes 1048576 | tf_op jit(solution)/shard_map/pallas_call | solution.py:25
  81.9 39.5 %all_to_all.22.parts = bf16[16,704,128]{2,1,0:T(8,128)(2,1)S(1)} all-to-all(bf16[16,704,128]{2,1,0:T(8,128)(2,1)S(1)} %shard_map.135), channel_id=1, replica_groups=mesh['ep'=32,'tp_0'=4,'tp_1'=4] {'tp_0','tp_1'}, dimensions={0} | all-to-all | bytes 5767168 | tf_op jit(solution)/shard_map/all_to_all | solution.py:260
  121.4 0.0 copy-start.4
  121.4 0.0 copy-start.5
  121.4 1.3 shard_map.136
  122.6 5.3 %all-to-all-start.3 = ((bf16[32,22,128]{2,1,0:T(8,128)(2,1)}), bf16[32,22,128]{2,1,0:T(8,128)(2,1)S(1)}, u32[]{:S(2)}, u32[]{:S(2)}) async-start(bf16[32,22,128]{2,1,0:T(8,128)(2,1)} %shard_map.136), calls=%async_computation.3 | async-start | bytes 393216 | tf_op jit(solution)/shard_map/all_to_all | solution.py:269
  127.9 0.0 copy-done.4
  128.0 0.1 slice.6
  128.0 0.1 copy.22
  128.1 0.0 copy-done.5
  128.1 0.1 slice.7
  128.2 0.1 copy.23
  128.3 2.0 %collective-permute-start = (f32[2,64]{1,0:T(2,128)S(1)}, f32[2,64]{1,0:T(2,128)S(1)}, u32[]{:S(2)}, u32[]{:S(2)}) collective-permute-start(f32[2,64]{1,0:T(2,128)S(1)} %convert_multiply_fusion), channel_id=1, source_target_pairs={{0,16},{16,32},{32,48},{48,64},{64,80},{80,96},{96,112},{112,128},... | collective-permute-start | bytes 1544 | tf_op jit(solution)/shard_map/ppermute | solution.py:21
  130.3 5.3 %collective-permute-done.halo = f32[2,64]{1,0:T(2,128)S(1)} collective-permute-done((f32[2,64]{1,0:T(2,128)S(1)}, f32[2,64]{1,0:T(2,128)S(1)}, u32[]{:S(2)}, u32[]{:S(2)}) %collective-permute-start) | collective-permute-done | bytes 544 | tf_op jit(solution)/shard_map/ppermute | solution.py:21
  135.6 0.6 copy-done.8
  136.2 2.4 %shard_map.131 = (bf16[4,256,128]{2,1,0:T(8,128)(2,1)}, bf16[4,256,128]{2,1,0:T(8,128)(2,1)}, bf16[4,256,128]{2,1,0:T(8,128)(2,1)}, bf16[4,256,128]{2,1,0:T(8,128)(2,1)}) custom-call(s32[1]{0:T(128)} %bitcast.1.place, bf16[64,256]{1,0:T(8,128)(2,1)} %bitcast.12, bf16[64,256]{1,0:T(8,128)(2,1)} %bitcast.10, bf16[64,256]{1,0:T(8,128)(2,1)} %bitcast.11, ...), custom_call_target="tpu_custom_call" | custom-call | flops 67108864 | bytes 1048576 | tf_op jit(solution)/shard_map/pallas_call | solution.py:25
  138.5 2.0 %collective-permute-start.1 = (bf16[4,256,128]{2,1,0:T(8,128)(2,1)}, bf16[4,256,128]{2,1,0:T(8,128)(2,1)S(1)}, u32[]{:S(2)}, u32[]{:S(2)}) collective-permute-start(bf16[4,256,128]{2,1,0:T(8,128)(2,1)} %get-tuple-element.13), channel_id=1, source_target_pairs={{0,1},{1,2},{2,3},{3,0},{4,5},{5,6},{6,7},{7,4},{8,9},{9,10},{10,1... | collective-permute-start | bytes 786440 | tf_op jit(solution)/shard_map/ppermute | solution.py:153
  140.5 4.5 %collective-permute-start.2 = (bf16[4,256,128]{2,1,0:T(8,128)(2,1)}, bf16[4,256,128]{2,1,0:T(8,128)(2,1)S(1)}, u32[]{:S(2)}, u32[]{:S(2)}) collective-permute-start(bf16[4,256,128]{2,1,0:T(8,128)(2,1)} %get-tuple-element.14), channel_id=1, source_target_pairs={{0,2},{1,3},{2,0},{3,1},{4,6},{5,7},{6,4},{7,5},{8,10},{9,11},{10,... | collective-permute-start | bytes 786440 | tf_op jit(solution)/shard_map/ppermute | solution.py:153
  145.0 3.4 %collective-permute-start.3 = (bf16[4,256,128]{2,1,0:T(8,128)(2,1)}, bf16[4,256,128]{2,1,0:T(8,128)(2,1)S(1)}, u32[]{:S(2)}, u32[]{:S(2)}) collective-permute-start(bf16[4,256,128]{2,1,0:T(8,128)(2,1)} %get-tuple-element.15), channel_id=1, source_target_pairs={{0,3},{1,0},{2,1},{3,2},{4,7},{5,4},{6,5},{7,6},{8,11},{9,8},{10,9... | collective-permute-start | bytes 786440 | tf_op jit(solution)/shard_map/ppermute | solution.py:153
  148.4 7.5 %collective-permute-done.1.refs_1_ = bf16[4,256,128]{2,1,0:T(8,128)(2,1)S(1)} collective-permute-done((bf16[4,256,128]{2,1,0:T(8,128)(2,1)}, bf16[4,256,128]{2,1,0:T(8,128)(2,1)S(1)}, u32[]{:S(2)}, u32[]{:S(2)}) %collective-permute-start.1) | collective-permute-done | bytes 262176 | tf_op jit(solution)/shard_map/ppermute | solution.py:153
  155.9 0.0 collective-permute-done.2.refs_2_
  155.9 2.5 %collective-permute-done.3.refs_3_ = bf16[4,256,128]{2,1,0:T(8,128)(2,1)S(1)} collective-permute-done((bf16[4,256,128]{2,1,0:T(8,128)(2,1)}, bf16[4,256,128]{2,1,0:T(8,128)(2,1)S(1)}, u32[]{:S(2)}, u32[]{:S(2)}) %collective-permute-start.3) | collective-permute-done | bytes 262176 | tf_op jit(solution)/shard_map/ppermute | solution.py:153
  158.5 0.9 copy-done
  159.4 0.1 shard_map.132
  159.6 2.7 %collective-permute-start.4 = (bf16[256,128]{1,0:T(8,128)(2,1)S(1)}, bf16[256,128]{1,0:T(8,128)(2,1)S(1)}, u32[]{:S(2)}, u32[]{:S(2)}) collective-permute-start(bf16[256,128]{1,0:T(8,128)(2,1)S(1)} %get-tuple-element.17), channel_id=1, source_target_pairs={{0,4},{4,8},{8,12},{12,0},{1,5},{5,9},{9,13},{13,1},{2,6},{6,10},{... | collective-permute-start | bytes 196616 | tf_op jit(solution)/shard_map/ppermute | solution.py:153
  162.2 5.2 %collective-permute-start.5 = (bf16[256,128]{1,0:T(8,128)(2,1)S(1)}, bf16[256,128]{1,0:T(8,128)(2,1)S(1)}, u32[]{:S(2)}, u32[]{:S(2)}) collective-permute-start(bf16[256,128]{1,0:T(8,128)(2,1)S(1)} %get-tuple-element.18), channel_id=1, source_target_pairs={{0,8},{4,12},{8,0},{12,4},{1,9},{5,13},{9,1},{13,5},{2,10},{6,14},... | collective-permute-start | bytes 196616 | tf_op jit(solution)/shard_map/ppermute | solution.py:153
  167.5 2.1 %collective-permute-start.6 = (bf16[256,128]{1,0:T(8,128)(2,1)S(1)}, bf16[256,128]{1,0:T(8,128)(2,1)S(1)}, u32[]{:S(2)}, u32[]{:S(2)}) collective-permute-start(bf16[256,128]{1,0:T(8,128)(2,1)S(1)} %get-tuple-element.19), channel_id=1, source_target_pairs={{0,12},{4,0},{8,4},{12,8},{1,13},{5,1},{9,5},{13,9},{2,14},{6,2},{... | collective-permute-start | bytes 196616 | tf_op jit(solution)/shard_map/ppermute | solution.py:153
  169.6 0.0 copy-done.7
  169.6 0.1 copy.20
  169.8 0.0 copy-done.6
  169.8 0.1 copy.21.scores
  169.9 0.0 collective-permute-done.4.refs_1_
  169.9 0.2 collective-permute-done.5.refs_2_
  170.1 3.5 %collective-permute-done.6.refs_3_ = bf16[256,128]{1,0:T(8,128)(2,1)S(1)} collective-permute-done((bf16[256,128]{1,0:T(8,128)(2,1)S(1)}, bf16[256,128]{1,0:T(8,128)(2,1)S(1)}, u32[]{:S(2)}, u32[]{:S(2)}) %collective-permute-start.6) | collective-permute-done | bytes 65568 | tf_op jit(solution)/shard_map/ppermute | solution.py:153
  173.6 0.7 shard_map.133
  174.3 0.0 all-to-all-done.3.rows
  174.3 1.1 shard_map.137
  (5 shorter events, 0.0 us)
Async XLA Ops:
  35.7 42.7 %copy-start.1 = (bf16[1,2048,256]{2,1,0:T(8,128)(2,1)S(1)}, bf16[1,2048,256]{2,1,0:T(8,128)(2,1)}, u32[]{:S(2)}) copy-start(bf16[1,2048,256]{2,1,0:T(8,128)(2,1)} %refs_1_.3) | copy-start | bytes 3145732
  35.7 42.7 %copy-start.2 = (bf16[1,2048,256]{2,1,0:T(8,128)(2,1)S(1)}, bf16[1,2048,256]{2,1,0:T(8,128)(2,1)}, u32[]{:S(2)}) copy-start(bf16[1,2048,256]{2,1,0:T(8,128)(2,1)} %refs_2_.1) | copy-start | bytes 3145732
  35.7 42.7 %copy-start.3 = (bf16[1,256,2048]{2,1,0:T(8,128)(2,1)S(1)}, bf16[1,256,2048]{2,1,0:T(8,128)(2,1)}, u32[]{:S(2)}) copy-start(bf16[1,256,2048]{2,1,0:T(8,128)(2,1)} %refs_3_.1) | copy-start | bytes 3145732
  121.4 6.6 %copy-start.4 = (bf16[256,64]{0,1:T(8,128)(2,1)S(1)}, bf16[256,64]{0,1:T(8,128)(2,1)}, u32[]{:S(2)}) copy-start(bf16[256,64]{0,1:T(8,128)(2,1)} %param.13) | copy-start | bytes 98308
  121.4 6.8 %copy-start.5 = (bf16[256,64]{0,1:T(8,128)(2,1)S(1)}, bf16[256,64]{0,1:T(8,128)(2,1)}, u32[]{:S(2)}) copy-start(bf16[256,64]{0,1:T(8,128)(2,1)} %param.14) | copy-start | bytes 98308
  121.4 48.3 %copy-start.7 = (s32[2,256]{1,0:T(2,128)S(1)}, s32[2,256]{1,0:T(2,128)}, u32[]{:S(2)}) copy-start(s32[2,256]{1,0:T(2,128)} %get-tuple-element.21) | copy-start | bytes 6148
  121.4 48.4 %copy-start.6 = (f32[256,2]{0,1:T(2,128)S(1)}, f32[256,2]{0,1:T(2,128)}, u32[]{:S(2)}) copy-start(f32[256,2]{0,1:T(2,128)} %param.20) | copy-start | bytes 6148
  122.6 51.7 %all-to-all-start.3 = ((bf16[32,22,128]{2,1,0:T(8,128)(2,1)}), bf16[32,22,128]{2,1,0:T(8,128)(2,1)S(1)}, u32[]{:S(2)}, u32[]{:S(2)}) async-start(bf16[32,22,128]{2,1,0:T(8,128)(2,1)} %shard_map.136), calls=%async_computation.3 | async-start | bytes 393216 | tf_op jit(solution)/shard_map/all_to_all | solution.py:269
  128.3 7.3 %collective-permute-start = (f32[2,64]{1,0:T(2,128)S(1)}, f32[2,64]{1,0:T(2,128)S(1)}, u32[]{:S(2)}, u32[]{:S(2)}) collective-permute-start(f32[2,64]{1,0:T(2,128)S(1)} %convert_multiply_fusion), channel_id=1, source_target_pairs={{0,16},{16,32},{32,48},{48,64},{64,80},{80,96},{96,112},{112,128},... | collective-permute-start | bytes 1544 | tf_op jit(solution)/shard_map/ppermute | solution.py:21
  135.6 0.6 copy-start.8
  138.5 17.4 %collective-permute-start.1 = (bf16[4,256,128]{2,1,0:T(8,128)(2,1)}, bf16[4,256,128]{2,1,0:T(8,128)(2,1)S(1)}, u32[]{:S(2)}, u32[]{:S(2)}) collective-permute-start(bf16[4,256,128]{2,1,0:T(8,128)(2,1)} %get-tuple-element.13), channel_id=1, source_target_pairs={{0,1},{1,2},{2,3},{3,0},{4,5},{5,6},{6,7},{7,4},{8,9},{9,10},{10,1... | collective-permute-start | bytes 786440 | tf_op jit(solution)/shard_map/ppermute | solution.py:153
  140.5 15.4 %collective-permute-start.2 = (bf16[4,256,128]{2,1,0:T(8,128)(2,1)}, bf16[4,256,128]{2,1,0:T(8,128)(2,1)S(1)}, u32[]{:S(2)}, u32[]{:S(2)}) collective-permute-start(bf16[4,256,128]{2,1,0:T(8,128)(2,1)} %get-tuple-element.14), channel_id=1, source_target_pairs={{0,2},{1,3},{2,0},{3,1},{4,6},{5,7},{6,4},{7,5},{8,10},{9,11},{10,... | collective-permute-start | bytes 786440 | tf_op jit(solution)/shard_map/ppermute | solution.py:153
  145.0 13.4 %collective-permute-start.3 = (bf16[4,256,128]{2,1,0:T(8,128)(2,1)}, bf16[4,256,128]{2,1,0:T(8,128)(2,1)S(1)}, u32[]{:S(2)}, u32[]{:S(2)}) collective-permute-start(bf16[4,256,128]{2,1,0:T(8,128)(2,1)} %get-tuple-element.15), channel_id=1, source_target_pairs={{0,3},{1,0},{2,1},{3,2},{4,7},{5,4},{6,5},{7,6},{8,11},{9,8},{10,9... | collective-permute-start | bytes 786440 | tf_op jit(solution)/shard_map/ppermute | solution.py:153
  158.5 1.0 copy-start
  159.6 10.4 %collective-permute-start.4 = (bf16[256,128]{1,0:T(8,128)(2,1)S(1)}, bf16[256,128]{1,0:T(8,128)(2,1)S(1)}, u32[]{:S(2)}, u32[]{:S(2)}) collective-permute-start(bf16[256,128]{1,0:T(8,128)(2,1)S(1)} %get-tuple-element.17), channel_id=1, source_target_pairs={{0,4},{4,8},{8,12},{12,0},{1,5},{5,9},{9,13},{13,1},{2,6},{6,10},{... | collective-permute-start | bytes 196616 | tf_op jit(solution)/shard_map/ppermute | solution.py:153
  162.2 7.9 %collective-permute-start.5 = (bf16[256,128]{1,0:T(8,128)(2,1)S(1)}, bf16[256,128]{1,0:T(8,128)(2,1)S(1)}, u32[]{:S(2)}, u32[]{:S(2)}) collective-permute-start(bf16[256,128]{1,0:T(8,128)(2,1)S(1)} %get-tuple-element.18), channel_id=1, source_target_pairs={{0,8},{4,12},{8,0},{12,4},{1,9},{5,13},{9,1},{13,5},{2,10},{6,14},... | collective-permute-start | bytes 196616 | tf_op jit(solution)/shard_map/ppermute | solution.py:153
  167.5 6.2 %collective-permute-start.6 = (bf16[256,128]{1,0:T(8,128)(2,1)S(1)}, bf16[256,128]{1,0:T(8,128)(2,1)S(1)}, u32[]{:S(2)}, u32[]{:S(2)}) collective-permute-start(bf16[256,128]{1,0:T(8,128)(2,1)S(1)} %get-tuple-element.19), channel_id=1, source_target_pairs={{0,12},{4,0},{8,4},{12,8},{1,13},{5,1},{9,5},{13,9},{2,14},{6,2},{... | collective-permute-start | bytes 196616 | tf_op jit(solution)/shard_map/ppermute | solution.py:153

commit v3 on v2

--- a/solution.py
+++ b/solution.py
@@ -21,12 +21,12 @@
     return lax.ppermute(block, axis, route)
 
 
-def call(body, out, limit, flops, *operands, specs=None, scratch=()):
+def call(body, out, limit, flops, *operands, specs=None, scratch=(), place=None):
     return pl.pallas_call(
         body,
         out_shape=out,
         in_specs=specs or [VMEM] * len(operands),
-        out_specs=jax.tree.map(lambda _: VMEM, out),
+        out_specs=jax.tree.map(lambda _: place or VMEM, out),
         scratch_shapes=scratch,
         compiler_params=pltpu.CompilerParams(vmem_limit_bytes=limit),
         cost_estimate=pl.CostEstimate(
@@ -35,16 +35,54 @@
     )(*operands)
 
 
+def far(array):
+    return pltpu.with_memory_space_constraint(array, pltpu.HBM)
+
+
 def dispatch_body(
-    stride, experts, place, rows_far, gain_far, ids_far, sent, slots, rows, gain, ids, done
+    stride,
+    experts,
+    place,
+    rows_far,
+    gain_far,
+    ids_far,
+    inner_far,
+    values_far,
+    outer_far,
+    proj_far,
+    sent,
+    slots,
+    tail,
+    product,
+    outer,
+    proj,
+    rows,
+    gain,
+    ids,
+    inner,
+    values,
+    done,
 ):
+    pairs = (
+        (rows_far, rows),
+        (gain_far, gain),
+        (ids_far, ids),
+        (inner_far, inner),
+        (values_far, values),
+        (outer_far, outer),
+        (proj_far, proj),
+    )
     copies = [
-        pltpu.make_async_copy(far, near, done.at[n])
-        for n, (far, near) in enumerate(((ids_far, ids), (gain_far, gain), (rows_far, rows)))
+        pltpu.make_async_copy(there, here, done.at[n]) for n, (there, here) in enumerate(pairs)
     ]
     for copy in copies:
         copy.start()
-    for copy in copies:
+    for copy in copies[3:5]:
+        copy.wait()
+    mixed = inner[...].astype(F32).T * values[...].astype(F32).T
+    product[...] = mixed
+    tail[...] = mixed[mixed.shape[0] - tail.shape[0] :, :]
+    for copy in copies[:3] + copies[5:]:
         copy.wait()
     tokens, width = rows.shape
     capacity, columns = sent.shape[1:]
@@ -82,21 +120,28 @@
     sent[...] = placed[:, :capacity, :].astype(BF16)
 
 
-def expert_body(step, tokens, gate_w, up_w, down_w, out):
+def expert_body(step, tokens, gate_w, up_w, down_w, out, held, done):
     blocks, rows, columns = tokens.shape
-
-    def tile(number, carry):
-        at = pl.ds(pl.multiple_of(number * step, step), step)
+    slots = held.shape[0]
+    copies = []
+    for number in range(rows // step):
+        at = slice(number * step, (number + 1) * step)
         left = jnp.concatenate([tokens[b, at, :] for b in range(blocks)], axis=1)
         gate = jnp.dot(left, gate_w[0], preferred_element_type=F32)
         up = jnp.dot(left, up_w[0], preferred_element_type=F32)
         hidden = (gate / (1.0 + jnp.exp(-gate)) * up).astype(BF16)
         part = jnp.dot(hidden, down_w[0], preferred_element_type=F32).astype(BF16)
+        slot = number % slots
+        if number >= slots:
+            copies[number - slots].wait()
         for b in range(blocks):
-            out[b, at, :] = part[:, b * columns : (b + 1) * columns]
-        return carry
-
-    lax.fori_loop(0, rows // step, tile, 0)
+            held[slot, b] = part[:, b * columns : (b + 1) * columns]
+        copies.append(
+            pltpu.make_async_copy(held.at[slot], out.at[:, pl.ds(at.start, step), :], done.at[slot])
+        )
+        copies[-1].start()
+    for copy in copies[-slots:]:
+        copy.wait()
 
 
 def sum_body(parts, out, total):
@@ -109,10 +154,10 @@
         out[e] = total[e * capacity : (e + 1) * capacity, :].astype(BF16)
 
 
-def mixer_body(place, gate_out, gate_in, values, taps, halo, proj, *outs):
+def mixer_body(place, outer, product_ref, taps, halo, proj, *outs):
     count = len(outs)
     groups, _, columns = outs[0].shape
-    product = gate_in[...].astype(F32).T * values[...].astype(F32).T
+    product = product_ref[...]
     row = lax.broadcasted_iota(jnp.int32, product.shape, 0)
     last = halo[1:2, :]
     back_one = jnp.where(row == 0, last, pltpu.roll(product, 1, 0))
@@ -120,7 +165,7 @@
         row == 0, halo[0:1, :], jnp.where(row == 1, last, pltpu.roll(product, 2, 0))
     )
     convolved = taps[0:1, :] * back_two + taps[1:2, :] * back_one + taps[2:3, :] * product
-    branch = (gate_out[...].astype(F32).T * convolved).astype(BF16)
+    branch = (outer[...].astype(F32).T * convolved).astype(BF16)
     for away, out in enumerate(outs):
         target = lax.rem(place[0] + away, count)
         for g in range(groups):
@@ -202,45 +247,53 @@
     groups = lax.axis_size(TP[0])
     turns = lax.axis_size(TP[1])
     seq_len = gate_in.shape[0]
-    tail = seq_len - (conv_taps.shape[0] - 1)
-
-    halo = shifted(gate_in[tail:].astype(F32) * conv_values[tail:].astype(F32), "ep", 1)
-
-    sent, slots = call(
+    channels = gate_in.shape[1]
+
+    sent, slots, tail, product, outer, proj = call(
         lambda *refs: dispatch_body(stride, experts, *refs),
         (
             jax.ShapeDtypeStruct((experts, capacity, columns), BF16),
             jax.ShapeDtypeStruct((choices, tokens), jnp.int32),
+            jax.ShapeDtypeStruct((conv_taps.shape[0] - 1, channels), F32),
+            jax.ShapeDtypeStruct((seq_len, channels), F32),
+            jax.ShapeDtypeStruct((channels, seq_len), BF16),
+            jax.ShapeDtypeStruct(mixer_proj.shape, BF16),
         ),
-        56 << 20,
+        16 << 20,
         1 << 28,
         place,
-        expert_in,
-        norm_gain.reshape(1, width),
-        route_ids.T,
-        specs=[SMEM, HBM, HBM, HBM],
+        far(expert_in),
+        far(norm_gain.reshape(1, width)),
+        far(route_ids.T),
+        far(gate_in.T),
+        far(conv_values.T),
+        far(gate_out.T),
+        far(mixer_proj),
+        specs=[SMEM] + [HBM] * 7,
         scratch=[
             pltpu.VMEM((tokens, width), BF16),
             pltpu.VMEM((1, width), F32),
             pltpu.VMEM((choices, tokens), jnp.int32),
-            pltpu.SemaphoreType.DMA((3,)),
+            pltpu.VMEM((channels, seq_len), BF16),
+            pltpu.VMEM((channels, seq_len), BF16),
+            pltpu.SemaphoreType.DMA((7,)),
         ],
     )
+    halo = shifted(tail, "ep", 1)
     arrived = lax.all_to_all(sent, "ep", 0, 0, tiled=True)
 
     first = call(
         mixer_body,
         (jax.ShapeDtypeStruct((groups, seq_len, columns), BF16),) * turns,
-        56 << 20,
+        12 << 20,
         1 << 26,
         place_1,
-        gate_out.T,
-        gate_in.T,
-        conv_values.T,
+        outer,
+        product,
         conv_taps,
         halo,
-        mixer_proj,
-        specs=[SMEM] + [VMEM] * 6,
+        proj,
+        specs=[SMEM] + [VMEM] * 5,
     )
     first = [first[0]] + [turned(first[d], TP[1], d) for d in range(1, turns)]
 
@@ -249,13 +302,18 @@
     gathered = lax.all_to_all(copies, TP, 0, 0, tiled=True)
     parts = call(
         lambda *refs: expert_body(slot_count // 4, *refs),
-        jax.ShapeDtypeStruct((tp_count, slot_count, columns), BF16),
+        pltpu.HBM((tp_count, slot_count, columns), BF16),
         24 << 20,
         1 << 32,
         gathered,
         gate_proj,
         up_proj,
         down_proj,
+        scratch=[
+            pltpu.VMEM((2, tp_count, slot_count // 4, columns), BF16),
+            pltpu.SemaphoreType.DMA((2,)),
+        ],
+        place=HBM,
     )
     shared = lax.all_to_all(parts, TP, 0, 0, tiled=True)
     outputs = call(

time: 176 us -> 174 us (0.989)
  local copies, waits for them, and re-layouts: 2.75 us -> 0.9 us
  transfers between devices with their start and end apart: 8 -> 8, of which waited for: 5 -> 5; matrix products, arithmetic and copies ran while one was open for 0% -> 0% of each run, Pallas kernels for 2% -> 1%
where the time goes in v3:
time: 174 us; the launch traced here: 173 us
  blocking collectives  114 us (66%)
  starting transfers between devices  28.2 us (16%)
  waiting for transfers between devices  18.7 us (11%)
  Pallas kernels  9.92 us (6%)
    all_to_all x1, blocking collectives, shards(): gathered = lax.all_to_all(copies, TP, 0, 0, tiled=True)  42.6 us
    all_to_all x1, blocking collectives, shards(): shared = lax.all_to_all(parts, TP, 0, 0, tiled=True)  40.2 us
    all_to_all x1, blocking collectives, shards(): arrived = lax.all_to_all(sent, 'ep', 0, 0, tiled=True)  31.6 us
    ppermute x6, starting transfers between devices, turned(): lax.ppermute(block, axis, [(i, (i + distance) % count) for i in range(cou...  20.9 us
    ppermute x6, waiting for transfers between devices, turned(): lax.ppermute(block, axis, [(i, (i + distance) % count) for i in range(cou...  13.1 us
    pallas_call x7, Pallas kernels, call(): pl.pallas_call(body, out_shape=out, in_specs=specs or [VMEM] * len(operan...  9.92 us
    ppermute x1, waiting for transfers between devices, shifted(): return lax.ppermute(block, axis, route)  5.62 us
    all_to_all x1, starting transfers between devices, shards(): returned = lax.all_to_all(outputs, 'ep', 0, 0, tiled=True)  5.35 us
  transfers between devices with their start and end apart: 8, of which 5 were waited for; matrix products, arithmetic and copies ran while one was open for 0% of the time, Pallas kernels for 1%

profile of v3, /device:TPU:72, one launch (start us, length us, event | category | flops | bytes accessed | tf_op | source)
XLA Modules:
  0.0 173.1 jit_solution(5847617310804695099)
XLA Ops:
  0.6 2.1 %shard_map.131 = (bf16[32,22,128]{2,1,0:T(8,128)(2,1)S(1)}, s32[2,256]{1,0:T(2,128)S(1)}, f32[2,64]{1,0:T(2,128)S(1)}, f32[256,64]{1,0:T(8,128)S(1)}, bf16[64,25...) custom-call(s32[1]{0:T(128)} %bitcast.2.refs_0_, bf16[256,2048]{1,0:T(8,128)(2,1)} %refs_1_.2, f32[1,2048]{1,0:T(1,128)} %bitcast.13, ...), custom_call_target="tpu_custom_call" | custom-call | flops 268435456 | bytes 1048576 | tf_op jit(solution)/shard_map/pallas_call | solution.py:25
  2.7 31.6 %all_to_all.20 = bf16[32,22,128]{2,1,0:T(8,128)(2,1)S(1)} all-to-all(bf16[32,22,128]{2,1,0:T(8,128)(2,1)S(1)} %get-tuple-element.28), channel_id=1, replica_groups=mesh['ep'=32,'tp_0'=4,'tp_1'=4] {'ep'}, dimensions={0} | all-to-all | bytes 360448 | tf_op jit(solution)/shard_map/all_to_all | solution.py:283
  34.3 0.1 broadcast_in_dim.7
  34.4 0.5 broadcast_in_dim.8
  34.9 0.0 copy-start.1
  34.9 0.0 copy-start.2
  34.9 0.0 copy-start.3
  35.0 42.6 %all_to_all.21.refs_0_ = bf16[16,704,128]{2,1,0:T(8,128)(2,1)S(1)} all-to-all(bf16[16,704,128]{2,1,0:T(8,128)(2,1)S(1)} %broadcast_in_dim.8), channel_id=1, replica_groups=mesh['ep'=32,'tp_0'=4,'tp_1'=4] {'tp_0','tp_1'}, dimensions={0} | all-to-all | bytes 5767168 | tf_op jit(solution)/shard_map/all_to_all | solution.py:302
  77.6 0.0 copy-done.1
  77.6 0.0 copy-done.2
  77.6 0.0 copy-done.3
  77.6 4.2 %shard_map.135 = bf16[16,704,128]{2,1,0:T(8,128)(2,1)} custom-call(bf16[16,704,128]{2,1,0:T(8,128)(2,1)S(1)} %all_to_all.21.refs_0_, bf16[1,2048,256]{2,1,0:T(8,128)(2,1)S(1)} %copy-done.1, bf16[1,2048,256]{2,1,0:T(8,128)(2,1)S(1)} %copy-done.2, bf16[1,256,2048]{2,1,0:T(8,128)(2,1)S(1)} %copy-done.3), custom_call_target="tpu_custom_call" | custom-call | flops 4294967296 | bytes 1048576 | tf_op jit(solution)/shard_map/pallas_call | solution.py:25
  81.8 40.2 %all_to_all.22.parts = bf16[16,704,128]{2,1,0:T(8,128)(2,1)S(1)} all-to-all(bf16[16,704,128]{2,1,0:T(8,128)(2,1)} %shard_map.135), channel_id=1, replica_groups=mesh['ep'=32,'tp_0'=4,'tp_1'=4] {'tp_0','tp_1'}, dimensions={0} | all-to-all | bytes 5767168 | tf_op jit(solution)/shard_map/all_to_all | solution.py:318
  122.1 0.0 copy-start
  122.1 0.0 copy-start.4
  122.1 1.3 shard_map.136
  123.4 5.3 %all-to-all-start.3 = ((bf16[32,22,128]{2,1,0:T(8,128)(2,1)}), bf16[32,22,128]{2,1,0:T(8,128)(2,1)S(1)}, u32[]{:S(2)}, u32[]{:S(2)}) async-start(bf16[32,22,128]{2,1,0:T(8,128)(2,1)} %shard_map.136), calls=%async_computation.3 | async-start | bytes 393216 | tf_op jit(solution)/shard_map/all_to_all | solution.py:327
  128.7 2.0 %collective-permute-start = (f32[2,64]{1,0:T(2,128)S(1)}, f32[2,64]{1,0:T(2,128)S(1)}, u32[]{:S(2)}, u32[]{:S(2)}) collective-permute-start(f32[2,64]{1,0:T(2,128)S(1)} %get-tuple-element.18), channel_id=1, source_target_pairs={{0,16},{16,32},{32,48},{48,64},{64,80},{80,96},{96,112},{112,128},... | collective-permute-start | bytes 1544 | tf_op jit(solution)/shard_map/ppermute | solution.py:21
  130.7 5.6 %collective-permute-done.halo = f32[2,64]{1,0:T(2,128)S(1)} collective-permute-done((f32[2,64]{1,0:T(2,128)S(1)}, f32[2,64]{1,0:T(2,128)S(1)}, u32[]{:S(2)}, u32[]{:S(2)}) %collective-permute-start) | collective-permute-done | bytes 544 | tf_op jit(solution)/shard_map/ppermute | solution.py:21
  136.4 0.0 copy-done
  136.4 0.5 shard_map.132
  136.9 2.4 %collective-permute-start.1 = (bf16[4,256,128]{2,1,0:T(8,128)(2,1)S(1)}, bf16[4,256,128]{2,1,0:T(8,128)(2,1)S(1)}, u32[]{:S(2)}, u32[]{:S(2)}) collective-permute-start(bf16[4,256,128]{2,1,0:T(8,128)(2,1)S(1)} %get-tuple-element.21), channel_id=1, source_target_pairs={{0,1},{1,2},{2,3},{3,0},{4,5},{5,6},{6,7},{7,4},{8,9},{9,10},{10,1... | collective-permute-start | bytes 786440 | tf_op jit(solution)/shard_map/ppermute | solution.py:198
  139.3 4.5 %collective-permute-start.2 = (bf16[4,256,128]{2,1,0:T(8,128)(2,1)S(1)}, bf16[4,256,128]{2,1,0:T(8,128)(2,1)S(1)}, u32[]{:S(2)}, u32[]{:S(2)}) collective-permute-start(bf16[4,256,128]{2,1,0:T(8,128)(2,1)S(1)} %get-tuple-element.22), channel_id=1, source_target_pairs={{0,2},{1,3},{2,0},{3,1},{4,6},{5,7},{6,4},{7,5},{8,10},{9,11},{10,... | collective-permute-start | bytes 786440 | tf_op jit(solution)/shard_map/ppermute | solution.py:198
  143.8 3.4 %collective-permute-start.3 = (bf16[4,256,128]{2,1,0:T(8,128)(2,1)S(1)}, bf16[4,256,128]{2,1,0:T(8,128)(2,1)S(1)}, u32[]{:S(2)}, u32[]{:S(2)}) collective-permute-start(bf16[4,256,128]{2,1,0:T(8,128)(2,1)S(1)} %get-tuple-element.23), channel_id=1, source_target_pairs={{0,3},{1,0},{2,1},{3,2},{4,7},{5,4},{6,5},{7,6},{8,11},{9,8},{10,9... | collective-permute-start | bytes 786440 | tf_op jit(solution)/shard_map/ppermute | solution.py:198
  147.2 6.8 %collective-permute-done.1.refs_1_ = bf16[4,256,128]{2,1,0:T(8,128)(2,1)S(1)} collective-permute-done((bf16[4,256,128]{2,1,0:T(8,128)(2,1)S(1)}, bf16[4,256,128]{2,1,0:T(8,128)(2,1)S(1)}, u32[]{:S(2)}, u32[]{:S(2)}) %collective-permute-start.1) | collective-permute-done | bytes 262176 | tf_op jit(solution)/shard_map/ppermute | solution.py:198
  154.1 0.0 collective-permute-done.2.refs_2_
  154.1 2.5 %collective-permute-done.3.refs_3_ = bf16[4,256,128]{2,1,0:T(8,128)(2,1)S(1)} collective-permute-done((bf16[4,256,128]{2,1,0:T(8,128)(2,1)S(1)}, bf16[4,256,128]{2,1,0:T(8,128)(2,1)S(1)}, u32[]{:S(2)}, u32[]{:S(2)}) %collective-permute-start.3) | collective-permute-done | bytes 262176 | tf_op jit(solution)/shard_map/ppermute | solution.py:198
  156.6 0.1 shard_map.133
  156.7 3.1 %collective-permute-start.4 = (bf16[256,128]{1,0:T(8,128)(2,1)S(1)}, bf16[256,128]{1,0:T(8,128)(2,1)S(1)}, u32[]{:S(2)}, u32[]{:S(2)}) collective-permute-start(bf16[256,128]{1,0:T(8,128)(2,1)S(1)} %get-tuple-element.25), channel_id=1, source_target_pairs={{0,4},{4,8},{8,12},{12,0},{1,5},{5,9},{9,13},{13,1},{2,6},{6,10},{... | collective-permute-start | bytes 196616 | tf_op jit(solution)/shard_map/ppermute | solution.py:198
  159.9 5.3 %collective-permute-start.5 = (bf16[256,128]{1,0:T(8,128)(2,1)S(1)}, bf16[256,128]{1,0:T(8,128)(2,1)S(1)}, u32[]{:S(2)}, u32[]{:S(2)}) collective-permute-start(bf16[256,128]{1,0:T(8,128)(2,1)S(1)} %get-tuple-element.26), channel_id=1, source_target_pairs={{0,8},{4,12},{8,0},{12,4},{1,9},{5,13},{9,1},{13,5},{2,10},{6,14},... | collective-permute-start | bytes 196616 | tf_op jit(solution)/shard_map/ppermute | solution.py:198
  165.2 2.1 %collective-permute-start.6 = (bf16[256,128]{1,0:T(8,128)(2,1)S(1)}, bf16[256,128]{1,0:T(8,128)(2,1)S(1)}, u32[]{:S(2)}, u32[]{:S(2)}) collective-permute-start(bf16[256,128]{1,0:T(8,128)(2,1)S(1)} %get-tuple-element.27), channel_id=1, source_target_pairs={{0,12},{4,0},{8,4},{12,8},{1,13},{5,1},{9,5},{13,9},{2,14},{6,2},{... | collective-permute-start | bytes 196616 | tf_op jit(solution)/shard_map/ppermute | solution.py:198
  167.3 0.1 copy.16
  167.4 0.0 copy-done.4
  167.4 0.1 copy.17.scores
  167.6 0.0 collective-permute-done.4.refs_1_
  167.6 0.2 collective-permute-done.5.refs_2_
  167.8 3.5 %collective-permute-done.6.refs_3_ = bf16[256,128]{1,0:T(8,128)(2,1)S(1)} collective-permute-done((bf16[256,128]{1,0:T(8,128)(2,1)S(1)}, bf16[256,128]{1,0:T(8,128)(2,1)S(1)}, u32[]{:S(2)}, u32[]{:S(2)}) %collective-permute-start.6) | collective-permute-done | bytes 65568 | tf_op jit(solution)/shard_map/ppermute | solution.py:198
  171.3 0.7 shard_map.134
  172.0 0.0 all-to-all-done.3.rows
  172.0 1.1 shard_map.137
Async XLA Ops:
  34.9 42.7 %copy-start.1 = (bf16[1,2048,256]{2,1,0:T(8,128)(2,1)S(1)}, bf16[1,2048,256]{2,1,0:T(8,128)(2,1)}, u32[]{:S(2)}) copy-start(bf16[1,2048,256]{2,1,0:T(8,128)(2,1)} %refs_1_.3) | copy-start | bytes 3145732
  34.9 42.7 %copy-start.2 = (bf16[1,2048,256]{2,1,0:T(8,128)(2,1)S(1)}, bf16[1,2048,256]{2,1,0:T(8,128)(2,1)}, u32[]{:S(2)}) copy-start(bf16[1,2048,256]{2,1,0:T(8,128)(2,1)} %refs_2_.1) | copy-start | bytes 3145732
  34.9 42.7 %copy-start.3 = (bf16[1,256,2048]{2,1,0:T(8,128)(2,1)S(1)}, bf16[1,256,2048]{2,1,0:T(8,128)(2,1)}, u32[]{:S(2)}) copy-start(bf16[1,256,2048]{2,1,0:T(8,128)(2,1)} %refs_3_.1) | copy-start | bytes 3145732
  122.1 14.3 %copy-start = (f32[3,64]{1,0:T(4,128)S(1)}, f32[3,64]{1,0:T(4,128)}, u32[]{:S(2)}) copy-start(f32[3,64]{1,0:T(4,128)} %taps.1) | copy-start | bytes 2308
  122.1 45.4 %copy-start.4 = (f32[256,2]{0,1:T(2,128)S(1)}, f32[256,2]{0,1:T(2,128)}, u32[]{:S(2)}) copy-start(f32[256,2]{0,1:T(2,128)} %param.20) | copy-start | bytes 6148
  123.4 48.6 %all-to-all-start.3 = ((bf16[32,22,128]{2,1,0:T(8,128)(2,1)}), bf16[32,22,128]{2,1,0:T(8,128)(2,1)S(1)}, u32[]{:S(2)}, u32[]{:S(2)}) async-start(bf16[32,22,128]{2,1,0:T(8,128)(2,1)} %shard_map.136), calls=%async_computation.3 | async-start | bytes 393216 | tf_op jit(solution)/shard_map/all_to_all | solution.py:327
  128.7 7.7 %collective-permute-start = (f32[2,64]{1,0:T(2,128)S(1)}, f32[2,64]{1,0:T(2,128)S(1)}, u32[]{:S(2)}, u32[]{:S(2)}) collective-permute-start(f32[2,64]{1,0:T(2,128)S(1)} %get-tuple-element.18), channel_id=1, source_target_pairs={{0,16},{16,32},{32,48},{48,64},{64,80},{80,96},{96,112},{112,128},... | collective-permute-start | bytes 1544 | tf_op jit(solution)/shard_map/ppermute | solution.py:21
  136.9 17.2 %collective-permute-start.1 = (bf16[4,256,128]{2,1,0:T(8,128)(2,1)S(1)}, bf16[4,256,128]{2,1,0:T(8,128)(2,1)S(1)}, u32[]{:S(2)}, u32[]{:S(2)}) collective-permute-start(bf16[4,256,128]{2,1,0:T(8,128)(2,1)S(1)} %get-tuple-element.21), channel_id=1, source_target_pairs={{0,1},{1,2},{2,3},{3,0},{4,5},{5,6},{6,7},{7,4},{8,9},{9,10},{10,1... | collective-permute-start | bytes 786440 | tf_op jit(solution)/shard_map/ppermute | solution.py:198
  139.3 14.8 %collective-permute-start.2 = (bf16[4,256,128]{2,1,0:T(8,128)(2,1)S(1)}, bf16[4,256,128]{2,1,0:T(8,128)(2,1)S(1)}, u32[]{:S(2)}, u32[]{:S(2)}) collective-permute-start(bf16[4,256,128]{2,1,0:T(8,128)(2,1)S(1)} %get-tuple-element.22), channel_id=1, source_target_pairs={{0,2},{1,3},{2,0},{3,1},{4,6},{5,7},{6,4},{7,5},{8,10},{9,11},{10,... | collective-permute-start | bytes 786440 | tf_op jit(solution)/shard_map/ppermute | solution.py:198
  143.8 12.8 %collective-permute-start.3 = (bf16[4,256,128]{2,1,0:T(8,128)(2,1)S(1)}, bf16[4,256,128]{2,1,0:T(8,128)(2,1)S(1)}, u32[]{:S(2)}, u32[]{:S(2)}) collective-permute-start(bf16[4,256,128]{2,1,0:T(8,128)(2,1)S(1)} %get-tuple-element.23), channel_id=1, source_target_pairs={{0,3},{1,0},{2,1},{3,2},{4,7},{5,4},{6,5},{7,6},{8,11},{9,8},{10,9... | collective-permute-start | bytes 786440 | tf_op jit(solution)/shard_map/ppermute | solution.py:198
  156.7 10.8 %collective-permute-start.4 = (bf16[256,128]{1,0:T(8,128)(2,1)S(1)}, bf16[256,128]{1,0:T(8,128)(2,1)S(1)}, u32[]{:S(2)}, u32[]{:S(2)}) collective-permute-start(bf16[256,128]{1,0:T(8,128)(2,1)S(1)} %get-tuple-element.25), channel_id=1, source_target_pairs={{0,4},{4,8},{8,12},{12,0},{1,5},{5,9},{9,13},{13,1},{2,6},{6,10},{... | collective-permute-start | bytes 196616 | tf_op jit(solution)/shard_map/ppermute | solution.py:198
  159.9 7.9 %collective-permute-start.5 = (bf16[256,128]{1,0:T(8,128)(2,1)S(1)}, bf16[256,128]{1,0:T(8,128)(2,1)S(1)}, u32[]{:S(2)}, u32[]{:S(2)}) collective-permute-start(bf16[256,128]{1,0:T(8,128)(2,1)S(1)} %get-tuple-element.26), channel_id=1, source_target_pairs={{0,8},{4,12},{8,0},{12,4},{1,9},{5,13},{9,1},{13,5},{2,10},{6,14},... | collective-permute-start | bytes 196616 | tf_op jit(solution)/shard_map/ppermute | solution.py:198
  165.2 6.2 %collective-permute-start.6 = (bf16[256,128]{1,0:T(8,128)(2,1)S(1)}, bf16[256,128]{1,0:T(8,128)(2,1)S(1)}, u32[]{:S(2)}, u32[]{:S(2)}) collective-permute-start(bf16[256,128]{1,0:T(8,128)(2,1)S(1)} %get-tuple-element.27), channel_id=1, source_target_pairs={{0,12},{4,0},{8,4},{12,8},{1,13},{5,1},{9,5},{13,9},{2,14},{6,2},{... | collective-permute-start | bytes 196616 | tf_op jit(solution)/shard_map/ppermute | solution.py:198

commit v4 on v3

--- a/solution.py
+++ b/solution.py
@@ -50,12 +50,14 @@
     values_far,
     outer_far,
     proj_far,
+    taps_far,
     sent,
     slots,
     tail,
     product,
     outer,
     proj,
+    taps,
     rows,
     gain,
     ids,
@@ -71,6 +73,7 @@
         (values_far, values),
         (outer_far, outer),
         (proj_far, proj),
+        (taps_far, taps),
     )
     copies = [
         pltpu.make_async_copy(there, here, done.at[n]) for n, (there, here) in enumerate(pairs)
@@ -120,28 +123,21 @@
     sent[...] = placed[:, :capacity, :].astype(BF16)
 
 
-def expert_body(step, tokens, gate_w, up_w, down_w, out, held, done):
+def expert_body(step, tokens, gate_w, up_w, down_w, out):
     blocks, rows, columns = tokens.shape
-    slots = held.shape[0]
-    copies = []
-    for number in range(rows // step):
-        at = slice(number * step, (number + 1) * step)
+
+    def tile(number, carry):
+        at = pl.ds(pl.multiple_of(number * step, step), step)
         left = jnp.concatenate([tokens[b, at, :] for b in range(blocks)], axis=1)
         gate = jnp.dot(left, gate_w[0], preferred_element_type=F32)
         up = jnp.dot(left, up_w[0], preferred_element_type=F32)
         hidden = (gate / (1.0 + jnp.exp(-gate)) * up).astype(BF16)
         part = jnp.dot(hidden, down_w[0], preferred_element_type=F32).astype(BF16)
-        slot = number % slots
-        if number >= slots:
-            copies[number - slots].wait()
         for b in range(blocks):
-            held[slot, b] = part[:, b * columns : (b + 1) * columns]
-        copies.append(
-            pltpu.make_async_copy(held.at[slot], out.at[:, pl.ds(at.start, step), :], done.at[slot])
-        )
-        copies[-1].start()
-    for copy in copies[-slots:]:
-        copy.wait()
+            out[b, at, :] = part[:, b * columns : (b + 1) * columns]
+        return carry
+
+    lax.fori_loop(0, rows // step, tile, 0)
 
 
 def sum_body(parts, out, total):
@@ -249,7 +245,7 @@
     seq_len = gate_in.shape[0]
     channels = gate_in.shape[1]
 
-    sent, slots, tail, product, outer, proj = call(
+    sent, slots, tail, product, outer, proj, taps = call(
         lambda *refs: dispatch_body(stride, experts, *refs),
         (
             jax.ShapeDtypeStruct((experts, capacity, columns), BF16),
@@ -258,6 +254,7 @@
             jax.ShapeDtypeStruct((seq_len, channels), F32),
             jax.ShapeDtypeStruct((channels, seq_len), BF16),
             jax.ShapeDtypeStruct(mixer_proj.shape, BF16),
+            jax.ShapeDtypeStruct(conv_taps.shape, F32),
         ),
         16 << 20,
         1 << 28,
@@ -269,14 +266,15 @@
         far(conv_values.T),
         far(gate_out.T),
         far(mixer_proj),
-        specs=[SMEM] + [HBM] * 7,
+        far(conv_taps),
+        specs=[SMEM] + [HBM] * 8,
         scratch=[
             pltpu.VMEM((tokens, width), BF16),
             pltpu.VMEM((1, width), F32),
             pltpu.VMEM((choices, tokens), jnp.int32),
             pltpu.VMEM((channels, seq_len), BF16),
             pltpu.VMEM((channels, seq_len), BF16),
-            pltpu.SemaphoreType.DMA((7,)),
+            pltpu.SemaphoreType.DMA((8,)),
         ],
     )
     halo = shifted(tail, "ep", 1)
@@ -290,7 +288,7 @@
         place_1,
         outer,
         product,
-        conv_taps,
+        taps,
         halo,
         proj,
         specs=[SMEM] + [VMEM] * 5,
@@ -302,18 +300,13 @@
     gathered = lax.all_to_all(copies, TP, 0, 0, tiled=True)
     parts = call(
         lambda *refs: expert_body(slot_count // 4, *refs),
-        pltpu.HBM((tp_count, slot_count, columns), BF16),
+        jax.ShapeDtypeStruct((tp_count, slot_count, columns), BF16),
         24 << 20,
         1 << 32,
         gathered,
         gate_proj,
         up_proj,
         down_proj,
-        scratch=[
-            pltpu.VMEM((2, tp_count, slot_count // 4, columns), BF16),
-            pltpu.SemaphoreType.DMA((2,)),
-        ],
-        place=HBM,
     )
     shared = lax.all_to_all(parts, TP, 0, 0, tiled=True)
     outputs = call(

time: 174 us -> 172 us (0.989)
  no operation moved by 1% of the time
where the time goes in v4:
time: 172 us; the launch traced here: 171 us
  blocking collectives  114 us (66%)
  starting transfers between devices  27.2 us (16%)
  waiting for transfers between devices  19.2 us (11%)
  Pallas kernels  9.16 us (5%)
    all_to_all x1, blocking collectives, shards(): gathered = lax.all_to_all(copies, TP, 0, 0, tiled=True)  42.6 us
    all_to_all x1, blocking collectives, shards(): shared = lax.all_to_all(parts, TP, 0, 0, tiled=True)  39.5 us
    all_to_all x1, blocking collectives, shards(): arrived = lax.all_to_all(sent, 'ep', 0, 0, tiled=True)  31.6 us
    ppermute x6, starting transfers between devices, turned(): lax.ppermute(block, axis, [(i, (i + distance) % count) for i in range(cou...  19.9 us
    ppermute x6, waiting for transfers between devices, turned(): lax.ppermute(block, axis, [(i, (i + distance) % count) for i in range(cou...  13.6 us
    pallas_call x7, Pallas kernels, call(): pl.pallas_call(body, out_shape=out, in_specs=specs or [VMEM] * len(operan...  9.16 us
    ppermute x1, waiting for transfers between devices, shifted(): return lax.ppermute(block, axis, route)  5.62 us
    all_to_all x1, starting transfers between devices, shards(): returned = lax.all_to_all(outputs, 'ep', 0, 0, tiled=True)  5.31 us
  transfers between devices with their start and end apart: 8, of which 5 were waited for; matrix products, arithmetic and copies ran while one was open for 0% of the time, Pallas kernels for 1%

profile of v4, /device:TPU:72, one launch (start us, length us, event | category | flops | bytes accessed | tf_op | source)
XLA Modules:
  0.0 171.0 jit_solution(17943720451331432594)
XLA Ops:
  0.6 2.1 %shard_map.131 = (bf16[32,22,128]{2,1,0:T(8,128)(2,1)S(1)}, s32[2,256]{1,0:T(2,128)S(1)}, f32[2,64]{1,0:T(2,128)S(1)}, f32[256,64]{1,0:T(8,128)S(1)}, bf16[64,25...) custom-call(s32[1]{0:T(128)} %bitcast.2.refs_0_, bf16[256,2048]{1,0:T(8,128)(2,1)} %refs_1_.2, ...), custom_call_target="tpu_custom_call" | custom-call | flops 268435456 | bytes 1048576 | tf_op jit(solution)/shard_map/pallas_call | solution.py:25
  2.7 31.6 %all_to_all.20 = bf16[32,22,128]{2,1,0:T(8,128)(2,1)S(1)} all-to-all(bf16[32,22,128]{2,1,0:T(8,128)(2,1)S(1)} %get-tuple-element.30), channel_id=1, replica_groups=mesh['ep'=32,'tp_0'=4,'tp_1'=4] {'ep'}, dimensions={0} | all-to-all | bytes 360448 | tf_op jit(solution)/shard_map/all_to_all | solution.py:281
  34.3 0.1 broadcast_in_dim.7
  34.4 0.5 broadcast_in_dim.8
  34.9 0.0 copy-start
  34.9 0.0 copy-start.1
  35.0 0.0 copy-start.2
  35.0 42.6 %all_to_all.21.refs_0_ = bf16[16,704,128]{2,1,0:T(8,128)(2,1)S(1)} all-to-all(bf16[16,704,128]{2,1,0:T(8,128)(2,1)S(1)} %broadcast_in_dim.8), channel_id=1, replica_groups=mesh['ep'=32,'tp_0'=4,'tp_1'=4] {'tp_0','tp_1'}, dimensions={0} | all-to-all | bytes 5767168 | tf_op jit(solution)/shard_map/all_to_all | solution.py:300
  77.6 0.0 copy-done
  77.6 0.0 copy-done.1
  77.6 0.0 copy-done.2
  77.6 3.5 %shard_map.135 = bf16[16,704,128]{2,1,0:T(8,128)(2,1)S(1)} custom-call(bf16[16,704,128]{2,1,0:T(8,128)(2,1)S(1)} %all_to_all.21.refs_0_, bf16[1,2048,256]{2,1,0:T(8,128)(2,1)S(1)} %copy-done, bf16[1,2048,256]{2,1,0:T(8,128)(2,1)S(1)} %copy-done.1, bf16[1,256,2048]{2,1,0:T(8,128)(2,1)S(1)} %copy-done.2), custom_call_target="tpu_custom_call" | custom-call | flops 4294967296 | bytes 1048576 | tf_op jit(solution)/shard_map/pallas_call | solution.py:25
  81.1 39.5 %all_to_all.22.parts = bf16[16,704,128]{2,1,0:T(8,128)(2,1)S(1)} all-to-all(bf16[16,704,128]{2,1,0:T(8,128)(2,1)S(1)} %shard_map.135), channel_id=1, replica_groups=mesh['ep'=32,'tp_0'=4,'tp_1'=4] {'tp_0','tp_1'}, dimensions={0} | all-to-all | bytes 5767168 | tf_op jit(solution)/shard_map/all_to_all | solution.py:311
  120.6 0.0 copy-start.3
  120.6 1.2 shard_map.136
  121.9 5.3 %all-to-all-start.3 = ((bf16[32,22,128]{2,1,0:T(8,128)(2,1)}), bf16[32,22,128]{2,1,0:T(8,128)(2,1)S(1)}, u32[]{:S(2)}, u32[]{:S(2)}) async-start(bf16[32,22,128]{2,1,0:T(8,128)(2,1)} %shard_map.136), calls=%async_computation.3 | async-start | bytes 393216 | tf_op jit(solution)/shard_map/all_to_all | solution.py:320
  127.2 2.0 %collective-permute-start = (f32[2,64]{1,0:T(2,128)S(1)}, f32[2,64]{1,0:T(2,128)S(1)}, u32[]{:S(2)}, u32[]{:S(2)}) collective-permute-start(f32[2,64]{1,0:T(2,128)S(1)} %get-tuple-element.20), channel_id=1, source_target_pairs={{0,16},{16,32},{32,48},{48,64},{64,80},{80,96},{96,112},{112,128},... | collective-permute-start | bytes 1544 | tf_op jit(solution)/shard_map/ppermute | solution.py:21
  129.2 5.6 %collective-permute-done.halo = f32[2,64]{1,0:T(2,128)S(1)} collective-permute-done((f32[2,64]{1,0:T(2,128)S(1)}, f32[2,64]{1,0:T(2,128)S(1)}, u32[]{:S(2)}, u32[]{:S(2)}) %collective-permute-start) | collective-permute-done | bytes 544 | tf_op jit(solution)/shard_map/ppermute | solution.py:21
  134.8 0.5 shard_map.132
  135.3 2.0 %collective-permute-start.1 = (bf16[4,256,128]{2,1,0:T(8,128)(2,1)S(1)}, bf16[4,256,128]{2,1,0:T(8,128)(2,1)S(1)}, u32[]{:S(2)}, u32[]{:S(2)}) collective-permute-start(bf16[4,256,128]{2,1,0:T(8,128)(2,1)S(1)} %get-tuple-element.23), channel_id=1, source_target_pairs={{0,1},{1,2},{2,3},{3,0},{4,5},{5,6},{6,7},{7,4},{8,9},{9,10},{10,1... | collective-permute-start | bytes 786440 | tf_op jit(solution)/shard_map/ppermute | solution.py:194
  137.3 4.5 %collective-permute-start.2 = (bf16[4,256,128]{2,1,0:T(8,128)(2,1)S(1)}, bf16[4,256,128]{2,1,0:T(8,128)(2,1)S(1)}, u32[]{:S(2)}, u32[]{:S(2)}) collective-permute-start(bf16[4,256,128]{2,1,0:T(8,128)(2,1)S(1)} %get-tuple-element.24), channel_id=1, source_target_pairs={{0,2},{1,3},{2,0},{3,1},{4,6},{5,7},{6,4},{7,5},{8,10},{9,11},{10,... | collective-permute-start | bytes 786440 | tf_op jit(solution)/shard_map/ppermute | solution.py:194
  141.9 3.4 %collective-permute-start.3 = (bf16[4,256,128]{2,1,0:T(8,128)(2,1)S(1)}, bf16[4,256,128]{2,1,0:T(8,128)(2,1)S(1)}, u32[]{:S(2)}, u32[]{:S(2)}) collective-permute-start(bf16[4,256,128]{2,1,0:T(8,128)(2,1)S(1)} %get-tuple-element.25), channel_id=1, source_target_pairs={{0,3},{1,0},{2,1},{3,2},{4,7},{5,4},{6,5},{7,6},{8,11},{9,8},{10,9... | collective-permute-start | bytes 786440 | tf_op jit(solution)/shard_map/ppermute | solution.py:194
  145.2 7.3 %collective-permute-done.1.refs_1_ = bf16[4,256,128]{2,1,0:T(8,128)(2,1)S(1)} collective-permute-done((bf16[4,256,128]{2,1,0:T(8,128)(2,1)S(1)}, bf16[4,256,128]{2,1,0:T(8,128)(2,1)S(1)}, u32[]{:S(2)}, u32[]{:S(2)}) %collective-permute-start.1) | collective-permute-done | bytes 262176 | tf_op jit(solution)/shard_map/ppermute | solution.py:194
  152.5 0.0 collective-permute-done.2.refs_2_
  152.5 2.5 %collective-permute-done.3.refs_3_ = bf16[4,256,128]{2,1,0:T(8,128)(2,1)S(1)} collective-permute-done((bf16[4,256,128]{2,1,0:T(8,128)(2,1)S(1)}, bf16[4,256,128]{2,1,0:T(8,128)(2,1)S(1)}, u32[]{:S(2)}, u32[]{:S(2)}) %collective-permute-start.3) | collective-permute-done | bytes 262176 | tf_op jit(solution)/shard_map/ppermute | solution.py:194
  155.1 0.1 shard_map.133
  155.2 2.7 %collective-permute-start.4 = (bf16[256,128]{1,0:T(8,128)(2,1)S(1)}, bf16[256,128]{1,0:T(8,128)(2,1)S(1)}, u32[]{:S(2)}, u32[]{:S(2)}) collective-permute-start(bf16[256,128]{1,0:T(8,128)(2,1)S(1)} %get-tuple-element.27), channel_id=1, source_target_pairs={{0,4},{4,8},{8,12},{12,0},{1,5},{5,9},{9,13},{13,1},{2,6},{6,10},{... | collective-permute-start | bytes 196616 | tf_op jit(solution)/shard_map/ppermute | solution.py:194
  157.9 5.3 %collective-permute-start.5 = (bf16[256,128]{1,0:T(8,128)(2,1)S(1)}, bf16[256,128]{1,0:T(8,128)(2,1)S(1)}, u32[]{:S(2)}, u32[]{:S(2)}) collective-permute-start(bf16[256,128]{1,0:T(8,128)(2,1)S(1)} %get-tuple-element.28), channel_id=1, source_target_pairs={{0,8},{4,12},{8,0},{12,4},{1,9},{5,13},{9,1},{13,5},{2,10},{6,14},... | collective-permute-start | bytes 196616 | tf_op jit(solution)/shard_map/ppermute | solution.py:194
  163.1 2.1 %collective-permute-start.6 = (bf16[256,128]{1,0:T(8,128)(2,1)S(1)}, bf16[256,128]{1,0:T(8,128)(2,1)S(1)}, u32[]{:S(2)}, u32[]{:S(2)}) collective-permute-start(bf16[256,128]{1,0:T(8,128)(2,1)S(1)} %get-tuple-element.29), channel_id=1, source_target_pairs={{0,12},{4,0},{8,4},{12,8},{1,13},{5,1},{9,5},{13,9},{2,14},{6,2},{... | collective-permute-start | bytes 196616 | tf_op jit(solution)/shard_map/ppermute | solution.py:194
  165.3 0.1 copy.16
  165.4 0.0 copy-done.3
  165.4 0.1 copy.17.scores
  165.6 0.0 collective-permute-done.4.refs_1_
  165.6 0.2 collective-permute-done.5.refs_2_
  165.8 3.5 %collective-permute-done.6.refs_3_ = bf16[256,128]{1,0:T(8,128)(2,1)S(1)} collective-permute-done((bf16[256,128]{1,0:T(8,128)(2,1)S(1)}, bf16[256,128]{1,0:T(8,128)(2,1)S(1)}, u32[]{:S(2)}, u32[]{:S(2)}) %collective-permute-start.6) | collective-permute-done | bytes 65568 | tf_op jit(solution)/shard_map/ppermute | solution.py:194
  169.3 0.7 shard_map.134
  170.0 0.0 all-to-all-done.3.rows
  170.0 1.1 shard_map.137
Async XLA Ops:
  34.9 42.7 %copy-start = (bf16[1,2048,256]{2,1,0:T(8,128)(2,1)S(1)}, bf16[1,2048,256]{2,1,0:T(8,128)(2,1)}, u32[]{:S(2)}) copy-start(bf16[1,2048,256]{2,1,0:T(8,128)(2,1)} %refs_1_.3) | copy-start | bytes 3145732
  34.9 42.7 %copy-start.1 = (bf16[1,2048,256]{2,1,0:T(8,128)(2,1)S(1)}, bf16[1,2048,256]{2,1,0:T(8,128)(2,1)}, u32[]{:S(2)}) copy-start(bf16[1,2048,256]{2,1,0:T(8,128)(2,1)} %refs_2_.1) | copy-start | bytes 3145732
  35.0 42.7 %copy-start.2 = (bf16[1,256,2048]{2,1,0:T(8,128)(2,1)S(1)}, bf16[1,256,2048]{2,1,0:T(8,128)(2,1)}, u32[]{:S(2)}) copy-start(bf16[1,256,2048]{2,1,0:T(8,128)(2,1)} %refs_3_.1) | copy-start | bytes 3145732
  120.6 44.8 %copy-start.3 = (f32[256,2]{0,1:T(2,128)S(1)}, f32[256,2]{0,1:T(2,128)}, u32[]{:S(2)}) copy-start(f32[256,2]{0,1:T(2,128)} %param.20) | copy-start | bytes 6148
  121.9 48.1 %all-to-all-start.3 = ((bf16[32,22,128]{2,1,0:T(8,128)(2,1)}), bf16[32,22,128]{2,1,0:T(8,128)(2,1)S(1)}, u32[]{:S(2)}, u32[]{:S(2)}) async-start(bf16[32,22,128]{2,1,0:T(8,128)(2,1)} %shard_map.136), calls=%async_computation.3 | async-start | bytes 393216 | tf_op jit(solution)/shard_map/all_to_all | solution.py:320
  127.2 7.7 %collective-permute-start = (f32[2,64]{1,0:T(2,128)S(1)}, f32[2,64]{1,0:T(2,128)S(1)}, u32[]{:S(2)}, u32[]{:S(2)}) collective-permute-start(f32[2,64]{1,0:T(2,128)S(1)} %get-tuple-element.20), channel_id=1, source_target_pairs={{0,16},{16,32},{32,48},{48,64},{64,80},{80,96},{96,112},{112,128},... | collective-permute-start | bytes 1544 | tf_op jit(solution)/shard_map/ppermute | solution.py:21
  135.3 17.2 %collective-permute-start.1 = (bf16[4,256,128]{2,1,0:T(8,128)(2,1)S(1)}, bf16[4,256,128]{2,1,0:T(8,128)(2,1)S(1)}, u32[]{:S(2)}, u32[]{:S(2)}) collective-permute-start(bf16[4,256,128]{2,1,0:T(8,128)(2,1)S(1)} %get-tuple-element.23), channel_id=1, source_target_pairs={{0,1},{1,2},{2,3},{3,0},{4,5},{5,6},{6,7},{7,4},{8,9},{9,10},{10,1... | collective-permute-start | bytes 786440 | tf_op jit(solution)/shard_map/ppermute | solution.py:194
  137.3 15.2 %collective-permute-start.2 = (bf16[4,256,128]{2,1,0:T(8,128)(2,1)S(1)}, bf16[4,256,128]{2,1,0:T(8,128)(2,1)S(1)}, u32[]{:S(2)}, u32[]{:S(2)}) collective-permute-start(bf16[4,256,128]{2,1,0:T(8,128)(2,1)S(1)} %get-tuple-element.24), channel_id=1, source_target_pairs={{0,2},{1,3},{2,0},{3,1},{4,6},{5,7},{6,4},{7,5},{8,10},{9,11},{10,... | collective-permute-start | bytes 786440 | tf_op jit(solution)/shard_map/ppermute | solution.py:194
  141.9 13.2 %collective-permute-start.3 = (bf16[4,256,128]{2,1,0:T(8,128)(2,1)S(1)}, bf16[4,256,128]{2,1,0:T(8,128)(2,1)S(1)}, u32[]{:S(2)}, u32[]{:S(2)}) collective-permute-start(bf16[4,256,128]{2,1,0:T(8,128)(2,1)S(1)} %get-tuple-element.25), channel_id=1, source_target_pairs={{0,3},{1,0},{2,1},{3,2},{4,7},{5,4},{6,5},{7,6},{8,11},{9,8},{10,9... | collective-permute-start | bytes 786440 | tf_op jit(solution)/shard_map/ppermute | solution.py:194
  155.2 10.3 %collective-permute-start.4 = (bf16[256,128]{1,0:T(8,128)(2,1)S(1)}, bf16[256,128]{1,0:T(8,128)(2,1)S(1)}, u32[]{:S(2)}, u32[]{:S(2)}) collective-permute-start(bf16[256,128]{1,0:T(8,128)(2,1)S(1)} %get-tuple-element.27), channel_id=1, source_target_pairs={{0,4},{4,8},{8,12},{12,0},{1,5},{5,9},{9,13},{13,1},{2,6},{6,10},{... | collective-permute-start | bytes 196616 | tf_op jit(solution)/shard_map/ppermute | solution.py:194
  157.9 7.9 %collective-permute-start.5 = (bf16[256,128]{1,0:T(8,128)(2,1)S(1)}, bf16[256,128]{1,0:T(8,128)(2,1)S(1)}, u32[]{:S(2)}, u32[]{:S(2)}) collective-permute-start(bf16[256,128]{1,0:T(8,128)(2,1)S(1)} %get-tuple-element.28), channel_id=1, source_target_pairs={{0,8},{4,12},{8,0},{12,4},{1,9},{5,13},{9,1},{13,5},{2,10},{6,14},... | collective-permute-start | bytes 196616 | tf_op jit(solution)/shard_map/ppermute | solution.py:194
  163.1 6.2 %collective-permute-start.6 = (bf16[256,128]{1,0:T(8,128)(2,1)S(1)}, bf16[256,128]{1,0:T(8,128)(2,1)S(1)}, u32[]{:S(2)}, u32[]{:S(2)}) collective-permute-start(bf16[256,128]{1,0:T(8,128)(2,1)S(1)} %get-tuple-element.29), channel_id=1, source_target_pairs={{0,12},{4,0},{8,4},{12,8},{1,13},{5,1},{9,5},{13,9},{2,14},{6,2},{... | collective-permute-start | bytes 196616 | tf_op jit(solution)/shard_map/ppermute | solution.py:194

commit v5 on v4

--- a/solution.py
+++ b/solution.py
@@ -123,21 +123,37 @@
     sent[...] = placed[:, :capacity, :].astype(BF16)
 
 
-def expert_body(step, tokens, gate_w, up_w, down_w, out):
-    blocks, rows, columns = tokens.shape
+def expert_body(step, core, tokens, gate_w, up_w, down_w, out):
+    sides, blocks, rows, columns = tokens.shape[0], tokens.shape[1], *tokens.shape[2:]
+    even = core[0] == 0
 
     def tile(number, carry):
         at = pl.ds(pl.multiple_of(number * step, step), step)
-        left = jnp.concatenate([tokens[b, at, :] for b in range(blocks)], axis=1)
+        left = []
+        for y in range(sides):
+            for x in range(blocks):
+                first, second = jnp.where(even, y, x), jnp.where(even, x, y)
+                left.append(tokens[first, second, at, :])
+        left = jnp.concatenate(left, axis=1)
         gate = jnp.dot(left, gate_w[0], preferred_element_type=F32)
         up = jnp.dot(left, up_w[0], preferred_element_type=F32)
         hidden = (gate / (1.0 + jnp.exp(-gate)) * up).astype(BF16)
         part = jnp.dot(hidden, down_w[0], preferred_element_type=F32).astype(BF16)
-        for b in range(blocks):
-            out[b, at, :] = part[:, b * columns : (b + 1) * columns]
+        for y in range(sides):
+            for x in range(blocks):
+                first, second = jnp.where(even, x, y), jnp.where(even, y, x)
+                start = (y * blocks + x) * columns
+                out[first, second, at, :] = part[:, start : start + columns]
         return carry
 
     lax.fori_loop(0, rows // step, tile, 0)
+
+
+def fold_body(parts, out):
+    value = parts[0].astype(F32)
+    for b in range(1, parts.shape[0]):
+        value = value + parts[b].astype(F32)
+    out[...] = value.astype(BF16)
 
 
 def sum_body(parts, out, total):
@@ -187,6 +203,18 @@
     for part in refs[1:-1]:
         total = total + part[...].astype(F32)
     refs[-1][...] = total.astype(BF16)
+
+
+def crossed(block, stage):
+    names = ("ep",) + TP
+    eps, ys, xs = (lax.axis_size(name) for name in names)
+    groups = []
+    for e in range(eps):
+        if (e + stage) % 2 == 0:
+            groups += [[(e * ys + y) * xs + x for x in range(xs)] for y in range(ys)]
+        else:
+            groups += [[(e * ys + y) * xs + x for y in range(ys)] for x in range(xs)]
+    return lax.all_to_all(block, names, 0, 0, axis_index_groups=groups, tiled=True)
 
 
 def turned(block, axis, distance):
@@ -295,20 +323,29 @@
     )
     first = [first[0]] + [turned(first[d], TP[1], d) for d in range(1, turns)]
 
-    own_block = arrived.reshape(1, slot_count, columns)
-    copies = jnp.broadcast_to(own_block, (tp_count, slot_count, columns))
-    gathered = lax.all_to_all(copies, TP, 0, 0, tiled=True)
+    side = lax.axis_size(TP[0])
+    block = (slot_count, columns)
+    core = (lax.axis_index("ep") % 2).astype(jnp.int32).reshape(1)
+    own_block = jnp.broadcast_to(arrived.reshape(1, *block), (side, *block))
+    own_block, core = lax.optimization_barrier((own_block, core))
+    line = crossed(own_block, 0)
+    line = jnp.broadcast_to(line[None], (side, side, *block))
+    gathered = crossed(line, 1)
     parts = call(
         lambda *refs: expert_body(slot_count // 4, *refs),
-        jax.ShapeDtypeStruct((tp_count, slot_count, columns), BF16),
+        jax.ShapeDtypeStruct((side, side, *block), BF16),
         24 << 20,
         1 << 32,
+        core,
         gathered,
         gate_proj,
         up_proj,
         down_proj,
-    )
-    shared = lax.all_to_all(parts, TP, 0, 0, tiled=True)
+        specs=[SMEM] + [VMEM] * 4,
+    )
+    line = crossed(parts, 0)
+    line = call(fold_body, jax.ShapeDtypeStruct((side, *block), BF16), 16 << 20, 1 << 24, line)
+    shared = crossed(line, 1)
     outputs = call(
         sum_body,
         jax.ShapeDtypeStruct((experts, capacity, columns), BF16),

time: 172 us -> 164 us (0.953)
  the two profiles are of different devices: /device:TPU:72 before, /device:TPU:96 now
where the time goes in v5:
time: 164 us; the launch traced here: 163 us
  blocking collectives  73.2 us (45%)
  starting transfers between devices  42.2 us (26%)
  waiting for transfers between devices  36 us (22%)
  Pallas kernels  9.76 us (6%)
    all_to_all x4, blocking collectives, crossed(): lax.all_to_all(block, names, 0, 0, axis_index_groups=groups, tiled=True)  73.2 us
    ppermute x6, starting transfers between devices, turned(): lax.ppermute(block, axis, [(i, (i + distance) % count) for i in range(cou...  18.5 us
    all_to_all x1, waiting for transfers between devices, shards(): arrived = lax.all_to_all(sent, 'ep', 0, 0, tiled=True)  16.6 us
    all_to_all x1, starting transfers between devices, shards(): arrived = lax.all_to_all(sent, 'ep', 0, 0, tiled=True)  14.5 us
    ppermute x6, waiting for transfers between devices, turned(): lax.ppermute(block, axis, [(i, (i + distance) % count) for i in range(cou...  12.5 us
    pallas_call x8, Pallas kernels, call(): pl.pallas_call(body, out_shape=out, in_specs=specs or [VMEM] * len(operan...  9.76 us
    all_to_all x1, starting transfers between devices, shards(): returned = lax.all_to_all(outputs, 'ep', 0, 0, tiled=True)  7.2 us
    ppermute x1, waiting for transfers between devices, shifted(): return lax.ppermute(block, axis, route)  6.93 us
  transfers between devices with their start and end apart: 9, of which 6 were waited for; matrix products, arithmetic and copies ran while one was open for 0% of the time, Pallas kernels for 1%

profile of v5, /device:TPU:96, one launch (start us, length us, event | category | flops | bytes accessed | tf_op | source)
XLA Modules:
  0.0 163.1 jit_solution(3234800071007072136)
XLA Ops:
  0.6 2.7 %shard_map.131 = (bf16[32,22,128]{2,1,0:T(8,128)(2,1)}, s32[2,256]{1,0:T(2,128)S(1)}, f32[2,64]{1,0:T(2,128)S(1)}, f32[256,64]{1,0:T(8,128)S(1)}, bf16[64,256]{1...) custom-call(s32[1]{0:T(128)} %bitcast.2.refs_0_, bf16[256,2048]{1,0:T(8,128)(2,1)} %refs_1_.1, ...), custom_call_target="tpu_custom_call" | custom-call | flops 268435456 | bytes 1048576 | tf_op jit(solution)/shard_map/pallas_call | solution.py:25
  3.4 14.5 %all-to-all-start = ((bf16[32,22,128]{2,1,0:T(8,128)(2,1)}), bf16[32,22,128]{2,1,0:T(8,128)(2,1)S(1)}, u32[]{:S(2)}, u32[]{:S(2)}) async-start(bf16[32,22,128]{2,1,0:T(8,128)(2,1)} %get-tuple-element.32), calls=%async_computation | async-start | bytes 393216 | tf_op jit(solution)/shard_map/all_to_all | solution.py:309
  17.9 16.6 %all-to-all-done = bf16[32,22,128]{2,1,0:T(8,128)(2,1)S(1)} async-done(((bf16[32,22,128]{2,1,0:T(8,128)(2,1)}), bf16[32,22,128]{2,1,0:T(8,128)(2,1)S(1)}, u32[]{:S(2)}, u32[]{:S(2)}) %all-to-all-start) | async-done | bytes 180256 | tf_op jit(solution)/shard_map/all_to_all | solution.py:309
  34.4 0.1 broadcast_in_dim.6
  34.5 0.1 broadcast_in_dim.14
  34.6 13.2 %all_to_all.30 = bf16[4,704,128]{2,1,0:T(8,128)(2,1)S(1)} all-to-all(bf16[4,704,128]{2,1,0:T(8,128)(2,1)S(1)} %broadcast_in_dim.14), channel_id=1, replica_groups={{0,1,2,3},{4,5,6,7},{8,9,10,11},{12,13,14,15},{16,20,24,28},{17,21,25,2..., dimensions={0} | all-to-all | bytes 1441792 | tf_op jit(solution)/shard_map/all_to_all | solution.py:217
  47.8 0.6 broadcast_in_dim.15
  48.4 0.0 copy-start
  48.4 0.0 copy-start.1
  48.4 0.0 copy-start.2
  48.4 25.3 %all_to_all.31.refs_1_ = bf16[4,4,704,128]{3,2,1,0:T(8,128)(2,1)S(1)} all-to-all(bf16[4,4,704,128]{3,2,1,0:T(8,128)(2,1)S(1)} %broadcast_in_dim.15), channel_id=1, replica_groups={{0,4,8,12},{1,5,9,13},{2,6,10,14},{3,7,11,15},{16,17,18,19},{20,21,22,2..., dimensions={0} | all-to-all | bytes 5767168 | tf_op jit(solution)/shard_map/all_to_all | solution.py:217
  73.7 0.0 copy-done
  73.7 0.0 copy-done.1
  73.7 0.0 copy-done.2
  73.7 3.5 %shard_map.135 = bf16[4,4,704,128]{3,2,1,0:T(8,128)(2,1)S(1)} custom-call(s32[1]{0:T(128)} %bitcast.8.refs_0_, bf16[4,4,704,128]{3,2,1,0:T(8,128)(2,1)S(1)} %all_to_all.31.refs_1_, bf16[1,2048,256]{2,1,0:T(8,128)(2,1)S(1)} %copy-done, bf16[1,2048,256]{2,1,0:T(8,128)(2,1)S(1)} %copy-done.1, bf16[1,256,2048]{2,1,0:T(8,128)(2,1)S(1)} %copy-done.2), custom_call_target="tpu_custom_call" | custom-call | flops 4294967296 | bytes 1048576 | tf_op jit(solution)/shard_map/pallas_call | solution.py:25
  77.2 23.2 %all_to_all.32.parts = bf16[4,4,704,128]{3,2,1,0:T(8,128)(2,1)S(1)} all-to-all(bf16[4,4,704,128]{3,2,1,0:T(8,128)(2,1)S(1)} %shard_map.135), channel_id=1, replica_groups={{0,1,2,3},{4,5,6,7},{8,9,10,11},{12,13,14,15},{16,20,24,28},{17,21,25,2..., dimensions={0} | all-to-all | bytes 5767168 | tf_op jit(solution)/shard_map/all_to_all | solution.py:217
  100.4 0.4 shard_map.136
  100.8 0.0 copy-start.3
  100.8 11.5 %all_to_all.33.parts = bf16[4,704,128]{2,1,0:T(8,128)(2,1)S(1)} all-to-all(bf16[4,704,128]{2,1,0:T(8,128)(2,1)S(1)} %shard_map.136), channel_id=1, replica_groups={{0,4,8,12},{1,5,9,13},{2,6,10,14},{3,7,11,15},{16,17,18,19},{20,21,22,2..., dimensions={0} | all-to-all | bytes 1441792 | tf_op jit(solution)/shard_map/all_to_all | solution.py:217
  112.3 0.8 shard_map.137
  113.1 7.2 %all-to-all-start.5 = ((bf16[32,22,128]{2,1,0:T(8,128)(2,1)}), bf16[32,22,128]{2,1,0:T(8,128)(2,1)S(1)}, u32[]{:S(2)}, u32[]{:S(2)}) async-start(bf16[32,22,128]{2,1,0:T(8,128)(2,1)} %shard_map.137), calls=%async_computation.5 | async-start | bytes 393216 | tf_op jit(solution)/shard_map/all_to_all | solution.py:357
  120.4 2.0 %collective-permute-start = (f32[2,64]{1,0:T(2,128)S(1)}, f32[2,64]{1,0:T(2,128)S(1)}, u32[]{:S(2)}, u32[]{:S(2)}) collective-permute-start(f32[2,64]{1,0:T(2,128)S(1)} %get-tuple-element.22), channel_id=1, source_target_pairs={{0,16},{16,32},{32,48},{48,64},{64,80},{80,96},{96,112},{112,128},... | collective-permute-start | bytes 1544 | tf_op jit(solution)/shard_map/ppermute | solution.py:21
  122.4 6.9 %collective-permute-done.halo = f32[2,64]{1,0:T(2,128)S(1)} collective-permute-done((f32[2,64]{1,0:T(2,128)S(1)}, f32[2,64]{1,0:T(2,128)S(1)}, u32[]{:S(2)}, u32[]{:S(2)}) %collective-permute-start) | collective-permute-done | bytes 544 | tf_op jit(solution)/shard_map/ppermute | solution.py:21
  129.3 0.5 shard_map.132
  129.8 2.5 %collective-permute-start.1 = (bf16[4,256,128]{2,1,0:T(8,128)(2,1)S(1)}, bf16[4,256,128]{2,1,0:T(8,128)(2,1)S(1)}, u32[]{:S(2)}, u32[]{:S(2)}) collective-permute-start(bf16[4,256,128]{2,1,0:T(8,128)(2,1)S(1)} %get-tuple-element.25), channel_id=1, source_target_pairs={{0,1},{1,2},{2,3},{3,0},{4,5},{5,6},{6,7},{7,4},{8,9},{9,10},{10,1... | collective-permute-start | bytes 786440 | tf_op jit(solution)/shard_map/ppermute | solution.py:222
  132.3 4.0 %collective-permute-start.2 = (bf16[4,256,128]{2,1,0:T(8,128)(2,1)S(1)}, bf16[4,256,128]{2,1,0:T(8,128)(2,1)S(1)}, u32[]{:S(2)}, u32[]{:S(2)}) collective-permute-start(bf16[4,256,128]{2,1,0:T(8,128)(2,1)S(1)} %get-tuple-element.26), channel_id=1, source_target_pairs={{0,2},{1,3},{2,0},{3,1},{4,6},{5,7},{6,4},{7,5},{8,10},{9,11},{10,... | collective-permute-start | bytes 786440 | tf_op jit(solution)/shard_map/ppermute | solution.py:222
  136.3 2.7 %collective-permute-start.3 = (bf16[4,256,128]{2,1,0:T(8,128)(2,1)S(1)}, bf16[4,256,128]{2,1,0:T(8,128)(2,1)S(1)}, u32[]{:S(2)}, u32[]{:S(2)}) collective-permute-start(bf16[4,256,128]{2,1,0:T(8,128)(2,1)S(1)} %get-tuple-element.27), channel_id=1, source_target_pairs={{0,3},{1,0},{2,1},{3,2},{4,7},{5,4},{6,5},{7,6},{8,11},{9,8},{10,9... | collective-permute-start | bytes 786440 | tf_op jit(solution)/shard_map/ppermute | solution.py:222
  139.0 7.1 %collective-permute-done.1.refs_1_ = bf16[4,256,128]{2,1,0:T(8,128)(2,1)S(1)} collective-permute-done((bf16[4,256,128]{2,1,0:T(8,128)(2,1)S(1)}, bf16[4,256,128]{2,1,0:T(8,128)(2,1)S(1)}, u32[]{:S(2)}, u32[]{:S(2)}) %collective-permute-start.1) | collective-permute-done | bytes 262176 | tf_op jit(solution)/shard_map/ppermute | solution.py:222
  146.1 0.0 collective-permute-done.2.refs_2_
  146.1 2.5 %collective-permute-done.3.refs_3_ = bf16[4,256,128]{2,1,0:T(8,128)(2,1)S(1)} collective-permute-done((bf16[4,256,128]{2,1,0:T(8,128)(2,1)S(1)}, bf16[4,256,128]{2,1,0:T(8,128)(2,1)S(1)}, u32[]{:S(2)}, u32[]{:S(2)}) %collective-permute-start.3) | collective-permute-done | bytes 262176 | tf_op jit(solution)/shard_map/ppermute | solution.py:222
  148.6 0.1 shard_map.133
  148.8 2.5 %collective-permute-start.4 = (bf16[256,128]{1,0:T(8,128)(2,1)S(1)}, bf16[256,128]{1,0:T(8,128)(2,1)S(1)}, u32[]{:S(2)}, u32[]{:S(2)}) collective-permute-start(bf16[256,128]{1,0:T(8,128)(2,1)S(1)} %get-tuple-element.29), channel_id=1, source_target_pairs={{0,4},{4,8},{8,12},{12,0},{1,5},{5,9},{9,13},{13,1},{2,6},{6,10},{... | collective-permute-start | bytes 196616 | tf_op jit(solution)/shard_map/ppermute | solution.py:222
  151.2 4.0 %collective-permute-start.5 = (bf16[256,128]{1,0:T(8,128)(2,1)S(1)}, bf16[256,128]{1,0:T(8,128)(2,1)S(1)}, u32[]{:S(2)}, u32[]{:S(2)}) collective-permute-start(bf16[256,128]{1,0:T(8,128)(2,1)S(1)} %get-tuple-element.30), channel_id=1, source_target_pairs={{0,8},{4,12},{8,0},{12,4},{1,9},{5,13},{9,1},{13,5},{2,10},{6,14},... | collective-permute-start | bytes 196616 | tf_op jit(solution)/shard_map/ppermute | solution.py:222
  155.2 2.9 %collective-permute-start.6 = (bf16[256,128]{1,0:T(8,128)(2,1)S(1)}, bf16[256,128]{1,0:T(8,128)(2,1)S(1)}, u32[]{:S(2)}, u32[]{:S(2)}) collective-permute-start(bf16[256,128]{1,0:T(8,128)(2,1)S(1)} %get-tuple-element.31), channel_id=1, source_target_pairs={{0,12},{4,0},{8,4},{12,8},{1,13},{5,1},{9,5},{13,9},{2,14},{6,2},{... | collective-permute-start | bytes 196616 | tf_op jit(solution)/shard_map/ppermute | solution.py:222
  158.1 0.1 copy.16
  158.3 0.0 copy-done.3
  158.3 0.1 copy.17.scores
  158.4 0.0 collective-permute-done.4.refs_1_
  158.4 0.5 collective-permute-done.5.refs_2_
  158.9 2.5 %collective-permute-done.6.refs_3_ = bf16[256,128]{1,0:T(8,128)(2,1)S(1)} collective-permute-done((bf16[256,128]{1,0:T(8,128)(2,1)S(1)}, bf16[256,128]{1,0:T(8,128)(2,1)S(1)}, u32[]{:S(2)}, u32[]{:S(2)}) %collective-permute-start.6) | collective-permute-done | bytes 65568 | tf_op jit(solution)/shard_map/ppermute | solution.py:222
  161.4 0.7 shard_map.134
  162.1 0.0 all-to-all-done.5.rows
  162.1 1.1 shard_map.138
Async XLA Ops:
  3.4 31.0 %all-to-all-start = ((bf16[32,22,128]{2,1,0:T(8,128)(2,1)}), bf16[32,22,128]{2,1,0:T(8,128)(2,1)S(1)}, u32[]{:S(2)}, u32[]{:S(2)}) async-start(bf16[32,22,128]{2,1,0:T(8,128)(2,1)} %get-tuple-element.32), calls=%async_computation | async-start | bytes 393216 | tf_op jit(solution)/shard_map/all_to_all | solution.py:309
  48.4 25.3 %copy-start = (bf16[1,2048,256]{2,1,0:T(8,128)(2,1)S(1)}, bf16[1,2048,256]{2,1,0:T(8,128)(2,1)}, u32[]{:S(2)}) copy-start(bf16[1,2048,256]{2,1,0:T(8,128)(2,1)} %refs_2_.1) | copy-start | bytes 3145732
  48.4 25.3 %copy-start.1 = (bf16[1,2048,256]{2,1,0:T(8,128)(2,1)S(1)}, bf16[1,2048,256]{2,1,0:T(8,128)(2,1)}, u32[]{:S(2)}) copy-start(bf16[1,2048,256]{2,1,0:T(8,128)(2,1)} %refs_3_.1) | copy-start | bytes 3145732
  48.4 25.3 %copy-start.2 = (bf16[1,256,2048]{2,1,0:T(8,128)(2,1)S(1)}, bf16[1,256,2048]{2,1,0:T(8,128)(2,1)}, u32[]{:S(2)}) copy-start(bf16[1,256,2048]{2,1,0:T(8,128)(2,1)} %refs_4_.1) | copy-start | bytes 3145732
  100.8 57.5 %copy-start.3 = (f32[256,2]{0,1:T(2,128)S(1)}, f32[256,2]{0,1:T(2,128)}, u32[]{:S(2)}) copy-start(f32[256,2]{0,1:T(2,128)} %param.20) | copy-start | bytes 6148
  113.1 48.9 %all-to-all-start.5 = ((bf16[32,22,128]{2,1,0:T(8,128)(2,1)}), bf16[32,22,128]{2,1,0:T(8,128)(2,1)S(1)}, u32[]{:S(2)}, u32[]{:S(2)}) async-start(bf16[32,22,128]{2,1,0:T(8,128)(2,1)} %shard_map.137), calls=%async_computation.5 | async-start | bytes 393216 | tf_op jit(solution)/shard_map/all_to_all | solution.py:357
  120.4 9.0 %collective-permute-start = (f32[2,64]{1,0:T(2,128)S(1)}, f32[2,64]{1,0:T(2,128)S(1)}, u32[]{:S(2)}, u32[]{:S(2)}) collective-permute-start(f32[2,64]{1,0:T(2,128)S(1)} %get-tuple-element.22), channel_id=1, source_target_pairs={{0,16},{16,32},{32,48},{48,64},{64,80},{80,96},{96,112},{112,128},... | collective-permute-start | bytes 1544 | tf_op jit(solution)/shard_map/ppermute | solution.py:21
  129.8 16.3 %collective-permute-start.1 = (bf16[4,256,128]{2,1,0:T(8,128)(2,1)S(1)}, bf16[4,256,128]{2,1,0:T(8,128)(2,1)S(1)}, u32[]{:S(2)}, u32[]{:S(2)}) collective-permute-start(bf16[4,256,128]{2,1,0:T(8,128)(2,1)S(1)} %get-tuple-element.25), channel_id=1, source_target_pairs={{0,1},{1,2},{2,3},{3,0},{4,5},{5,6},{6,7},{7,4},{8,9},{9,10},{10,1... | collective-permute-start | bytes 786440 | tf_op jit(solution)/shard_map/ppermute | solution.py:222
  132.3 13.8 %collective-permute-start.2 = (bf16[4,256,128]{2,1,0:T(8,128)(2,1)S(1)}, bf16[4,256,128]{2,1,0:T(8,128)(2,1)S(1)}, u32[]{:S(2)}, u32[]{:S(2)}) collective-permute-start(bf16[4,256,128]{2,1,0:T(8,128)(2,1)S(1)} %get-tuple-element.26), channel_id=1, source_target_pairs={{0,2},{1,3},{2,0},{3,1},{4,6},{5,7},{6,4},{7,5},{8,10},{9,11},{10,... | collective-permute-start | bytes 786440 | tf_op jit(solution)/shard_map/ppermute | solution.py:222
  136.3 12.3 %collective-permute-start.3 = (bf16[4,256,128]{2,1,0:T(8,128)(2,1)S(1)}, bf16[4,256,128]{2,1,0:T(8,128)(2,1)S(1)}, u32[]{:S(2)}, u32[]{:S(2)}) collective-permute-start(bf16[4,256,128]{2,1,0:T(8,128)(2,1)S(1)} %get-tuple-element.27), channel_id=1, source_target_pairs={{0,3},{1,0},{2,1},{3,2},{4,7},{5,4},{6,5},{7,6},{8,11},{9,8},{10,9... | collective-permute-start | bytes 786440 | tf_op jit(solution)/shard_map/ppermute | solution.py:222
  148.8 9.7 %collective-permute-start.4 = (bf16[256,128]{1,0:T(8,128)(2,1)S(1)}, bf16[256,128]{1,0:T(8,128)(2,1)S(1)}, u32[]{:S(2)}, u32[]{:S(2)}) collective-permute-start(bf16[256,128]{1,0:T(8,128)(2,1)S(1)} %get-tuple-element.29), channel_id=1, source_target_pairs={{0,4},{4,8},{8,12},{12,0},{1,5},{5,9},{9,13},{13,1},{2,6},{6,10},{... | collective-permute-start | bytes 196616 | tf_op jit(solution)/shard_map/ppermute | solution.py:222
  151.2 7.7 %collective-permute-start.5 = (bf16[256,128]{1,0:T(8,128)(2,1)S(1)}, bf16[256,128]{1,0:T(8,128)(2,1)S(1)}, u32[]{:S(2)}, u32[]{:S(2)}) collective-permute-start(bf16[256,128]{1,0:T(8,128)(2,1)S(1)} %get-tuple-element.30), channel_id=1, source_target_pairs={{0,8},{4,12},{8,0},{12,4},{1,9},{5,13},{9,1},{13,5},{2,10},{6,14},... | collective-permute-start | bytes 196616 | tf_op jit(solution)/shard_map/ppermute | solution.py:222
  155.2 6.2 %collective-permute-start.6 = (bf16[256,128]{1,0:T(8,128)(2,1)S(1)}, bf16[256,128]{1,0:T(8,128)(2,1)S(1)}, u32[]{:S(2)}, u32[]{:S(2)}) collective-permute-start(bf16[256,128]{1,0:T(8,128)(2,1)S(1)} %get-tuple-element.31), channel_id=1, source_target_pairs={{0,12},{4,0},{8,4},{12,8},{1,13},{5,1},{9,5},{13,9},{2,14},{6,2},{... | collective-permute-start | bytes 196616 | tf_op jit(solution)/shard_map/ppermute | solution.py:222

commit v6 on v4

--- a/solution.py
+++ b/solution.py
@@ -123,21 +123,52 @@
     sent[...] = placed[:, :capacity, :].astype(BF16)
 
 
-def expert_body(step, tokens, gate_w, up_w, down_w, out):
-    blocks, rows, columns = tokens.shape
+def weights_body(order, gate_far, up_far, down_far, gate_w, up_w, down_w, done):
+    count = order.shape[0]
+    columns = gate_w.shape[0] // count
+    copies = []
+    for p in range(count):
+        near = pl.ds(p * columns, columns)
+        there = pl.ds(pl.multiple_of(order[p] * columns, columns), columns)
+        for n, (source, target) in enumerate(
+            (
+                (gate_far.at[0, there, :], gate_w.at[near, :]),
+                (up_far.at[0, there, :], up_w.at[near, :]),
+                (down_far.at[0, :, there], down_w.at[:, near]),
+            )
+        ):
+            copies.append(pltpu.make_async_copy(source, target, done.at[3 * p + n]))
+            copies[-1].start()
+    for copy in copies:
+        copy.wait()
+
+
+def expert_body(step, *refs):
+    sides = (len(refs) - 3) // 2
+    tokens, outs = refs[:sides], refs[sides + 3 :]
+    gate_w, up_w, down_w = refs[sides : sides + 3]
+    blocks, rows, columns = tokens[0].shape
+    spots = [(n, m) for n in range(sides) for m in range(blocks)]
 
     def tile(number, carry):
         at = pl.ds(pl.multiple_of(number * step, step), step)
-        left = jnp.concatenate([tokens[b, at, :] for b in range(blocks)], axis=1)
-        gate = jnp.dot(left, gate_w[0], preferred_element_type=F32)
-        up = jnp.dot(left, up_w[0], preferred_element_type=F32)
+        left = jnp.concatenate([tokens[n][m, at, :] for n, m in spots], axis=1)
+        gate = jnp.dot(left, gate_w[...], preferred_element_type=F32)
+        up = jnp.dot(left, up_w[...], preferred_element_type=F32)
         hidden = (gate / (1.0 + jnp.exp(-gate)) * up).astype(BF16)
-        part = jnp.dot(hidden, down_w[0], preferred_element_type=F32).astype(BF16)
-        for b in range(blocks):
-            out[b, at, :] = part[:, b * columns : (b + 1) * columns]
+        part = jnp.dot(hidden, down_w[...], preferred_element_type=F32).astype(BF16)
+        for p, (n, m) in enumerate(spots):
+            outs[n][m, at, :] = part[:, p * columns : (p + 1) * columns]
         return carry
 
     lax.fori_loop(0, rows // step, tile, 0)
+
+
+def fold_body(*refs):
+    value = refs[0][...].astype(F32)
+    for part in refs[1:-1]:
+        value = value + part[...].astype(F32)
+    refs[-1][...] = value.astype(BF16)
 
 
 def sum_body(parts, out, total):
@@ -187,6 +218,56 @@
     for part in refs[1:-1]:
         total = total + part[...].astype(F32)
     refs[-1][...] = total.astype(BF16)
+
+
+PAIRS = (((1, 2), (3, 0)), ((0, 1), (2, 3)))
+
+
+def squares(pairing):
+    return [[(y, x) for y in ys for x in xs] for ys in PAIRS[pairing] for xs in PAIRS[pairing]]
+
+
+def crossed(block, stage):
+    names = ("ep",) + TP
+    eps, _, xs = (lax.axis_size(name) for name in names)
+    groups = []
+    for e in range(eps):
+        for square in squares((e + stage) % 2):
+            groups.append([(e * xs + y) * xs + x for y, x in square])
+    return lax.all_to_all(block, names, 0, 0, axis_index_groups=groups, tiled=True)
+
+
+def flipped(spot, stage, flip):
+    pair = {}
+    for low, high in PAIRS[stage]:
+        pair[low], pair[high] = high, low
+    return (pair[spot[0]] if flip & 2 else spot[0], pair[spot[1]] if flip & 1 else spot[1])
+
+
+def arrivals(side):
+    rows = []
+    for core in range(2):
+        for y in range(side):
+            for x in range(side):
+                row = []
+                for flip in range(4):
+                    member = flipped((y, x), (core + 1) % 2, flip)
+                    group = next(g for g in squares(core % 2) if member in g)
+                    row += [there_y * side + there_x for there_y, there_x in group]
+                rows.append(row)
+    return rows
+
+
+def swapped(block, flip):
+    names = ("ep",) + TP
+    eps, ys, xs = (lax.axis_size(name) for name in names)
+    route = []
+    for e in range(eps):
+        for y in range(ys):
+            for x in range(xs):
+                to_y, to_x = flipped((y, x), (e + 1) % 2, flip)
+                route.append(((e * ys + y) * xs + x, (e * ys + to_y) * xs + to_x))
+    return lax.ppermute(block, names, route)
 
 
 def turned(block, axis, distance):
@@ -295,20 +376,52 @@
     )
     first = [first[0]] + [turned(first[d], TP[1], d) for d in range(1, turns)]
 
-    own_block = arrived.reshape(1, slot_count, columns)
-    copies = jnp.broadcast_to(own_block, (tp_count, slot_count, columns))
-    gathered = lax.all_to_all(copies, TP, 0, 0, tiled=True)
+    side = lax.axis_size(TP[0])
+    block = (slot_count, columns)
+    table = jnp.array(arrivals(side), jnp.int32)
+    core = lax.axis_index("ep") % 2
+    order = lax.dynamic_index_in_dim(
+        table, core * tp_count + lax.axis_index(TP), keepdims=False
+    )
+    own_block = jnp.broadcast_to(arrived.reshape(1, *block), (side, *block))
+    own_block, order = lax.optimization_barrier((own_block, order))
+    line = crossed(own_block, 0)
+    lines = [line]
+    for flip in (1, 2, 3):
+        lines.append(swapped(line, flip))
+    weights = call(
+        weights_body,
+        tuple(
+            jax.ShapeDtypeStruct(w.shape[1:], BF16) for w in (gate_proj, up_proj, down_proj)
+        ),
+        8 << 20,
+        1 << 22,
+        order,
+        far(gate_proj),
+        far(up_proj),
+        far(down_proj),
+        specs=[SMEM, HBM, HBM, HBM],
+        scratch=[pltpu.SemaphoreType.DMA((3 * tp_count,))],
+    )
     parts = call(
-        lambda *refs: expert_body(slot_count // 4, *refs),
-        jax.ShapeDtypeStruct((tp_count, slot_count, columns), BF16),
+        lambda *refs: expert_body(slot_count // 2, *refs),
+        (jax.ShapeDtypeStruct((side, *block), BF16),) * side,
         24 << 20,
         1 << 32,
-        gathered,
-        gate_proj,
-        up_proj,
-        down_proj,
-    )
-    shared = lax.all_to_all(parts, TP, 0, 0, tiled=True)
+        *lines,
+        *weights,
+    )
+    parts = list(parts)
+    for flip in (1, 2, 3):
+        parts[flip] = swapped(parts[flip], flip)
+    line = call(
+        fold_body,
+        jax.ShapeDtypeStruct((side, *block), BF16),
+        16 << 20,
+        1 << 24,
+        *parts,
+    )
+    shared = crossed(line, 0)
     outputs = call(
         sum_body,
         jax.ShapeDtypeStruct((experts, capacity, columns), BF16),

time: 172 us -> 165 us (0.959)
  the two profiles are of different devices: /device:TPU:72 before, /device:TPU:64 now
where the time goes in v6:
time: 165 us
  starting transfers between devices  62.3 us (38%)
  waiting for transfers between devices  61.1 us (37%)
  blocking collectives  26.8 us (16%)
  Pallas kernels  11.9 us (7%)
    all_to_all x2, blocking collectives, crossed(): lax.all_to_all(block, names, 0, 0, axis_index_groups=groups, tiled=True)  26.8 us
    ppermute x6, waiting for transfers between devices, swapped(): return lax.ppermute(block, names, route)  26.3 us
    ppermute x6, starting transfers between devices, turned(): lax.ppermute(block, axis, [(i, (i + distance) % count) for i in range(cou...  20.1 us
    ppermute x6, starting transfers between devices, swapped(): return lax.ppermute(block, names, route)  18.4 us
    all_to_all x1, waiting for transfers between devices, shards(): arrived = lax.all_to_all(sent, 'ep', 0, 0, tiled=True)  16.2 us
    all_to_all x1, starting transfers between devices, shards(): arrived = lax.all_to_all(sent, 'ep', 0, 0, tiled=True)  14.9 us
    ppermute x6, waiting for transfers between devices, turned(): lax.ppermute(block, axis, [(i, (i + distance) % count) for i in range(cou...  13.1 us
    pallas_call x9, Pallas kernels, call(): pl.pallas_call(body, out_shape=out, in_specs=specs or [VMEM] * len(operan...  11.9 us
  transfers between devices with their start and end apart: 15, of which 10 were waited for; matrix products, arithmetic and copies ran while one was open for 1% of the time, Pallas kernels for 3%

profile of v6, /device:TPU:64, one launch (start us, length us, event | category | flops | bytes accessed | tf_op | source)
XLA Modules:
  0.0 164.6 jit_solution(4222993410300204825)
XLA Ops:
  0.6 2.7 %shard_map.140 = (bf16[32,22,128]{2,1,0:T(8,128)(2,1)}, s32[2,256]{1,0:T(2,128)S(1)}, f32[2,64]{1,0:T(2,128)S(1)}, f32[256,64]{1,0:T(8,128)S(1)}, bf16[64,256]{1...) custom-call(s32[1]{0:T(128)} %bitcast.2.refs_0_, bf16[256,2048]{1,0:T(8,128)(2,1)} %refs_1_.1, ...), custom_call_target="tpu_custom_call" | custom-call | flops 268435456 | bytes 1048576 | tf_op jit(solution)/shard_map/pallas_call | solution.py:25
  3.4 14.9 %all-to-all-start = ((bf16[32,22,128]{2,1,0:T(8,128)(2,1)}), bf16[32,22,128]{2,1,0:T(8,128)(2,1)S(1)}, u32[]{:S(2)}, u32[]{:S(2)}) async-start(bf16[32,22,128]{2,1,0:T(8,128)(2,1)} %get-tuple-element.39), calls=%async_computation | async-start | bytes 393216 | tf_op jit(solution)/shard_map/all_to_all | solution.py:362
  18.3 0.7 dynamic-slice_bitcast_fusion.order
  19.0 16.2 %all-to-all-done = bf16[32,22,128]{2,1,0:T(8,128)(2,1)S(1)} async-done(((bf16[32,22,128]{2,1,0:T(8,128)(2,1)}), bf16[32,22,128]{2,1,0:T(8,128)(2,1)S(1)}, u32[]{:S(2)}, u32[]{:S(2)}) %all-to-all-start) | async-done | bytes 180256 | tf_op jit(solution)/shard_map/all_to_all | solution.py:362
  35.2 0.1 broadcast_in_dim.7
  35.3 0.1 broadcast_in_dim.8
  35.4 13.6 %all_to_all.20.refs_0_ = bf16[4,704,128]{2,1,0:T(8,128)(2,1)S(1)} all-to-all(bf16[4,704,128]{2,1,0:T(8,128)(2,1)S(1)} %broadcast_in_dim.8), channel_id=1, replica_groups={{5,6,9,10},{7,4,11,8},{13,14,1,2},{15,12,3,0},{16,17,20,21},{18,19,22,2..., dimensions={0} | all-to-all | bytes 1441792 | tf_op jit(solution)/shard_map/all_to_all | solution.py:237
  49.0 2.4 %collective-permute-start.7 = (bf16[4,704,128]{2,1,0:T(8,128)(2,1)S(1)}, bf16[4,704,128]{2,1,0:T(8,128)(2,1)S(1)}, u32[]{:S(2)}, u32[]{:S(2)}) collective-permute-start(bf16[4,704,128]{2,1,0:T(8,128)(2,1)S(1)} %all_to_all.20.refs_0_), channel_id=1, source_target_pairs={{0,1},{1,0},{2,3},{3,2},{4,5},{5,4},{6,7},{7,6},{8,9},{9,8},{10,11... | collective-permute-start | bytes 2162696 | tf_op jit(solution)/shard_map/ppermute | solution.py:270
  51.4 2.8 %collective-permute-start.8 = (bf16[4,704,128]{2,1,0:T(8,128)(2,1)S(1)}, bf16[4,704,128]{2,1,0:T(8,128)(2,1)S(1)}, u32[]{:S(2)}, u32[]{:S(2)}) collective-permute-start(bf16[4,704,128]{2,1,0:T(8,128)(2,1)S(1)} %all_to_all.20.refs_0_), channel_id=1, source_target_pairs={{0,4},{1,5},{2,6},{3,7},{4,0},{5,1},{6,2},{7,3},{8,12},{9,13},{10,... | collective-permute-start | bytes 2162696 | tf_op jit(solution)/shard_map/ppermute | solution.py:270
  54.2 4.0 %collective-permute-start.9 = (bf16[4,704,128]{2,1,0:T(8,128)(2,1)S(1)}, bf16[4,704,128]{2,1,0:T(8,128)(2,1)S(1)}, u32[]{:S(2)}, u32[]{:S(2)}) collective-permute-start(bf16[4,704,128]{2,1,0:T(8,128)(2,1)S(1)} %all_to_all.20.refs_0_), channel_id=1, source_target_pairs={{0,5},{1,4},{2,7},{3,6},{4,1},{5,0},{6,3},{7,2},{8,13},{9,12},{10,... | collective-permute-start | bytes 2162696 | tf_op jit(solution)/shard_map/ppermute | solution.py:270
  58.2 2.9 %shard_map.144 = (bf16[2048,256]{1,0:T(8,128)(2,1)S(1)}, bf16[2048,256]{1,0:T(8,128)(2,1)S(1)}, bf16[256,2048]{1,0:T(8,128)(2,1)S(1)}) custom-call(s32[16]{0:T(128)S(1)} %dynamic-slice_bitcast_fusion.order, bf16[1,2048,256]{2,1,0:T(8,128)(2,1)} %gate_far.1, bf16[1,2048,256]{2,1,0:T(8,128)(2,1)} %up_far.1, bf16[1,256,2048]{2,1,0:T(8,128)(2,1)} %down_far.1), custom_call_target="tpu_custom_call" | custom-call | flops 4194304 | bytes 1048576 | tf_op jit(solution)/shard_map/pallas_call | solution.py:25
  61.1 1.1 collective-permute-done.7.refs_1_
  62.1 10.2 %collective-permute-done.8.refs_2_ = bf16[4,704,128]{2,1,0:T(8,128)(2,1)S(1)} collective-permute-done((bf16[4,704,128]{2,1,0:T(8,128)(2,1)S(1)}, bf16[4,704,128]{2,1,0:T(8,128)(2,1)S(1)}, u32[]{:S(2)}, u32[]{:S(2)}) %collective-permute-start.8) | collective-permute-done | bytes 720928 | tf_op jit(solution)/shard_map/ppermute | solution.py:270
  72.3 0.0 collective-permute-done.9.refs_3_
  72.3 2.7 %shard_map.145 = (bf16[4,704,128]{2,1,0:T(8,128)(2,1)S(1)}, bf16[4,704,128]{2,1,0:T(8,128)(2,1)S(1)}, bf16[4,704,128]{2,1,0:T(8,128)(2,1)S(1)}, bf16[4,704,128]{2,1,0:T(8,128)(2,1)S(1)}) custom-call(bf16[4,704,128]{2,1,0:T(8,128)(2,1)S(1)} %all_to_all.20.refs_0_, bf16[4,704,128]{2,1,0:T(8,128)(2,1)S(1)} %collective-permute-done.7.refs_1_, ...), custom_call_target="tpu_custom_call" | custom-call | flops 4294967296 | bytes 1048576 | tf_op jit(solution)/shard_map/pallas_call | solution.py:25
  75.1 3.4 %collective-permute-start.10 = (bf16[4,704,128]{2,1,0:T(8,128)(2,1)S(1)}, bf16[4,704,128]{2,1,0:T(8,128)(2,1)S(1)}, u32[]{:S(2)}, u32[]{:S(2)}) collective-permute-start(bf16[4,704,128]{2,1,0:T(8,128)(2,1)S(1)} %get-tuple-element.46), channel_id=1, source_target_pairs={{0,1},{1,0},{2,3},{3,2},{4,5},{5,4},{6,7},{7,6},{8,9},{9,8},{10,11... | collective-permute-start | bytes 2162696 | tf_op jit(solution)/shard_map/ppermute | solution.py:270
  78.5 2.4 %collective-permute-start.11 = (bf16[4,704,128]{2,1,0:T(8,128)(2,1)S(1)}, bf16[4,704,128]{2,1,0:T(8,128)(2,1)S(1)}, u32[]{:S(2)}, u32[]{:S(2)}) collective-permute-start(bf16[4,704,128]{2,1,0:T(8,128)(2,1)S(1)} %get-tuple-element.47), channel_id=1, source_target_pairs={{0,4},{1,5},{2,6},{3,7},{4,0},{5,1},{6,2},{7,3},{8,12},{9,13},{10,... | collective-permute-start | bytes 2162696 | tf_op jit(solution)/shard_map/ppermute | solution.py:270
  80.8 3.5 %collective-permute-start.12 = (bf16[4,704,128]{2,1,0:T(8,128)(2,1)S(1)}, bf16[4,704,128]{2,1,0:T(8,128)(2,1)S(1)}, u32[]{:S(2)}, u32[]{:S(2)}) collective-permute-start(bf16[4,704,128]{2,1,0:T(8,128)(2,1)S(1)} %get-tuple-element.48), channel_id=1, source_target_pairs={{0,5},{1,4},{2,7},{3,6},{4,1},{5,0},{6,3},{7,2},{8,13},{9,12},{10,... | collective-permute-start | bytes 2162696 | tf_op jit(solution)/shard_map/ppermute | solution.py:270
  84.3 3.9 %collective-permute-done.10.refs_1_ = bf16[4,704,128]{2,1,0:T(8,128)(2,1)S(1)} collective-permute-done((bf16[4,704,128]{2,1,0:T(8,128)(2,1)S(1)}, bf16[4,704,128]{2,1,0:T(8,128)(2,1)S(1)}, u32[]{:S(2)}, u32[]{:S(2)}) %collective-permute-start.10) | collective-permute-done | bytes 720928 | tf_op jit(solution)/shard_map/ppermute | solution.py:270
  88.3 11.1 %collective-permute-done.11.refs_2_ = bf16[4,704,128]{2,1,0:T(8,128)(2,1)S(1)} collective-permute-done((bf16[4,704,128]{2,1,0:T(8,128)(2,1)S(1)}, bf16[4,704,128]{2,1,0:T(8,128)(2,1)S(1)}, u32[]{:S(2)}, u32[]{:S(2)}) %collective-permute-start.11) | collective-permute-done | bytes 720928 | tf_op jit(solution)/shard_map/ppermute | solution.py:270
  99.4 0.0 collective-permute-done.12.refs_3_
  99.4 0.4 shard_map.146
  99.7 13.2 %all_to_all.21.parts = bf16[4,704,128]{2,1,0:T(8,128)(2,1)S(1)} all-to-all(bf16[4,704,128]{2,1,0:T(8,128)(2,1)S(1)} %shard_map.146), channel_id=1, replica_groups={{5,6,9,10},{7,4,11,8},{13,14,1,2},{15,12,3,0},{16,17,20,21},{18,19,22,2..., dimensions={0} | all-to-all | bytes 1441792 | tf_op jit(solution)/shard_map/all_to_all | solution.py:237
  112.9 0.8 shard_map.147
  113.7 6.9 %all-to-all-start.3 = ((bf16[32,22,128]{2,1,0:T(8,128)(2,1)}), bf16[32,22,128]{2,1,0:T(8,128)(2,1)S(1)}, u32[]{:S(2)}, u32[]{:S(2)}) async-start(bf16[32,22,128]{2,1,0:T(8,128)(2,1)} %shard_map.147), calls=%async_computation.3 | async-start | bytes 393216 | tf_op jit(solution)/shard_map/all_to_all | solution.py:433
  120.6 2.0 %collective-permute-start = (f32[2,64]{1,0:T(2,128)S(1)}, f32[2,64]{1,0:T(2,128)S(1)}, u32[]{:S(2)}, u32[]{:S(2)}) collective-permute-start(f32[2,64]{1,0:T(2,128)S(1)} %get-tuple-element.29), channel_id=1, source_target_pairs={{0,16},{16,32},{32,48},{48,64},{64,80},{80,96},{96,112},{112,128},... | collective-permute-start | bytes 1544 | tf_op jit(solution)/shard_map/ppermute | solution.py:21
  122.6 5.5 %collective-permute-done.halo = f32[2,64]{1,0:T(2,128)S(1)} collective-permute-done((f32[2,64]{1,0:T(2,128)S(1)}, f32[2,64]{1,0:T(2,128)S(1)}, u32[]{:S(2)}, u32[]{:S(2)}) %collective-permute-start) | collective-permute-done | bytes 544 | tf_op jit(solution)/shard_map/ppermute | solution.py:21
  128.2 0.5 shard_map.141
  128.7 1.9 %collective-permute-start.1 = (bf16[4,256,128]{2,1,0:T(8,128)(2,1)S(1)}, bf16[4,256,128]{2,1,0:T(8,128)(2,1)S(1)}, u32[]{:S(2)}, u32[]{:S(2)}) collective-permute-start(bf16[4,256,128]{2,1,0:T(8,128)(2,1)S(1)} %get-tuple-element.32), channel_id=1, source_target_pairs={{0,1},{1,2},{2,3},{3,0},{4,5},{5,6},{6,7},{7,4},{8,9},{9,10},{10,1... | collective-permute-start | bytes 786440 | tf_op jit(solution)/shard_map/ppermute | solution.py:275
  130.6 6.2 %collective-permute-start.2 = (bf16[4,256,128]{2,1,0:T(8,128)(2,1)S(1)}, bf16[4,256,128]{2,1,0:T(8,128)(2,1)S(1)}, u32[]{:S(2)}, u32[]{:S(2)}) collective-permute-start(bf16[4,256,128]{2,1,0:T(8,128)(2,1)S(1)} %get-tuple-element.33), channel_id=1, source_target_pairs={{0,2},{1,3},{2,0},{3,1},{4,6},{5,7},{6,4},{7,5},{8,10},{9,11},{10,... | collective-permute-start | bytes 786440 | tf_op jit(solution)/shard_map/ppermute | solution.py:275
  136.8 1.9 %collective-permute-start.3 = (bf16[4,256,128]{2,1,0:T(8,128)(2,1)S(1)}, bf16[4,256,128]{2,1,0:T(8,128)(2,1)S(1)}, u32[]{:S(2)}, u32[]{:S(2)}) collective-permute-start(bf16[4,256,128]{2,1,0:T(8,128)(2,1)S(1)} %get-tuple-element.34), channel_id=1, source_target_pairs={{0,3},{1,0},{2,1},{3,2},{4,7},{5,4},{6,5},{7,6},{8,11},{9,8},{10,9... | collective-permute-start | bytes 786440 | tf_op jit(solution)/shard_map/ppermute | solution.py:275
  138.7 1.5 collective-permute-done.1.refs_1_
  140.3 6.7 %collective-permute-done.2.refs_2_ = bf16[4,256,128]{2,1,0:T(8,128)(2,1)S(1)} collective-permute-done((bf16[4,256,128]{2,1,0:T(8,128)(2,1)S(1)}, bf16[4,256,128]{2,1,0:T(8,128)(2,1)S(1)}, u32[]{:S(2)}, u32[]{:S(2)}) %collective-permute-start.2) | collective-permute-done | bytes 262176 | tf_op jit(solution)/shard_map/ppermute | solution.py:275
  147.0 1.5 collective-permute-done.3.refs_3_
  148.4 0.1 shard_map.142
  148.6 1.9 %collective-permute-start.4 = (bf16[256,128]{1,0:T(8,128)(2,1)S(1)}, bf16[256,128]{1,0:T(8,128)(2,1)S(1)}, u32[]{:S(2)}, u32[]{:S(2)}) collective-permute-start(bf16[256,128]{1,0:T(8,128)(2,1)S(1)} %get-tuple-element.36), channel_id=1, source_target_pairs={{0,4},{4,8},{8,12},{12,0},{1,5},{5,9},{9,13},{13,1},{2,6},{6,10},{... | collective-permute-start | bytes 196616 | tf_op jit(solution)/shard_map/ppermute | solution.py:275
  150.5 6.2 %collective-permute-start.5 = (bf16[256,128]{1,0:T(8,128)(2,1)S(1)}, bf16[256,128]{1,0:T(8,128)(2,1)S(1)}, u32[]{:S(2)}, u32[]{:S(2)}) collective-permute-start(bf16[256,128]{1,0:T(8,128)(2,1)S(1)} %get-tuple-element.37), channel_id=1, source_target_pairs={{0,8},{4,12},{8,0},{12,4},{1,9},{5,13},{9,1},{13,5},{2,10},{6,14},... | collective-permute-start | bytes 196616 | tf_op jit(solution)/shard_map/ppermute | solution.py:275
  156.7 1.9 %collective-permute-start.6 = (bf16[256,128]{1,0:T(8,128)(2,1)S(1)}, bf16[256,128]{1,0:T(8,128)(2,1)S(1)}, u32[]{:S(2)}, u32[]{:S(2)}) collective-permute-start(bf16[256,128]{1,0:T(8,128)(2,1)S(1)} %get-tuple-element.38), channel_id=1, source_target_pairs={{0,12},{4,0},{8,4},{12,8},{1,13},{5,1},{9,5},{13,9},{2,14},{6,2},{... | collective-permute-start | bytes 196616 | tf_op jit(solution)/shard_map/ppermute | solution.py:275
  158.6 0.0 copy-start
  158.6 0.1 copy.17
  158.8 0.5 copy-done
  159.3 0.1 copy.18.scores
  159.5 0.0 collective-permute-done.4.refs_1_
  159.5 0.0 collective-permute-done.5.refs_2_
  159.5 3.4 %collective-permute-done.6.refs_3_ = bf16[256,128]{1,0:T(8,128)(2,1)S(1)} collective-permute-done((bf16[256,128]{1,0:T(8,128)(2,1)S(1)}, bf16[256,128]{1,0:T(8,128)(2,1)S(1)}, u32[]{:S(2)}, u32[]{:S(2)}) %collective-permute-start.6) | collective-permute-done | bytes 65568 | tf_op jit(solution)/shard_map/ppermute | solution.py:275
  162.9 0.7 shard_map.143
  163.5 0.0 all-to-all-done.3.rows
  163.5 1.1 shard_map.148
Async XLA Ops:
  3.4 31.8 %all-to-all-start = ((bf16[32,22,128]{2,1,0:T(8,128)(2,1)}), bf16[32,22,128]{2,1,0:T(8,128)(2,1)S(1)}, u32[]{:S(2)}, u32[]{:S(2)}) async-start(bf16[32,22,128]{2,1,0:T(8,128)(2,1)} %get-tuple-element.39), calls=%async_computation | async-start | bytes 393216 | tf_op jit(solution)/shard_map/all_to_all | solution.py:362
  49.0 13.2 %collective-permute-start.7 = (bf16[4,704,128]{2,1,0:T(8,128)(2,1)S(1)}, bf16[4,704,128]{2,1,0:T(8,128)(2,1)S(1)}, u32[]{:S(2)}, u32[]{:S(2)}) collective-permute-start(bf16[4,704,128]{2,1,0:T(8,128)(2,1)S(1)} %all_to_all.20.refs_0_), channel_id=1, source_target_pairs={{0,1},{1,0},{2,3},{3,2},{4,5},{5,4},{6,7},{7,6},{8,9},{9,8},{10,11... | collective-permute-start | bytes 2162696 | tf_op jit(solution)/shard_map/ppermute | solution.py:270
  51.4 20.9 %collective-permute-start.8 = (bf16[4,704,128]{2,1,0:T(8,128)(2,1)S(1)}, bf16[4,704,128]{2,1,0:T(8,128)(2,1)S(1)}, u32[]{:S(2)}, u32[]{:S(2)}) collective-permute-start(bf16[4,704,128]{2,1,0:T(8,128)(2,1)S(1)} %all_to_all.20.refs_0_), channel_id=1, source_target_pairs={{0,4},{1,5},{2,6},{3,7},{4,0},{5,1},{6,2},{7,3},{8,12},{9,13},{10,... | collective-permute-start | bytes 2162696 | tf_op jit(solution)/shard_map/ppermute | solution.py:270
  54.2 18.1 %collective-permute-start.9 = (bf16[4,704,128]{2,1,0:T(8,128)(2,1)S(1)}, bf16[4,704,128]{2,1,0:T(8,128)(2,1)S(1)}, u32[]{:S(2)}, u32[]{:S(2)}) collective-permute-start(bf16[4,704,128]{2,1,0:T(8,128)(2,1)S(1)} %all_to_all.20.refs_0_), channel_id=1, source_target_pairs={{0,5},{1,4},{2,7},{3,6},{4,1},{5,0},{6,3},{7,2},{8,13},{9,12},{10,... | collective-permute-start | bytes 2162696 | tf_op jit(solution)/shard_map/ppermute | solution.py:270
  75.1 13.2 %collective-permute-start.10 = (bf16[4,704,128]{2,1,0:T(8,128)(2,1)S(1)}, bf16[4,704,128]{2,1,0:T(8,128)(2,1)S(1)}, u32[]{:S(2)}, u32[]{:S(2)}) collective-permute-start(bf16[4,704,128]{2,1,0:T(8,128)(2,1)S(1)} %get-tuple-element.46), channel_id=1, source_target_pairs={{0,1},{1,0},{2,3},{3,2},{4,5},{5,4},{6,7},{7,6},{8,9},{9,8},{10,11... | collective-permute-start | bytes 2162696 | tf_op jit(solution)/shard_map/ppermute | solution.py:270
  78.5 20.9 %collective-permute-start.11 = (bf16[4,704,128]{2,1,0:T(8,128)(2,1)S(1)}, bf16[4,704,128]{2,1,0:T(8,128)(2,1)S(1)}, u32[]{:S(2)}, u32[]{:S(2)}) collective-permute-start(bf16[4,704,128]{2,1,0:T(8,128)(2,1)S(1)} %get-tuple-element.47), channel_id=1, source_target_pairs={{0,4},{1,5},{2,6},{3,7},{4,0},{5,1},{6,2},{7,3},{8,12},{9,13},{10,... | collective-permute-start | bytes 2162696 | tf_op jit(solution)/shard_map/ppermute | solution.py:270
  80.8 18.5 %collective-permute-start.12 = (bf16[4,704,128]{2,1,0:T(8,128)(2,1)S(1)}, bf16[4,704,128]{2,1,0:T(8,128)(2,1)S(1)}, u32[]{:S(2)}, u32[]{:S(2)}) collective-permute-start(bf16[4,704,128]{2,1,0:T(8,128)(2,1)S(1)} %get-tuple-element.48), channel_id=1, source_target_pairs={{0,5},{1,4},{2,7},{3,6},{4,1},{5,0},{6,3},{7,2},{8,13},{9,12},{10,... | collective-permute-start | bytes 2162696 | tf_op jit(solution)/shard_map/ppermute | solution.py:270
  113.7 49.8 %all-to-all-start.3 = ((bf16[32,22,128]{2,1,0:T(8,128)(2,1)}), bf16[32,22,128]{2,1,0:T(8,128)(2,1)S(1)}, u32[]{:S(2)}, u32[]{:S(2)}) async-start(bf16[32,22,128]{2,1,0:T(8,128)(2,1)} %shard_map.147), calls=%async_computation.3 | async-start | bytes 393216 | tf_op jit(solution)/shard_map/all_to_all | solution.py:433
  120.6 7.6 %collective-permute-start = (f32[2,64]{1,0:T(2,128)S(1)}, f32[2,64]{1,0:T(2,128)S(1)}, u32[]{:S(2)}, u32[]{:S(2)}) collective-permute-start(f32[2,64]{1,0:T(2,128)S(1)} %get-tuple-element.29), channel_id=1, source_target_pairs={{0,16},{16,32},{32,48},{48,64},{64,80},{80,96},{96,112},{112,128},... | collective-permute-start | bytes 1544 | tf_op jit(solution)/shard_map/ppermute | solution.py:21
  128.7 11.6 %collective-permute-start.1 = (bf16[4,256,128]{2,1,0:T(8,128)(2,1)S(1)}, bf16[4,256,128]{2,1,0:T(8,128)(2,1)S(1)}, u32[]{:S(2)}, u32[]{:S(2)}) collective-permute-start(bf16[4,256,128]{2,1,0:T(8,128)(2,1)S(1)} %get-tuple-element.32), channel_id=1, source_target_pairs={{0,1},{1,2},{2,3},{3,0},{4,5},{5,6},{6,7},{7,4},{8,9},{9,10},{10,1... | collective-permute-start | bytes 786440 | tf_op jit(solution)/shard_map/ppermute | solution.py:275
  130.6 16.4 %collective-permute-start.2 = (bf16[4,256,128]{2,1,0:T(8,128)(2,1)S(1)}, bf16[4,256,128]{2,1,0:T(8,128)(2,1)S(1)}, u32[]{:S(2)}, u32[]{:S(2)}) collective-permute-start(bf16[4,256,128]{2,1,0:T(8,128)(2,1)S(1)} %get-tuple-element.33), channel_id=1, source_target_pairs={{0,2},{1,3},{2,0},{3,1},{4,6},{5,7},{6,4},{7,5},{8,10},{9,11},{10,... | collective-permute-start | bytes 786440 | tf_op jit(solution)/shard_map/ppermute | solution.py:275
  136.8 11.6 %collective-permute-start.3 = (bf16[4,256,128]{2,1,0:T(8,128)(2,1)S(1)}, bf16[4,256,128]{2,1,0:T(8,128)(2,1)S(1)}, u32[]{:S(2)}, u32[]{:S(2)}) collective-permute-start(bf16[4,256,128]{2,1,0:T(8,128)(2,1)S(1)} %get-tuple-element.34), channel_id=1, source_target_pairs={{0,3},{1,0},{2,1},{3,2},{4,7},{5,4},{6,5},{7,6},{8,11},{9,8},{10,9... | collective-permute-start | bytes 786440 | tf_op jit(solution)/shard_map/ppermute | solution.py:275
  148.6 10.9 %collective-permute-start.4 = (bf16[256,128]{1,0:T(8,128)(2,1)S(1)}, bf16[256,128]{1,0:T(8,128)(2,1)S(1)}, u32[]{:S(2)}, u32[]{:S(2)}) collective-permute-start(bf16[256,128]{1,0:T(8,128)(2,1)S(1)} %get-tuple-element.36), channel_id=1, source_target_pairs={{0,4},{4,8},{8,12},{12,0},{1,5},{5,9},{9,13},{13,1},{2,6},{6,10},{... | collective-permute-start | bytes 196616 | tf_op jit(solution)/shard_map/ppermute | solution.py:275
  150.5 9.0 %collective-permute-start.5 = (bf16[256,128]{1,0:T(8,128)(2,1)S(1)}, bf16[256,128]{1,0:T(8,128)(2,1)S(1)}, u32[]{:S(2)}, u32[]{:S(2)}) collective-permute-start(bf16[256,128]{1,0:T(8,128)(2,1)S(1)} %get-tuple-element.37), channel_id=1, source_target_pairs={{0,8},{4,12},{8,0},{12,4},{1,9},{5,13},{9,1},{13,5},{2,10},{6,14},... | collective-permute-start | bytes 196616 | tf_op jit(solution)/shard_map/ppermute | solution.py:275
  156.7 6.2 %collective-permute-start.6 = (bf16[256,128]{1,0:T(8,128)(2,1)S(1)}, bf16[256,128]{1,0:T(8,128)(2,1)S(1)}, u32[]{:S(2)}, u32[]{:S(2)}) collective-permute-start(bf16[256,128]{1,0:T(8,128)(2,1)S(1)} %get-tuple-element.38), channel_id=1, source_target_pairs={{0,12},{4,0},{8,4},{12,8},{1,13},{5,1},{9,5},{13,9},{2,14},{6,2},{... | collective-permute-start | bytes 196616 | tf_op jit(solution)/shard_map/ppermute | solution.py:275
  158.6 0.7 copy-start

commit v7 on v6

--- a/solution.py
+++ b/solution.py
@@ -124,7 +124,7 @@
 
 
 def weights_body(order, gate_far, up_far, down_far, gate_w, up_w, down_w, done):
-    count = order.shape[0]
+    count = order.shape[0] // 2
     columns = gate_w.shape[0] // count
     copies = []
     for p in range(count):
@@ -181,9 +181,9 @@
         out[e] = total[e * capacity : (e + 1) * capacity, :].astype(BF16)
 
 
-def mixer_body(place, outer, product_ref, taps, halo, proj, *outs):
-    count = len(outs)
+def mixer_body(order, outer, product_ref, taps, halo, proj, *outs):
     groups, _, columns = outs[0].shape
+    base = order.shape[0] // 2
     product = product_ref[...]
     row = lax.broadcasted_iota(jnp.int32, product.shape, 0)
     last = halo[1:2, :]
@@ -193,23 +193,22 @@
     )
     convolved = taps[0:1, :] * back_two + taps[1:2, :] * back_one + taps[2:3, :] * product
     branch = (outer[...].astype(F32).T * convolved).astype(BF16)
-    for away, out in enumerate(outs):
-        target = lax.rem(place[0] + away, count)
-        for g in range(groups):
-            start = pl.multiple_of((g * count + target) * columns, columns)
-            out[g] = jnp.dot(
+    for flip, out in enumerate(outs):
+        for turn in range(groups):
+            number = order[base + flip * groups + turn]
+            start = pl.multiple_of(number * columns, columns)
+            out[turn] = jnp.dot(
                 branch, proj[:, pl.ds(start, columns)], preferred_element_type=F32
             ).astype(BF16)
 
 
-def regroup_body(place, *refs):
+def regroup_body(*refs):
     half = len(refs) // 2
     parts, outs = refs[:half], refs[half:]
-    for away, out in enumerate(outs):
-        target = lax.rem(place[0] + away, half)
-        total = parts[0][target].astype(F32)
+    for turn, out in enumerate(outs):
+        total = parts[0][turn].astype(F32)
         for part in parts[1:]:
-            total = total + part[target].astype(F32)
+            total = total + part[turn].astype(F32)
         out[...] = total.astype(BF16)
 
 
@@ -254,25 +253,25 @@
                     member = flipped((y, x), (core + 1) % 2, flip)
                     group = next(g for g in squares(core % 2) if member in g)
                     row += [there_y * side + there_x for there_y, there_x in group]
+                for flip in range(4):
+                    member = flipped((y, x), (core + 1) % 2, flip)
+                    for turn in range(4):
+                        there_y, there_x = flipped(member, core, turn)
+                        row.append(there_y * side + there_x)
                 rows.append(row)
     return rows
 
 
-def swapped(block, flip):
+def swapped(block, flip, stage=1):
     names = ("ep",) + TP
     eps, ys, xs = (lax.axis_size(name) for name in names)
     route = []
     for e in range(eps):
         for y in range(ys):
             for x in range(xs):
-                to_y, to_x = flipped((y, x), (e + 1) % 2, flip)
+                to_y, to_x = flipped((y, x), (e + stage) % 2, flip)
                 route.append(((e * ys + y) * xs + x, (e * ys + to_y) * xs + to_x))
     return lax.ppermute(block, names, route)
-
-
-def turned(block, axis, distance):
-    count = lax.axis_size(axis)
-    return lax.ppermute(block, axis, [(i, (i + distance) % count) for i in range(count)])
 
 
 def combine_body(rows, slots, scores, out, padded):
@@ -319,8 +318,11 @@
     stride = (capacity + 7) // 8 * 8
     columns = width // tp_count
     place = lax.axis_index(TP).astype(jnp.int32).reshape(1)
-    place_0 = lax.axis_index(TP[0]).astype(jnp.int32).reshape(1)
-    place_1 = lax.axis_index(TP[1]).astype(jnp.int32).reshape(1)
+    side = lax.axis_size(TP[0])
+    table = jnp.array(arrivals(side), jnp.int32)
+    order = lax.dynamic_index_in_dim(
+        table, (lax.axis_index("ep") % 2) * tp_count + lax.axis_index(TP), keepdims=False
+    )
     groups = lax.axis_size(TP[0])
     turns = lax.axis_size(TP[1])
     seq_len = gate_in.shape[0]
@@ -366,7 +368,7 @@
         (jax.ShapeDtypeStruct((groups, seq_len, columns), BF16),) * turns,
         12 << 20,
         1 << 26,
-        place_1,
+        order,
         outer,
         product,
         taps,
@@ -374,15 +376,11 @@
         proj,
         specs=[SMEM] + [VMEM] * 5,
     )
-    first = [first[0]] + [turned(first[d], TP[1], d) for d in range(1, turns)]
-
-    side = lax.axis_size(TP[0])
+    first = list(first)
+    for flip in (1, 2, 3):
+        first[flip] = swapped(first[flip], flip)
+
     block = (slot_count, columns)
-    table = jnp.array(arrivals(side), jnp.int32)
-    core = lax.axis_index("ep") % 2
-    order = lax.dynamic_index_in_dim(
-        table, core * tp_count + lax.axis_index(TP), keepdims=False
-    )
     own_block = jnp.broadcast_to(arrived.reshape(1, *block), (side, *block))
     own_block, order = lax.optimization_barrier((own_block, order))
     line = crossed(own_block, 0)
@@ -404,7 +402,7 @@
         scratch=[pltpu.SemaphoreType.DMA((3 * tp_count,))],
     )
     parts = call(
-        lambda *refs: expert_body(slot_count // 2, *refs),
+        lambda *refs: expert_body(slot_count, *refs),
         (jax.ShapeDtypeStruct((side, *block), BF16),) * side,
         24 << 20,
         1 << 32,
@@ -437,11 +435,11 @@
         (jax.ShapeDtypeStruct((seq_len, columns), BF16),) * groups,
         12 << 20,
         1 << 22,
-        place_0,
         *first,
-        specs=[SMEM] + [VMEM] * turns,
-    )
-    second = [second[0]] + [turned(second[d], TP[0], d) for d in range(1, groups)]
+    )
+    second = list(second)
+    for flip in (1, 2, 3):
+        second[flip] = swapped(second[flip], flip, 0)
     mixed = call(
         final_body, jax.ShapeDtypeStruct((seq_len, columns), BF16), 8 << 20, 1 << 20, *second
     )

time: 165 us -> 165 us (level)
  the two profiles are of different devices: /device:TPU:64 before, /device:TPU:128 now
where the time goes in v7:
time: 165 us; the launch traced here: 164 us
  starting transfers between devices  65.9 us (40%)
  waiting for transfers between devices  56.7 us (34%)
  blocking collectives  26.8 us (16%)
  Pallas kernels  12.1 us (7%)
    ppermute x12, starting transfers between devices, swapped(): return lax.ppermute(block, names, route)  39.3 us
    ppermute x12, waiting for transfers between devices, swapped(): return lax.ppermute(block, names, route)  36.8 us
    all_to_all x2, blocking collectives, crossed(): lax.all_to_all(block, names, 0, 0, axis_index_groups=groups, tiled=True)  26.8 us
    all_to_all x1, starting transfers between devices, shards(): arrived = lax.all_to_all(sent, 'ep', 0, 0, tiled=True)  14 us
    all_to_all x1, waiting for transfers between devices, shards(): arrived = lax.all_to_all(sent, 'ep', 0, 0, tiled=True)  12.4 us
    pallas_call x9, Pallas kernels, call(): pl.pallas_call(body, out_shape=out, in_specs=specs or [VMEM] * len(operan...  12.1 us
    all_to_all x1, starting transfers between devices, shards(): returned = lax.all_to_all(outputs, 'ep', 0, 0, tiled=True)  10.6 us
    ppermute x1, waiting for transfers between devices, shifted(): return lax.ppermute(block, axis, route)  7.48 us
  transfers between devices with their start and end apart: 15, of which 9 were waited for; matrix products, arithmetic and copies ran while one was open for 1% of the time, Pallas kernels for 3%

profile of v7, /device:TPU:128, one launch (start us, length us, event | category | flops | bytes accessed | tf_op | source)
XLA Modules:
  0.0 164.0 jit_solution(8626441054979780028)
XLA Ops:
  0.6 2.7 %shard_map.140 = (bf16[32,22,128]{2,1,0:T(8,128)(2,1)}, s32[2,256]{1,0:T(2,128)S(1)}, f32[2,64]{1,0:T(2,128)S(1)}, f32[256,64]{1,0:T(8,128)S(1)}, bf16[64,256]{1...) custom-call(s32[1]{0:T(128)} %bitcast.1.refs_0_, bf16[256,2048]{1,0:T(8,128)(2,1)} %refs_1_.1, ...), custom_call_target="tpu_custom_call" | custom-call | flops 268435456 | bytes 1048576 | tf_op jit(solution)/shard_map/pallas_call | solution.py:25
  3.4 14.0 %all-to-all-start = ((bf16[32,22,128]{2,1,0:T(8,128)(2,1)}), bf16[32,22,128]{2,1,0:T(8,128)(2,1)S(1)}, u32[]{:S(2)}, u32[]{:S(2)}) async-start(bf16[32,22,128]{2,1,0:T(8,128)(2,1)} %get-tuple-element.39), calls=%async_computation | async-start | bytes 393216 | tf_op jit(solution)/shard_map/all_to_all | solution.py:364
  17.4 0.7 dynamic-slice_bitcast_fusion.order
  18.1 12.4 %all-to-all-done = bf16[32,22,128]{2,1,0:T(8,128)(2,1)S(1)} async-done(((bf16[32,22,128]{2,1,0:T(8,128)(2,1)}), bf16[32,22,128]{2,1,0:T(8,128)(2,1)S(1)}, u32[]{:S(2)}, u32[]{:S(2)}) %all-to-all-start) | async-done | bytes 180256 | tf_op jit(solution)/shard_map/all_to_all | solution.py:364
  30.5 0.1 broadcast_in_dim.7
  30.6 0.1 broadcast_in_dim.8
  30.7 13.6 %all_to_all.20.refs_0_ = bf16[4,704,128]{2,1,0:T(8,128)(2,1)S(1)} all-to-all(bf16[4,704,128]{2,1,0:T(8,128)(2,1)S(1)} %broadcast_in_dim.8), channel_id=1, replica_groups={{5,6,9,10},{7,4,11,8},{13,14,1,2},{15,12,3,0},{16,17,20,21},{18,19,22,2..., dimensions={0} | all-to-all | bytes 1441792 | tf_op jit(solution)/shard_map/all_to_all | solution.py:236
  44.3 2.4 %collective-permute-start.7 = (bf16[4,704,128]{2,1,0:T(8,128)(2,1)S(1)}, bf16[4,704,128]{2,1,0:T(8,128)(2,1)S(1)}, u32[]{:S(2)}, u32[]{:S(2)}) collective-permute-start(bf16[4,704,128]{2,1,0:T(8,128)(2,1)S(1)} %all_to_all.20.refs_0_), channel_id=1, source_target_pairs={{0,1},{1,0},{2,3},{3,2},{4,5},{5,4},{6,7},{7,6},{8,9},{9,8},{10,11... | collective-permute-start | bytes 2162696 | tf_op jit(solution)/shard_map/ppermute | solution.py:274
  46.7 2.8 %collective-permute-start.8 = (bf16[4,704,128]{2,1,0:T(8,128)(2,1)S(1)}, bf16[4,704,128]{2,1,0:T(8,128)(2,1)S(1)}, u32[]{:S(2)}, u32[]{:S(2)}) collective-permute-start(bf16[4,704,128]{2,1,0:T(8,128)(2,1)S(1)} %all_to_all.20.refs_0_), channel_id=1, source_target_pairs={{0,4},{1,5},{2,6},{3,7},{4,0},{5,1},{6,2},{7,3},{8,12},{9,13},{10,... | collective-permute-start | bytes 2162696 | tf_op jit(solution)/shard_map/ppermute | solution.py:274
  49.5 4.0 %collective-permute-start.9 = (bf16[4,704,128]{2,1,0:T(8,128)(2,1)S(1)}, bf16[4,704,128]{2,1,0:T(8,128)(2,1)S(1)}, u32[]{:S(2)}, u32[]{:S(2)}) collective-permute-start(bf16[4,704,128]{2,1,0:T(8,128)(2,1)S(1)} %all_to_all.20.refs_0_), channel_id=1, source_target_pairs={{0,5},{1,4},{2,7},{3,6},{4,1},{5,0},{6,3},{7,2},{8,13},{9,12},{10,... | collective-permute-start | bytes 2162696 | tf_op jit(solution)/shard_map/ppermute | solution.py:274
  53.5 2.9 %shard_map.144 = (bf16[2048,256]{1,0:T(8,128)(2,1)S(1)}, bf16[2048,256]{1,0:T(8,128)(2,1)S(1)}, bf16[256,2048]{1,0:T(8,128)(2,1)S(1)}) custom-call(s32[32]{0:T(128)S(1)} %dynamic-slice_bitcast_fusion.order, bf16[1,2048,256]{2,1,0:T(8,128)(2,1)} %gate_far.1, bf16[1,2048,256]{2,1,0:T(8,128)(2,1)} %up_far.1, bf16[1,256,2048]{2,1,0:T(8,128)(2,1)} %down_far.1), custom_call_target="tpu_custom_call" | custom-call | flops 4194304 | bytes 1048576 | tf_op jit(solution)/shard_map/pallas_call | solution.py:25
  56.4 1.1 collective-permute-done.7.refs_1_
  57.5 10.2 %collective-permute-done.8.refs_2_ = bf16[4,704,128]{2,1,0:T(8,128)(2,1)S(1)} collective-permute-done((bf16[4,704,128]{2,1,0:T(8,128)(2,1)S(1)}, bf16[4,704,128]{2,1,0:T(8,128)(2,1)S(1)}, u32[]{:S(2)}, u32[]{:S(2)}) %collective-permute-start.8) | collective-permute-done | bytes 720928 | tf_op jit(solution)/shard_map/ppermute | solution.py:274
  67.7 0.0 collective-permute-done.9.refs_3_
  67.7 2.4 %shard_map.145 = (bf16[4,704,128]{2,1,0:T(8,128)(2,1)S(1)}, bf16[4,704,128]{2,1,0:T(8,128)(2,1)S(1)}, bf16[4,704,128]{2,1,0:T(8,128)(2,1)S(1)}, bf16[4,704,128]{2,1,0:T(8,128)(2,1)S(1)}) custom-call(bf16[4,704,128]{2,1,0:T(8,128)(2,1)S(1)} %all_to_all.20.refs_0_, bf16[4,704,128]{2,1,0:T(8,128)(2,1)S(1)} %collective-permute-done.7.refs_1_, ...), custom_call_target="tpu_custom_call" | custom-call | flops 4294967296 | bytes 1048576 | tf_op jit(solution)/shard_map/pallas_call | solution.py:25
  70.1 3.4 %collective-permute-start.10 = (bf16[4,704,128]{2,1,0:T(8,128)(2,1)S(1)}, bf16[4,704,128]{2,1,0:T(8,128)(2,1)S(1)}, u32[]{:S(2)}, u32[]{:S(2)}) collective-permute-start(bf16[4,704,128]{2,1,0:T(8,128)(2,1)S(1)} %get-tuple-element.46), channel_id=1, source_target_pairs={{0,1},{1,0},{2,3},{3,2},{4,5},{5,4},{6,7},{7,6},{8,9},{9,8},{10,11... | collective-permute-start | bytes 2162696 | tf_op jit(solution)/shard_map/ppermute | solution.py:274
  73.5 2.4 %collective-permute-start.11 = (bf16[4,704,128]{2,1,0:T(8,128)(2,1)S(1)}, bf16[4,704,128]{2,1,0:T(8,128)(2,1)S(1)}, u32[]{:S(2)}, u32[]{:S(2)}) collective-permute-start(bf16[4,704,128]{2,1,0:T(8,128)(2,1)S(1)} %get-tuple-element.47), channel_id=1, source_target_pairs={{0,4},{1,5},{2,6},{3,7},{4,0},{5,1},{6,2},{7,3},{8,12},{9,13},{10,... | collective-permute-start | bytes 2162696 | tf_op jit(solution)/shard_map/ppermute | solution.py:274
  75.8 3.5 %collective-permute-start.12 = (bf16[4,704,128]{2,1,0:T(8,128)(2,1)S(1)}, bf16[4,704,128]{2,1,0:T(8,128)(2,1)S(1)}, u32[]{:S(2)}, u32[]{:S(2)}) collective-permute-start(bf16[4,704,128]{2,1,0:T(8,128)(2,1)S(1)} %get-tuple-element.48), channel_id=1, source_target_pairs={{0,5},{1,4},{2,7},{3,6},{4,1},{5,0},{6,3},{7,2},{8,13},{9,12},{10,... | collective-permute-start | bytes 2162696 | tf_op jit(solution)/shard_map/ppermute | solution.py:274
  79.3 3.9 %collective-permute-done.10.refs_1_ = bf16[4,704,128]{2,1,0:T(8,128)(2,1)S(1)} collective-permute-done((bf16[4,704,128]{2,1,0:T(8,128)(2,1)S(1)}, bf16[4,704,128]{2,1,0:T(8,128)(2,1)S(1)}, u32[]{:S(2)}, u32[]{:S(2)}) %collective-permute-start.10) | collective-permute-done | bytes 720928 | tf_op jit(solution)/shard_map/ppermute | solution.py:274
  83.3 11.1 %collective-permute-done.11.refs_2_ = bf16[4,704,128]{2,1,0:T(8,128)(2,1)S(1)} collective-permute-done((bf16[4,704,128]{2,1,0:T(8,128)(2,1)S(1)}, bf16[4,704,128]{2,1,0:T(8,128)(2,1)S(1)}, u32[]{:S(2)}, u32[]{:S(2)}) %collective-permute-start.11) | collective-permute-done | bytes 720928 | tf_op jit(solution)/shard_map/ppermute | solution.py:274
  94.4 0.0 collective-permute-done.12.refs_3_
  94.4 0.4 shard_map.146
  94.7 13.2 %all_to_all.21.parts = bf16[4,704,128]{2,1,0:T(8,128)(2,1)S(1)} all-to-all(bf16[4,704,128]{2,1,0:T(8,128)(2,1)S(1)} %shard_map.146), channel_id=1, replica_groups={{5,6,9,10},{7,4,11,8},{13,14,1,2},{15,12,3,0},{16,17,20,21},{18,19,22,2..., dimensions={0} | all-to-all | bytes 1441792 | tf_op jit(solution)/shard_map/all_to_all | solution.py:236
  107.9 0.8 shard_map.147
  108.7 10.6 %all-to-all-start.3 = ((bf16[32,22,128]{2,1,0:T(8,128)(2,1)}), bf16[32,22,128]{2,1,0:T(8,128)(2,1)S(1)}, u32[]{:S(2)}, u32[]{:S(2)}) async-start(bf16[32,22,128]{2,1,0:T(8,128)(2,1)} %shard_map.147), calls=%async_computation.3 | async-start | bytes 393216 | tf_op jit(solution)/shard_map/all_to_all | solution.py:431
  119.4 2.0 %collective-permute-start = (f32[2,64]{1,0:T(2,128)S(1)}, f32[2,64]{1,0:T(2,128)S(1)}, u32[]{:S(2)}, u32[]{:S(2)}) collective-permute-start(f32[2,64]{1,0:T(2,128)S(1)} %get-tuple-element.29), channel_id=1, source_target_pairs={{0,16},{16,32},{32,48},{48,64},{64,80},{80,96},{96,112},{112,128},... | collective-permute-start | bytes 1544 | tf_op jit(solution)/shard_map/ppermute | solution.py:21
  121.4 7.5 %collective-permute-done.halo = f32[2,64]{1,0:T(2,128)S(1)} collective-permute-done((f32[2,64]{1,0:T(2,128)S(1)}, f32[2,64]{1,0:T(2,128)S(1)}, u32[]{:S(2)}, u32[]{:S(2)}) %collective-permute-start) | collective-permute-done | bytes 544 | tf_op jit(solution)/shard_map/ppermute | solution.py:21
  128.9 1.0 shard_map.141
  129.9 1.9 %collective-permute-start.1 = (bf16[4,256,128]{2,1,0:T(8,128)(2,1)S(1)}, bf16[4,256,128]{2,1,0:T(8,128)(2,1)S(1)}, u32[]{:S(2)}, u32[]{:S(2)}) collective-permute-start(bf16[4,256,128]{2,1,0:T(8,128)(2,1)S(1)} %get-tuple-element.32), channel_id=1, source_target_pairs={{0,1},{1,0},{2,3},{3,2},{4,5},{5,4},{6,7},{7,6},{8,9},{9,8},{10,11... | collective-permute-start | bytes 786440 | tf_op jit(solution)/shard_map/ppermute | solution.py:274
  131.9 1.9 %collective-permute-start.2 = (bf16[4,256,128]{2,1,0:T(8,128)(2,1)S(1)}, bf16[4,256,128]{2,1,0:T(8,128)(2,1)S(1)}, u32[]{:S(2)}, u32[]{:S(2)}) collective-permute-start(bf16[4,256,128]{2,1,0:T(8,128)(2,1)S(1)} %get-tuple-element.33), channel_id=1, source_target_pairs={{0,4},{1,5},{2,6},{3,7},{4,0},{5,1},{6,2},{7,3},{8,12},{9,13},{10,... | collective-permute-start | bytes 786440 | tf_op jit(solution)/shard_map/ppermute | solution.py:274
  133.8 5.4 %collective-permute-start.3 = (bf16[4,256,128]{2,1,0:T(8,128)(2,1)S(1)}, bf16[4,256,128]{2,1,0:T(8,128)(2,1)S(1)}, u32[]{:S(2)}, u32[]{:S(2)}) collective-permute-start(bf16[4,256,128]{2,1,0:T(8,128)(2,1)S(1)} %get-tuple-element.34), channel_id=1, source_target_pairs={{0,5},{1,4},{2,7},{3,6},{4,1},{5,0},{6,3},{7,2},{8,13},{9,12},{10,... | collective-permute-start | bytes 786440 | tf_op jit(solution)/shard_map/ppermute | solution.py:274
  139.2 0.0 collective-permute-done.1.refs_1_
  139.2 0.9 collective-permute-done.2.refs_2_
  140.1 3.4 %collective-permute-done.3.refs_3_ = bf16[4,256,128]{2,1,0:T(8,128)(2,1)S(1)} collective-permute-done((bf16[4,256,128]{2,1,0:T(8,128)(2,1)S(1)}, bf16[4,256,128]{2,1,0:T(8,128)(2,1)S(1)}, u32[]{:S(2)}, u32[]{:S(2)}) %collective-permute-start.3) | collective-permute-done | bytes 262176 | tf_op jit(solution)/shard_map/ppermute | solution.py:274
  143.5 0.1 shard_map.142
  143.6 4.8 %collective-permute-start.4 = (bf16[256,128]{1,0:T(8,128)(2,1)S(1)}, bf16[256,128]{1,0:T(8,128)(2,1)S(1)}, u32[]{:S(2)}, u32[]{:S(2)}) collective-permute-start(bf16[256,128]{1,0:T(8,128)(2,1)S(1)} %get-tuple-element.36), channel_id=1, source_target_pairs={{0,3},{1,2},{2,1},{3,0},{4,7},{5,6},{6,5},{7,4},{8,11},{9,10},{10,... | collective-permute-start | bytes 196616 | tf_op jit(solution)/shard_map/ppermute | solution.py:274
  148.4 4.4 %collective-permute-start.5 = (bf16[256,128]{1,0:T(8,128)(2,1)S(1)}, bf16[256,128]{1,0:T(8,128)(2,1)S(1)}, u32[]{:S(2)}, u32[]{:S(2)}) collective-permute-start(bf16[256,128]{1,0:T(8,128)(2,1)S(1)} %get-tuple-element.37), channel_id=1, source_target_pairs={{0,12},{1,13},{2,14},{3,15},{4,8},{5,9},{6,10},{7,11},{8,4},{9,5},... | collective-permute-start | bytes 196616 | tf_op jit(solution)/shard_map/ppermute | solution.py:274
  152.8 2.5 %collective-permute-start.6 = (bf16[256,128]{1,0:T(8,128)(2,1)S(1)}, bf16[256,128]{1,0:T(8,128)(2,1)S(1)}, u32[]{:S(2)}, u32[]{:S(2)}) collective-permute-start(bf16[256,128]{1,0:T(8,128)(2,1)S(1)} %get-tuple-element.38), channel_id=1, source_target_pairs={{0,15},{1,14},{2,13},{3,12},{4,11},{5,10},{6,9},{7,8},{8,7},{9,6},... | collective-permute-start | bytes 196616 | tf_op jit(solution)/shard_map/ppermute | solution.py:274
  155.3 0.0 copy-start
  155.3 0.1 copy.17
  155.5 0.5 copy-done
  156.0 0.1 copy.18.scores
  156.1 0.0 collective-permute-done.4.refs_1_
  156.1 0.0 collective-permute-done.5.refs_2_
  156.1 6.2 %collective-permute-done.6.refs_3_ = bf16[256,128]{1,0:T(8,128)(2,1)S(1)} collective-permute-done((bf16[256,128]{1,0:T(8,128)(2,1)S(1)}, bf16[256,128]{1,0:T(8,128)(2,1)S(1)}, u32[]{:S(2)}, u32[]{:S(2)}) %collective-permute-start.6) | collective-permute-done | bytes 65568 | tf_op jit(solution)/shard_map/ppermute | solution.py:274
  162.3 0.7 shard_map.143
  163.0 0.0 all-to-all-done.3.rows
  163.0 1.1 shard_map.148
Async XLA Ops:
  3.4 27.2 %all-to-all-start = ((bf16[32,22,128]{2,1,0:T(8,128)(2,1)}), bf16[32,22,128]{2,1,0:T(8,128)(2,1)S(1)}, u32[]{:S(2)}, u32[]{:S(2)}) async-start(bf16[32,22,128]{2,1,0:T(8,128)(2,1)} %get-tuple-element.39), calls=%async_computation | async-start | bytes 393216 | tf_op jit(solution)/shard_map/all_to_all | solution.py:364
  44.3 13.2 %collective-permute-start.7 = (bf16[4,704,128]{2,1,0:T(8,128)(2,1)S(1)}, bf16[4,704,128]{2,1,0:T(8,128)(2,1)S(1)}, u32[]{:S(2)}, u32[]{:S(2)}) collective-permute-start(bf16[4,704,128]{2,1,0:T(8,128)(2,1)S(1)} %all_to_all.20.refs_0_), channel_id=1, source_target_pairs={{0,1},{1,0},{2,3},{3,2},{4,5},{5,4},{6,7},{7,6},{8,9},{9,8},{10,11... | collective-permute-start | bytes 2162696 | tf_op jit(solution)/shard_map/ppermute | solution.py:274
  46.7 20.9 %collective-permute-start.8 = (bf16[4,704,128]{2,1,0:T(8,128)(2,1)S(1)}, bf16[4,704,128]{2,1,0:T(8,128)(2,1)S(1)}, u32[]{:S(2)}, u32[]{:S(2)}) collective-permute-start(bf16[4,704,128]{2,1,0:T(8,128)(2,1)S(1)} %all_to_all.20.refs_0_), channel_id=1, source_target_pairs={{0,4},{1,5},{2,6},{3,7},{4,0},{5,1},{6,2},{7,3},{8,12},{9,13},{10,... | collective-permute-start | bytes 2162696 | tf_op jit(solution)/shard_map/ppermute | solution.py:274
  49.5 18.1 %collective-permute-start.9 = (bf16[4,704,128]{2,1,0:T(8,128)(2,1)S(1)}, bf16[4,704,128]{2,1,0:T(8,128)(2,1)S(1)}, u32[]{:S(2)}, u32[]{:S(2)}) collective-permute-start(bf16[4,704,128]{2,1,0:T(8,128)(2,1)S(1)} %all_to_all.20.refs_0_), channel_id=1, source_target_pairs={{0,5},{1,4},{2,7},{3,6},{4,1},{5,0},{6,3},{7,2},{8,13},{9,12},{10,... | collective-permute-start | bytes 2162696 | tf_op jit(solution)/shard_map/ppermute | solution.py:274
  70.1 13.2 %collective-permute-start.10 = (bf16[4,704,128]{2,1,0:T(8,128)(2,1)S(1)}, bf16[4,704,128]{2,1,0:T(8,128)(2,1)S(1)}, u32[]{:S(2)}, u32[]{:S(2)}) collective-permute-start(bf16[4,704,128]{2,1,0:T(8,128)(2,1)S(1)} %get-tuple-element.46), channel_id=1, source_target_pairs={{0,1},{1,0},{2,3},{3,2},{4,5},{5,4},{6,7},{7,6},{8,9},{9,8},{10,11... | collective-permute-start | bytes 2162696 | tf_op jit(solution)/shard_map/ppermute | solution.py:274
  73.5 20.9 %collective-permute-start.11 = (bf16[4,704,128]{2,1,0:T(8,128)(2,1)S(1)}, bf16[4,704,128]{2,1,0:T(8,128)(2,1)S(1)}, u32[]{:S(2)}, u32[]{:S(2)}) collective-permute-start(bf16[4,704,128]{2,1,0:T(8,128)(2,1)S(1)} %get-tuple-element.47), channel_id=1, source_target_pairs={{0,4},{1,5},{2,6},{3,7},{4,0},{5,1},{6,2},{7,3},{8,12},{9,13},{10,... | collective-permute-start | bytes 2162696 | tf_op jit(solution)/shard_map/ppermute | solution.py:274
  75.8 18.5 %collective-permute-start.12 = (bf16[4,704,128]{2,1,0:T(8,128)(2,1)S(1)}, bf16[4,704,128]{2,1,0:T(8,128)(2,1)S(1)}, u32[]{:S(2)}, u32[]{:S(2)}) collective-permute-start(bf16[4,704,128]{2,1,0:T(8,128)(2,1)S(1)} %get-tuple-element.48), channel_id=1, source_target_pairs={{0,5},{1,4},{2,7},{3,6},{4,1},{5,0},{6,3},{7,2},{8,13},{9,12},{10,... | collective-permute-start | bytes 2162696 | tf_op jit(solution)/shard_map/ppermute | solution.py:274
  108.7 54.3 %all-to-all-start.3 = ((bf16[32,22,128]{2,1,0:T(8,128)(2,1)}), bf16[32,22,128]{2,1,0:T(8,128)(2,1)S(1)}, u32[]{:S(2)}, u32[]{:S(2)}) async-start(bf16[32,22,128]{2,1,0:T(8,128)(2,1)} %shard_map.147), calls=%async_computation.3 | async-start | bytes 393216 | tf_op jit(solution)/shard_map/all_to_all | solution.py:431
  119.4 9.5 %collective-permute-start = (f32[2,64]{1,0:T(2,128)S(1)}, f32[2,64]{1,0:T(2,128)S(1)}, u32[]{:S(2)}, u32[]{:S(2)}) collective-permute-start(f32[2,64]{1,0:T(2,128)S(1)} %get-tuple-element.29), channel_id=1, source_target_pairs={{0,16},{16,32},{32,48},{48,64},{64,80},{80,96},{96,112},{112,128},... | collective-permute-start | bytes 1544 | tf_op jit(solution)/shard_map/ppermute | solution.py:21
  129.9 9.2 %collective-permute-start.1 = (bf16[4,256,128]{2,1,0:T(8,128)(2,1)S(1)}, bf16[4,256,128]{2,1,0:T(8,128)(2,1)S(1)}, u32[]{:S(2)}, u32[]{:S(2)}) collective-permute-start(bf16[4,256,128]{2,1,0:T(8,128)(2,1)S(1)} %get-tuple-element.32), channel_id=1, source_target_pairs={{0,1},{1,0},{2,3},{3,2},{4,5},{5,4},{6,7},{7,6},{8,9},{9,8},{10,11... | collective-permute-start | bytes 786440 | tf_op jit(solution)/shard_map/ppermute | solution.py:274
  131.9 8.3 %collective-permute-start.2 = (bf16[4,256,128]{2,1,0:T(8,128)(2,1)S(1)}, bf16[4,256,128]{2,1,0:T(8,128)(2,1)S(1)}, u32[]{:S(2)}, u32[]{:S(2)}) collective-permute-start(bf16[4,256,128]{2,1,0:T(8,128)(2,1)S(1)} %get-tuple-element.33), channel_id=1, source_target_pairs={{0,4},{1,5},{2,6},{3,7},{4,0},{5,1},{6,2},{7,3},{8,12},{9,13},{10,... | collective-permute-start | bytes 786440 | tf_op jit(solution)/shard_map/ppermute | solution.py:274
  133.8 9.7 %collective-permute-start.3 = (bf16[4,256,128]{2,1,0:T(8,128)(2,1)S(1)}, bf16[4,256,128]{2,1,0:T(8,128)(2,1)S(1)}, u32[]{:S(2)}, u32[]{:S(2)}) collective-permute-start(bf16[4,256,128]{2,1,0:T(8,128)(2,1)S(1)} %get-tuple-element.34), channel_id=1, source_target_pairs={{0,5},{1,4},{2,7},{3,6},{4,1},{5,0},{6,3},{7,2},{8,13},{9,12},{10,... | collective-permute-start | bytes 786440 | tf_op jit(solution)/shard_map/ppermute | solution.py:274
  143.6 12.5 %collective-permute-start.4 = (bf16[256,128]{1,0:T(8,128)(2,1)S(1)}, bf16[256,128]{1,0:T(8,128)(2,1)S(1)}, u32[]{:S(2)}, u32[]{:S(2)}) collective-permute-start(bf16[256,128]{1,0:T(8,128)(2,1)S(1)} %get-tuple-element.36), channel_id=1, source_target_pairs={{0,3},{1,2},{2,1},{3,0},{4,7},{5,6},{6,5},{7,4},{8,11},{9,10},{10,... | collective-permute-start | bytes 196616 | tf_op jit(solution)/shard_map/ppermute | solution.py:274
  148.4 7.7 %collective-permute-start.5 = (bf16[256,128]{1,0:T(8,128)(2,1)S(1)}, bf16[256,128]{1,0:T(8,128)(2,1)S(1)}, u32[]{:S(2)}, u32[]{:S(2)}) collective-permute-start(bf16[256,128]{1,0:T(8,128)(2,1)S(1)} %get-tuple-element.37), channel_id=1, source_target_pairs={{0,12},{1,13},{2,14},{3,15},{4,8},{5,9},{6,10},{7,11},{8,4},{9,5},... | collective-permute-start | bytes 196616 | tf_op jit(solution)/shard_map/ppermute | solution.py:274
  152.8 9.5 %collective-permute-start.6 = (bf16[256,128]{1,0:T(8,128)(2,1)S(1)}, bf16[256,128]{1,0:T(8,128)(2,1)S(1)}, u32[]{:S(2)}, u32[]{:S(2)}) collective-permute-start(bf16[256,128]{1,0:T(8,128)(2,1)S(1)} %get-tuple-element.38), channel_id=1, source_target_pairs={{0,15},{1,14},{2,13},{3,12},{4,11},{5,10},{6,9},{7,8},{8,7},{9,6},... | collective-permute-start | bytes 196616 | tf_op jit(solution)/shard_map/ppermute | solution.py:274
  155.3 0.7 copy-start

commit v8 on v7

--- a/solution.py
+++ b/solution.py
@@ -143,25 +143,29 @@
         copy.wait()
 
 
-def expert_body(step, *refs):
-    sides = (len(refs) - 3) // 2
-    tokens, outs = refs[:sides], refs[sides + 3 :]
-    gate_w, up_w, down_w = refs[sides : sides + 3]
-    blocks, rows, columns = tokens[0].shape
-    spots = [(n, m) for n in range(sides) for m in range(blocks)]
-
-    def tile(number, carry):
-        at = pl.ds(pl.multiple_of(number * step, step), step)
-        left = jnp.concatenate([tokens[n][m, at, :] for n, m in spots], axis=1)
-        gate = jnp.dot(left, gate_w[...], preferred_element_type=F32)
-        up = jnp.dot(left, up_w[...], preferred_element_type=F32)
-        hidden = (gate / (1.0 + jnp.exp(-gate)) * up).astype(BF16)
-        part = jnp.dot(hidden, down_w[...], preferred_element_type=F32).astype(BF16)
-        for p, (n, m) in enumerate(spots):
-            outs[n][m, at, :] = part[:, p * columns : (p + 1) * columns]
-        return carry
-
-    lax.fori_loop(0, rows // step, tile, 0)
+def expert_body(*refs):
+    sides = len(refs) - 6
+    tokens = refs[:sides]
+    gate_w, up_w, down_w, hidden_out = refs[sides : sides + 4]
+    outs = refs[sides + 4 :]
+    blocks, _, columns = tokens[0].shape
+    left = jnp.concatenate([t[m] for t in tokens for m in range(blocks)], axis=1)
+    gate = jnp.dot(left, gate_w[...], preferred_element_type=F32)
+    up = jnp.dot(left, up_w[...], preferred_element_type=F32)
+    hidden = (gate / (1.0 + jnp.exp(-gate)) * up).astype(BF16)
+    hidden_out[...] = hidden
+    first = (sides - len(outs)) * blocks * columns
+    part = jnp.dot(hidden, down_w[:, first:], preferred_element_type=F32).astype(BF16)
+    for p in range(len(outs) * blocks):
+        outs[p // blocks][p % blocks] = part[:, p * columns : (p + 1) * columns]
+
+
+def rest_body(hidden, down_w, *outs):
+    blocks, _, columns = outs[0].shape
+    width = len(outs) * blocks * columns
+    part = jnp.dot(hidden[...], down_w[:, :width], preferred_element_type=F32).astype(BF16)
+    for p in range(len(outs) * blocks):
+        outs[p // blocks][p % blocks] = part[:, p * columns : (p + 1) * columns]
 
 
 def fold_body(*refs):
@@ -401,15 +405,24 @@
         specs=[SMEM, HBM, HBM, HBM],
         scratch=[pltpu.SemaphoreType.DMA((3 * tp_count,))],
     )
-    parts = call(
-        lambda *refs: expert_body(slot_count, *refs),
-        (jax.ShapeDtypeStruct((side, *block), BF16),) * side,
+    hidden, *last = call(
+        expert_body,
+        (jax.ShapeDtypeStruct((slot_count, gate_proj.shape[2]), BF16),)
+        + (jax.ShapeDtypeStruct((side, *block), BF16),) * 2,
         24 << 20,
-        1 << 32,
+        1 << 31,
         *lines,
         *weights,
     )
-    parts = list(parts)
+    parts = call(
+        rest_body,
+        (jax.ShapeDtypeStruct((side, *block), BF16),) * 2,
+        24 << 20,
+        1 << 29,
+        hidden,
+        weights[2],
+    )
+    parts = list(parts) + list(last)
     for flip in (1, 2, 3):
         parts[flip] = swapped(parts[flip], flip)
     line = call(

time: 165 us -> 165 us (level)
    pallas_call x9 -> x10, Pallas kernels: 12.1 us -> 12.2 us  [call(): pl.pallas_call(body, out_shape=out, in_specs=specs or [VMEM] * len(operan...]
where the time goes in v8:
time: 165 us; the launch traced here: 164 us
  starting transfers between devices  65.9 us (40%)
  waiting for transfers between devices  56.7 us (34%)
  blocking collectives  26.8 us (16%)
  Pallas kernels  12.2 us (7%)
    ppermute x12, starting transfers between devices, swapped(): return lax.ppermute(block, names, route)  39.3 us
    ppermute x12, waiting for transfers between devices, swapped(): return lax.ppermute(block, names, route)  36.8 us
    all_to_all x2, blocking collectives, crossed(): lax.all_to_all(block, names, 0, 0, axis_index_groups=groups, tiled=True)  26.8 us
    all_to_all x1, starting transfers between devices, shards(): arrived = lax.all_to_all(sent, 'ep', 0, 0, tiled=True)  14 us
    all_to_all x1, waiting for transfers between devices, shards(): arrived = lax.all_to_all(sent, 'ep', 0, 0, tiled=True)  12.4 us
    pallas_call x10, Pallas kernels, call(): pl.pallas_call(body, out_shape=out, in_specs=specs or [VMEM] * len(operan...  12.2 us
    all_to_all x1, starting transfers between devices, shards(): returned = lax.all_to_all(outputs, 'ep', 0, 0, tiled=True)  10.6 us
    ppermute x1, waiting for transfers between devices, shifted(): return lax.ppermute(block, axis, route)  7.48 us
  transfers between devices with their start and end apart: 15, of which 9 were waited for; matrix products, arithmetic and copies ran while one was open for 1% of the time, Pallas kernels for 3%

profile of v8, /device:TPU:128, one launch (start us, length us, event | category | flops | bytes accessed | tf_op | source)
XLA Modules:
  0.0 164.2 jit_solution(14581228482344614580)
XLA Ops:
  0.6 2.7 %shard_map.140 = (bf16[32,22,128]{2,1,0:T(8,128)(2,1)}, s32[2,256]{1,0:T(2,128)S(1)}, f32[2,64]{1,0:T(2,128)S(1)}, f32[256,64]{1,0:T(8,128)S(1)}, bf16[64,256]{1...) custom-call(s32[1]{0:T(128)} %bitcast.1.refs_0_, bf16[256,2048]{1,0:T(8,128)(2,1)} %refs_1_.1, ...), custom_call_target="tpu_custom_call" | custom-call | flops 268435456 | bytes 1048576 | tf_op jit(solution)/shard_map/pallas_call | solution.py:25
  3.4 14.0 %all-to-all-start = ((bf16[32,22,128]{2,1,0:T(8,128)(2,1)}), bf16[32,22,128]{2,1,0:T(8,128)(2,1)S(1)}, u32[]{:S(2)}, u32[]{:S(2)}) async-start(bf16[32,22,128]{2,1,0:T(8,128)(2,1)} %get-tuple-element.40), calls=%async_computation | async-start | bytes 393216 | tf_op jit(solution)/shard_map/all_to_all | solution.py:368
  17.4 0.7 dynamic-slice_bitcast_fusion.order
  18.1 12.4 %all-to-all-done = bf16[32,22,128]{2,1,0:T(8,128)(2,1)S(1)} async-done(((bf16[32,22,128]{2,1,0:T(8,128)(2,1)}), bf16[32,22,128]{2,1,0:T(8,128)(2,1)S(1)}, u32[]{:S(2)}, u32[]{:S(2)}) %all-to-all-start) | async-done | bytes 180256 | tf_op jit(solution)/shard_map/all_to_all | solution.py:368
  30.5 0.1 broadcast_in_dim.7
  30.6 0.1 broadcast_in_dim.8
  30.7 13.6 %all_to_all.20.refs_0_ = bf16[4,704,128]{2,1,0:T(8,128)(2,1)S(1)} all-to-all(bf16[4,704,128]{2,1,0:T(8,128)(2,1)S(1)} %broadcast_in_dim.8), channel_id=1, replica_groups={{5,6,9,10},{7,4,11,8},{13,14,1,2},{15,12,3,0},{16,17,20,21},{18,19,22,2..., dimensions={0} | all-to-all | bytes 1441792 | tf_op jit(solution)/shard_map/all_to_all | solution.py:240
  44.3 2.4 %collective-permute-start.7 = (bf16[4,704,128]{2,1,0:T(8,128)(2,1)S(1)}, bf16[4,704,128]{2,1,0:T(8,128)(2,1)S(1)}, u32[]{:S(2)}, u32[]{:S(2)}) collective-permute-start(bf16[4,704,128]{2,1,0:T(8,128)(2,1)S(1)} %all_to_all.20.refs_0_), channel_id=1, source_target_pairs={{0,1},{1,0},{2,3},{3,2},{4,5},{5,4},{6,7},{7,6},{8,9},{9,8},{10,11... | collective-permute-start | bytes 2162696 | tf_op jit(solution)/shard_map/ppermute | solution.py:278
  46.7 2.8 %collective-permute-start.8 = (bf16[4,704,128]{2,1,0:T(8,128)(2,1)S(1)}, bf16[4,704,128]{2,1,0:T(8,128)(2,1)S(1)}, u32[]{:S(2)}, u32[]{:S(2)}) collective-permute-start(bf16[4,704,128]{2,1,0:T(8,128)(2,1)S(1)} %all_to_all.20.refs_0_), channel_id=1, source_target_pairs={{0,4},{1,5},{2,6},{3,7},{4,0},{5,1},{6,2},{7,3},{8,12},{9,13},{10,... | collective-permute-start | bytes 2162696 | tf_op jit(solution)/shard_map/ppermute | solution.py:278
  49.5 4.0 %collective-permute-start.9 = (bf16[4,704,128]{2,1,0:T(8,128)(2,1)S(1)}, bf16[4,704,128]{2,1,0:T(8,128)(2,1)S(1)}, u32[]{:S(2)}, u32[]{:S(2)}) collective-permute-start(bf16[4,704,128]{2,1,0:T(8,128)(2,1)S(1)} %all_to_all.20.refs_0_), channel_id=1, source_target_pairs={{0,5},{1,4},{2,7},{3,6},{4,1},{5,0},{6,3},{7,2},{8,13},{9,12},{10,... | collective-permute-start | bytes 2162696 | tf_op jit(solution)/shard_map/ppermute | solution.py:278
  53.5 2.9 %shard_map.144 = (bf16[2048,256]{1,0:T(8,128)(2,1)S(1)}, bf16[2048,256]{1,0:T(8,128)(2,1)S(1)}, bf16[256,2048]{1,0:T(8,128)(2,1)S(1)}) custom-call(s32[32]{0:T(128)S(1)} %dynamic-slice_bitcast_fusion.order, bf16[1,2048,256]{2,1,0:T(8,128)(2,1)} %gate_far.1, bf16[1,2048,256]{2,1,0:T(8,128)(2,1)} %up_far.1, bf16[1,256,2048]{2,1,0:T(8,128)(2,1)} %down_far.1), custom_call_target="tpu_custom_call" | custom-call | flops 4194304 | bytes 1048576 | tf_op jit(solution)/shard_map/pallas_call | solution.py:25
  56.4 1.1 collective-permute-done.7.refs_1_
  57.5 10.2 %collective-permute-done.8.refs_2_ = bf16[4,704,128]{2,1,0:T(8,128)(2,1)S(1)} collective-permute-done((bf16[4,704,128]{2,1,0:T(8,128)(2,1)S(1)}, bf16[4,704,128]{2,1,0:T(8,128)(2,1)S(1)}, u32[]{:S(2)}, u32[]{:S(2)}) %collective-permute-start.8) | collective-permute-done | bytes 720928 | tf_op jit(solution)/shard_map/ppermute | solution.py:278
  67.7 0.0 collective-permute-done.9.refs_3_
  67.7 2.0 %shard_map.145 = (bf16[704,256]{1,0:T(8,128)(2,1)S(1)}, bf16[4,704,128]{2,1,0:T(8,128)(2,1)S(1)}, bf16[4,704,128]{2,1,0:T(8,128)(2,1)S(1)}) custom-call(bf16[4,704,128]{2,1,0:T(8,128)(2,1)S(1)} %all_to_all.20.refs_0_, bf16[4,704,128]{2,1,0:T(8,128)(2,1)S(1)} %collective-permute-done.7.refs_1_, bf16[4,704,128]{2,1,0:T(8,128)(2,1)S(1)} %collective-permute-done.8.refs_2_, ...), custom_call_target="tpu_custom_call" | custom-call | flops 2147483648 | bytes 1048576 | tf_op jit(solution)/shard_map/pallas_call | solution.py:25
  69.7 0.5 shard_map.146
  70.2 3.4 %collective-permute-start.10 = (bf16[4,704,128]{2,1,0:T(8,128)(2,1)S(1)}, bf16[4,704,128]{2,1,0:T(8,128)(2,1)S(1)}, u32[]{:S(2)}, u32[]{:S(2)}) collective-permute-start(bf16[4,704,128]{2,1,0:T(8,128)(2,1)S(1)} %get-tuple-element.48), channel_id=1, source_target_pairs={{0,1},{1,0},{2,3},{3,2},{4,5},{5,4},{6,7},{7,6},{8,9},{9,8},{10,11... | collective-permute-start | bytes 2162696 | tf_op jit(solution)/shard_map/ppermute | solution.py:278
  73.6 2.4 %collective-permute-start.11 = (bf16[4,704,128]{2,1,0:T(8,128)(2,1)S(1)}, bf16[4,704,128]{2,1,0:T(8,128)(2,1)S(1)}, u32[]{:S(2)}, u32[]{:S(2)}) collective-permute-start(bf16[4,704,128]{2,1,0:T(8,128)(2,1)S(1)} %get-tuple-element.49), channel_id=1, source_target_pairs={{0,4},{1,5},{2,6},{3,7},{4,0},{5,1},{6,2},{7,3},{8,12},{9,13},{10,... | collective-permute-start | bytes 2162696 | tf_op jit(solution)/shard_map/ppermute | solution.py:278
  76.0 3.5 %collective-permute-start.12 = (bf16[4,704,128]{2,1,0:T(8,128)(2,1)S(1)}, bf16[4,704,128]{2,1,0:T(8,128)(2,1)S(1)}, u32[]{:S(2)}, u32[]{:S(2)}) collective-permute-start(bf16[4,704,128]{2,1,0:T(8,128)(2,1)S(1)} %get-tuple-element.50), channel_id=1, source_target_pairs={{0,5},{1,4},{2,7},{3,6},{4,1},{5,0},{6,3},{7,2},{8,13},{9,12},{10,... | collective-permute-start | bytes 2162696 | tf_op jit(solution)/shard_map/ppermute | solution.py:278
  79.5 3.9 %collective-permute-done.10.refs_1_ = bf16[4,704,128]{2,1,0:T(8,128)(2,1)S(1)} collective-permute-done((bf16[4,704,128]{2,1,0:T(8,128)(2,1)S(1)}, bf16[4,704,128]{2,1,0:T(8,128)(2,1)S(1)}, u32[]{:S(2)}, u32[]{:S(2)}) %collective-permute-start.10) | collective-permute-done | bytes 720928 | tf_op jit(solution)/shard_map/ppermute | solution.py:278
  83.4 11.1 %collective-permute-done.11.refs_2_ = bf16[4,704,128]{2,1,0:T(8,128)(2,1)S(1)} collective-permute-done((bf16[4,704,128]{2,1,0:T(8,128)(2,1)S(1)}, bf16[4,704,128]{2,1,0:T(8,128)(2,1)S(1)}, u32[]{:S(2)}, u32[]{:S(2)}) %collective-permute-start.11) | collective-permute-done | bytes 720928 | tf_op jit(solution)/shard_map/ppermute | solution.py:278
  94.5 0.0 collective-permute-done.12.refs_3_
  94.5 0.4 shard_map.147
  94.9 13.2 %all_to_all.21.parts = bf16[4,704,128]{2,1,0:T(8,128)(2,1)S(1)} all-to-all(bf16[4,704,128]{2,1,0:T(8,128)(2,1)S(1)} %shard_map.147), channel_id=1, replica_groups={{5,6,9,10},{7,4,11,8},{13,14,1,2},{15,12,3,0},{16,17,20,21},{18,19,22,2..., dimensions={0} | all-to-all | bytes 1441792 | tf_op jit(solution)/shard_map/all_to_all | solution.py:240
  108.1 0.8 shard_map.148
  108.9 10.6 %all-to-all-start.3 = ((bf16[32,22,128]{2,1,0:T(8,128)(2,1)}), bf16[32,22,128]{2,1,0:T(8,128)(2,1)S(1)}, u32[]{:S(2)}, u32[]{:S(2)}) async-start(bf16[32,22,128]{2,1,0:T(8,128)(2,1)} %shard_map.148), calls=%async_computation.3 | async-start | bytes 393216 | tf_op jit(solution)/shard_map/all_to_all | solution.py:444
  119.5 2.0 %collective-permute-start = (f32[2,64]{1,0:T(2,128)S(1)}, f32[2,64]{1,0:T(2,128)S(1)}, u32[]{:S(2)}, u32[]{:S(2)}) collective-permute-start(f32[2,64]{1,0:T(2,128)S(1)} %get-tuple-element.30), channel_id=1, source_target_pairs={{0,16},{16,32},{32,48},{48,64},{64,80},{80,96},{96,112},{112,128},... | collective-permute-start | bytes 1544 | tf_op jit(solution)/shard_map/ppermute | solution.py:21
  121.6 7.5 %collective-permute-done.halo = f32[2,64]{1,0:T(2,128)S(1)} collective-permute-done((f32[2,64]{1,0:T(2,128)S(1)}, f32[2,64]{1,0:T(2,128)S(1)}, u32[]{:S(2)}, u32[]{:S(2)}) %collective-permute-start) | collective-permute-done | bytes 544 | tf_op jit(solution)/shard_map/ppermute | solution.py:21
  129.0 1.0 shard_map.141
  130.1 1.9 %collective-permute-start.1 = (bf16[4,256,128]{2,1,0:T(8,128)(2,1)S(1)}, bf16[4,256,128]{2,1,0:T(8,128)(2,1)S(1)}, u32[]{:S(2)}, u32[]{:S(2)}) collective-permute-start(bf16[4,256,128]{2,1,0:T(8,128)(2,1)S(1)} %get-tuple-element.33), channel_id=1, source_target_pairs={{0,1},{1,0},{2,3},{3,2},{4,5},{5,4},{6,7},{7,6},{8,9},{9,8},{10,11... | collective-permute-start | bytes 786440 | tf_op jit(solution)/shard_map/ppermute | solution.py:278
  132.0 1.9 %collective-permute-start.2 = (bf16[4,256,128]{2,1,0:T(8,128)(2,1)S(1)}, bf16[4,256,128]{2,1,0:T(8,128)(2,1)S(1)}, u32[]{:S(2)}, u32[]{:S(2)}) collective-permute-start(bf16[4,256,128]{2,1,0:T(8,128)(2,1)S(1)} %get-tuple-element.34), channel_id=1, source_target_pairs={{0,4},{1,5},{2,6},{3,7},{4,0},{5,1},{6,2},{7,3},{8,12},{9,13},{10,... | collective-permute-start | bytes 786440 | tf_op jit(solution)/shard_map/ppermute | solution.py:278
  133.9 5.4 %collective-permute-start.3 = (bf16[4,256,128]{2,1,0:T(8,128)(2,1)S(1)}, bf16[4,256,128]{2,1,0:T(8,128)(2,1)S(1)}, u32[]{:S(2)}, u32[]{:S(2)}) collective-permute-start(bf16[4,256,128]{2,1,0:T(8,128)(2,1)S(1)} %get-tuple-element.35), channel_id=1, source_target_pairs={{0,5},{1,4},{2,7},{3,6},{4,1},{5,0},{6,3},{7,2},{8,13},{9,12},{10,... | collective-permute-start | bytes 786440 | tf_op jit(solution)/shard_map/ppermute | solution.py:278
  139.3 0.0 collective-permute-done.1.refs_1_
  139.3 0.9 collective-permute-done.2.refs_2_
  140.3 3.4 %collective-permute-done.3.refs_3_ = bf16[4,256,128]{2,1,0:T(8,128)(2,1)S(1)} collective-permute-done((bf16[4,256,128]{2,1,0:T(8,128)(2,1)S(1)}, bf16[4,256,128]{2,1,0:T(8,128)(2,1)S(1)}, u32[]{:S(2)}, u32[]{:S(2)}) %collective-permute-start.3) | collective-permute-done | bytes 262176 | tf_op jit(solution)/shard_map/ppermute | solution.py:278
  143.7 0.1 shard_map.142
  143.8 4.8 %collective-permute-start.4 = (bf16[256,128]{1,0:T(8,128)(2,1)S(1)}, bf16[256,128]{1,0:T(8,128)(2,1)S(1)}, u32[]{:S(2)}, u32[]{:S(2)}) collective-permute-start(bf16[256,128]{1,0:T(8,128)(2,1)S(1)} %get-tuple-element.37), channel_id=1, source_target_pairs={{0,3},{1,2},{2,1},{3,0},{4,7},{5,6},{6,5},{7,4},{8,11},{9,10},{10,... | collective-permute-start | bytes 196616 | tf_op jit(solution)/shard_map/ppermute | solution.py:278
  148.6 4.4 %collective-permute-start.5 = (bf16[256,128]{1,0:T(8,128)(2,1)S(1)}, bf16[256,128]{1,0:T(8,128)(2,1)S(1)}, u32[]{:S(2)}, u32[]{:S(2)}) collective-permute-start(bf16[256,128]{1,0:T(8,128)(2,1)S(1)} %get-tuple-element.38), channel_id=1, source_target_pairs={{0,12},{1,13},{2,14},{3,15},{4,8},{5,9},{6,10},{7,11},{8,4},{9,5},... | collective-permute-start | bytes 196616 | tf_op jit(solution)/shard_map/ppermute | solution.py:278
  153.0 2.5 %collective-permute-start.6 = (bf16[256,128]{1,0:T(8,128)(2,1)S(1)}, bf16[256,128]{1,0:T(8,128)(2,1)S(1)}, u32[]{:S(2)}, u32[]{:S(2)}) collective-permute-start(bf16[256,128]{1,0:T(8,128)(2,1)S(1)} %get-tuple-element.39), channel_id=1, source_target_pairs={{0,15},{1,14},{2,13},{3,12},{4,11},{5,10},{6,9},{7,8},{8,7},{9,6},... | collective-permute-start | bytes 196616 | tf_op jit(solution)/shard_map/ppermute | solution.py:278
  155.5 0.0 copy-start
  155.5 0.1 copy.17
  155.6 0.5 copy-done
  156.1 0.1 copy.18.scores
  156.3 0.0 collective-permute-done.4.refs_1_
  156.3 0.0 collective-permute-done.5.refs_2_
  156.3 6.2 %collective-permute-done.6.refs_3_ = bf16[256,128]{1,0:T(8,128)(2,1)S(1)} collective-permute-done((bf16[256,128]{1,0:T(8,128)(2,1)S(1)}, bf16[256,128]{1,0:T(8,128)(2,1)S(1)}, u32[]{:S(2)}, u32[]{:S(2)}) %collective-permute-start.6) | collective-permute-done | bytes 65568 | tf_op jit(solution)/shard_map/ppermute | solution.py:278
  162.5 0.7 shard_map.143
  163.1 1.1 shard_map.149
  (1 shorter events, 0.0 us)
Async XLA Ops:
  3.4 27.2 %all-to-all-start = ((bf16[32,22,128]{2,1,0:T(8,128)(2,1)}), bf16[32,22,128]{2,1,0:T(8,128)(2,1)S(1)}, u32[]{:S(2)}, u32[]{:S(2)}) async-start(bf16[32,22,128]{2,1,0:T(8,128)(2,1)} %get-tuple-element.40), calls=%async_computation | async-start | bytes 393216 | tf_op jit(solution)/shard_map/all_to_all | solution.py:368
  44.3 13.2 %collective-permute-start.7 = (bf16[4,704,128]{2,1,0:T(8,128)(2,1)S(1)}, bf16[4,704,128]{2,1,0:T(8,128)(2,1)S(1)}, u32[]{:S(2)}, u32[]{:S(2)}) collective-permute-start(bf16[4,704,128]{2,1,0:T(8,128)(2,1)S(1)} %all_to_all.20.refs_0_), channel_id=1, source_target_pairs={{0,1},{1,0},{2,3},{3,2},{4,5},{5,4},{6,7},{7,6},{8,9},{9,8},{10,11... | collective-permute-start | bytes 2162696 | tf_op jit(solution)/shard_map/ppermute | solution.py:278
  46.7 20.9 %collective-permute-start.8 = (bf16[4,704,128]{2,1,0:T(8,128)(2,1)S(1)}, bf16[4,704,128]{2,1,0:T(8,128)(2,1)S(1)}, u32[]{:S(2)}, u32[]{:S(2)}) collective-permute-start(bf16[4,704,128]{2,1,0:T(8,128)(2,1)S(1)} %all_to_all.20.refs_0_), channel_id=1, source_target_pairs={{0,4},{1,5},{2,6},{3,7},{4,0},{5,1},{6,2},{7,3},{8,12},{9,13},{10,... | collective-permute-start | bytes 2162696 | tf_op jit(solution)/shard_map/ppermute | solution.py:278
  49.5 18.1 %collective-permute-start.9 = (bf16[4,704,128]{2,1,0:T(8,128)(2,1)S(1)}, bf16[4,704,128]{2,1,0:T(8,128)(2,1)S(1)}, u32[]{:S(2)}, u32[]{:S(2)}) collective-permute-start(bf16[4,704,128]{2,1,0:T(8,128)(2,1)S(1)} %all_to_all.20.refs_0_), channel_id=1, source_target_pairs={{0,5},{1,4},{2,7},{3,6},{4,1},{5,0},{6,3},{7,2},{8,13},{9,12},{10,... | collective-permute-start | bytes 2162696 | tf_op jit(solution)/shard_map/ppermute | solution.py:278
  70.2 13.2 %collective-permute-start.10 = (bf16[4,704,128]{2,1,0:T(8,128)(2,1)S(1)}, bf16[4,704,128]{2,1,0:T(8,128)(2,1)S(1)}, u32[]{:S(2)}, u32[]{:S(2)}) collective-permute-start(bf16[4,704,128]{2,1,0:T(8,128)(2,1)S(1)} %get-tuple-element.48), channel_id=1, source_target_pairs={{0,1},{1,0},{2,3},{3,2},{4,5},{5,4},{6,7},{7,6},{8,9},{9,8},{10,11... | collective-permute-start | bytes 2162696 | tf_op jit(solution)/shard_map/ppermute | solution.py:278
  73.6 20.9 %collective-permute-start.11 = (bf16[4,704,128]{2,1,0:T(8,128)(2,1)S(1)}, bf16[4,704,128]{2,1,0:T(8,128)(2,1)S(1)}, u32[]{:S(2)}, u32[]{:S(2)}) collective-permute-start(bf16[4,704,128]{2,1,0:T(8,128)(2,1)S(1)} %get-tuple-element.49), channel_id=1, source_target_pairs={{0,4},{1,5},{2,6},{3,7},{4,0},{5,1},{6,2},{7,3},{8,12},{9,13},{10,... | collective-permute-start | bytes 2162696 | tf_op jit(solution)/shard_map/ppermute | solution.py:278
  76.0 18.5 %collective-permute-start.12 = (bf16[4,704,128]{2,1,0:T(8,128)(2,1)S(1)}, bf16[4,704,128]{2,1,0:T(8,128)(2,1)S(1)}, u32[]{:S(2)}, u32[]{:S(2)}) collective-permute-start(bf16[4,704,128]{2,1,0:T(8,128)(2,1)S(1)} %get-tuple-element.50), channel_id=1, source_target_pairs={{0,5},{1,4},{2,7},{3,6},{4,1},{5,0},{6,3},{7,2},{8,13},{9,12},{10,... | collective-permute-start | bytes 2162696 | tf_op jit(solution)/shard_map/ppermute | solution.py:278
  108.9 54.2 %all-to-all-start.3 = ((bf16[32,22,128]{2,1,0:T(8,128)(2,1)}), bf16[32,22,128]{2,1,0:T(8,128)(2,1)S(1)}, u32[]{:S(2)}, u32[]{:S(2)}) async-start(bf16[32,22,128]{2,1,0:T(8,128)(2,1)} %shard_map.148), calls=%async_computation.3 | async-start | bytes 393216 | tf_op jit(solution)/shard_map/all_to_all | solution.py:444
  119.5 9.5 %collective-permute-start = (f32[2,64]{1,0:T(2,128)S(1)}, f32[2,64]{1,0:T(2,128)S(1)}, u32[]{:S(2)}, u32[]{:S(2)}) collective-permute-start(f32[2,64]{1,0:T(2,128)S(1)} %get-tuple-element.30), channel_id=1, source_target_pairs={{0,16},{16,32},{32,48},{48,64},{64,80},{80,96},{96,112},{112,128},... | collective-permute-start | bytes 1544 | tf_op jit(solution)/shard_map/ppermute | solution.py:21
  130.1 9.2 %collective-permute-start.1 = (bf16[4,256,128]{2,1,0:T(8,128)(2,1)S(1)}, bf16[4,256,128]{2,1,0:T(8,128)(2,1)S(1)}, u32[]{:S(2)}, u32[]{:S(2)}) collective-permute-start(bf16[4,256,128]{2,1,0:T(8,128)(2,1)S(1)} %get-tuple-element.33), channel_id=1, source_target_pairs={{0,1},{1,0},{2,3},{3,2},{4,5},{5,4},{6,7},{7,6},{8,9},{9,8},{10,11... | collective-permute-start | bytes 786440 | tf_op jit(solution)/shard_map/ppermute | solution.py:278
  132.0 8.3 %collective-permute-start.2 = (bf16[4,256,128]{2,1,0:T(8,128)(2,1)S(1)}, bf16[4,256,128]{2,1,0:T(8,128)(2,1)S(1)}, u32[]{:S(2)}, u32[]{:S(2)}) collective-permute-start(bf16[4,256,128]{2,1,0:T(8,128)(2,1)S(1)} %get-tuple-element.34), channel_id=1, source_target_pairs={{0,4},{1,5},{2,6},{3,7},{4,0},{5,1},{6,2},{7,3},{8,12},{9,13},{10,... | collective-permute-start | bytes 786440 | tf_op jit(solution)/shard_map/ppermute | solution.py:278
  133.9 9.7 %collective-permute-start.3 = (bf16[4,256,128]{2,1,0:T(8,128)(2,1)S(1)}, bf16[4,256,128]{2,1,0:T(8,128)(2,1)S(1)}, u32[]{:S(2)}, u32[]{:S(2)}) collective-permute-start(bf16[4,256,128]{2,1,0:T(8,128)(2,1)S(1)} %get-tuple-element.35), channel_id=1, source_target_pairs={{0,5},{1,4},{2,7},{3,6},{4,1},{5,0},{6,3},{7,2},{8,13},{9,12},{10,... | collective-permute-start | bytes 786440 | tf_op jit(solution)/shard_map/ppermute | solution.py:278
  143.8 12.5 %collective-permute-start.4 = (bf16[256,128]{1,0:T(8,128)(2,1)S(1)}, bf16[256,128]{1,0:T(8,128)(2,1)S(1)}, u32[]{:S(2)}, u32[]{:S(2)}) collective-permute-start(bf16[256,128]{1,0:T(8,128)(2,1)S(1)} %get-tuple-element.37), channel_id=1, source_target_pairs={{0,3},{1,2},{2,1},{3,0},{4,7},{5,6},{6,5},{7,4},{8,11},{9,10},{10,... | collective-permute-start | bytes 196616 | tf_op jit(solution)/shard_map/ppermute | solution.py:278
  148.6 7.7 %collective-permute-start.5 = (bf16[256,128]{1,0:T(8,128)(2,1)S(1)}, bf16[256,128]{1,0:T(8,128)(2,1)S(1)}, u32[]{:S(2)}, u32[]{:S(2)}) collective-permute-start(bf16[256,128]{1,0:T(8,128)(2,1)S(1)} %get-tuple-element.38), channel_id=1, source_target_pairs={{0,12},{1,13},{2,14},{3,15},{4,8},{5,9},{6,10},{7,11},{8,4},{9,5},... | collective-permute-start | bytes 196616 | tf_op jit(solution)/shard_map/ppermute | solution.py:278
  153.0 9.5 %collective-permute-start.6 = (bf16[256,128]{1,0:T(8,128)(2,1)S(1)}, bf16[256,128]{1,0:T(8,128)(2,1)S(1)}, u32[]{:S(2)}, u32[]{:S(2)}) collective-permute-start(bf16[256,128]{1,0:T(8,128)(2,1)S(1)} %get-tuple-element.39), channel_id=1, source_target_pairs={{0,15},{1,14},{2,13},{3,12},{4,11},{5,10},{6,9},{7,8},{8,7},{9,6},... | collective-permute-start | bytes 196616 | tf_op jit(solution)/shard_map/ppermute | solution.py:278
  155.5 0.7 copy-start
